TPU v7x, 256 devices: a whole 4x4x8 slice. The times are simulated.
256 devices in a mesh: sp: 32 (over z, x), tp: 8 (over y, core).
Axes of the slice: x: 4, y: 4, z: 8, core: 2. Of those that a mesh axis runs over, the one named last changes fastest.
Arguments:
- hidden_in: bfloat16 [12288, 2048], P('sp', 'tp'), may hold values from -6 to 6
- in_gain: float32 [2048], replicated, may hold values from 0.1 to 1.9
- receptance_weight: bfloat16 [2048, 1024], P(None, 'tp'), may hold values from -0.125 to 0.125
- key_weight: bfloat16 [2048, 1024], P(None, 'tp'), may hold values from -0.125 to 0.125
- value_weight: bfloat16 [2048, 1024], P(None, 'tp'), may hold values from -0.125 to 0.125
- decay_down: bfloat16 [2048, 128], replicated, may hold values from -0.125 to 0.125
- decay_up: bfloat16 [128, 1024], P(None, 'tp'), may hold values from -0.5 to 0.5
- decay_base: float32 [1024], P('tp'), may hold values from -14 to -2
- decay_shift: float32 [12288, 1024], P('sp', 'tp'), may hold values from -1 to 0
- learn_rate: float32 [1024], P('tp'), may hold values from 0 to 1
- query_pair: bfloat16 [2048, 8, 128], P(None, 'tp'), may hold values from -1 to 1
- key_pair: bfloat16 [2048, 8, 128], P(None, 'tp'), may hold values from -1 to 1
- value_pair: bfloat16 [2048, 8, 128], P(None, 'tp'), may hold values from -0.125 to 0.125
- mix_lambda: float32 [8], P('tp'), may hold values from 0.3 to 0.8
- out_recurrent: bfloat16 [1024, 2048], P('tp'), may hold values from -0.1875 to 0.1875
- out_attention: bfloat16 [1024, 2048], P('tp'), may hold values from -0.1875 to 0.1875
- out_gain: float32 [2048], replicated, may hold values from 0.1 to 1.9
Outputs:
- layer_out: bfloat16 [12288, 2048], P(('sp', 'tp'))
- log_sums: float32 [8, 2, 12288], P('tp', None, 'sp')
All inputs are finite; a program needn't handle non-finite values.
Results may differ from a plain program's by a relative error of at most 0.018.
Values may be sent and summed in bfloat16 or wider, within the bound.
No kernel may reach another device: no remote copies, remote signals or barrier semaphores. Data moves between devices by JAX's collectives and lax.ppermute only.
A program may use at most 128 MiB of HBM per device.

v0:
```python
import functools
import math

import jax
import jax.numpy as jnp
from jax import lax
from jax.experimental import pallas as pl
from jax.experimental.pallas import tpu as pltpu
from jax.sharding import Mesh
from jax.sharding import PartitionSpec as P

HD = 64
F32 = jnp.float32
BF16 = jnp.bfloat16
HIGHEST = lax.Precision.HIGHEST
DECAY_SCALE = math.exp(-0.5)
NORM_EPS = 1e-06
GROUP_EPS = 0.00064
HEAD_EPS = 1e-05
KEY_EPS = 1e-06
NEGATIVE = -1e30
SPAN = 64
VMEM_LIMIT = 60 * 1024 * 1024
NT = (((1,), (1,)), ((), ()))
TN = (((0,), (0,)), ((), ()))
NN = (((1,), (0,)), ((), ()))


def call(kernel, outs, scalars, arrays, scratch=(), flops=0, name=None):
    return pl.pallas_call(
        kernel,
        out_shape=outs,
        in_specs=[pl.BlockSpec(memory_space=pltpu.SMEM)] * len(scalars)
        + [pl.BlockSpec(memory_space=pltpu.VMEM)] * len(arrays),
        out_specs=jax.tree.map(lambda _: pl.BlockSpec(memory_space=pltpu.VMEM), outs),
        scratch_shapes=list(scratch),
        compiler_params=pltpu.CompilerParams(vmem_limit_bytes=VMEM_LIMIT),
        cost_estimate=pl.CostEstimate(flops=flops, bytes_accessed=flops // 1000, transcendentals=0),
        name=name,
    )(*scalars, *arrays)


def dot(left, right, dims=NN, precision=None):
    return lax.dot_general(left, right, dims, precision=precision, preferred_element_type=F32)


def exact(left, right, dims=NN):
    return dot(left, right, dims, HIGHEST)


def ring(size, shift):
    return [(i, (i + shift) % size) for i in range(size)]


def lane_ids(shape):
    return lax.broadcasted_iota(jnp.int32, shape, len(shape) - 1)


def row_ids(shape):
    return lax.broadcasted_iota(jnp.int32, shape, len(shape) - 2)


def project_kernel(
    piece_ref,
    h0, h1, h2, h3, h4, g0, g1, g2, g3, g4,
    gain_ref, wq, wkp, wvp,
    normed, q_out, kv_out,
):
    pieces = []
    for own, up, down, far_a, far_b in ((h0, h1, h2, h3, h4), (g0, g1, g2, g3, g4)):
        pieces += [own[...], up[...], down[...], jnp.concatenate([far_a[...], far_b[...]], axis=0)]
    squares = None
    for piece in pieces:
        wide = piece.astype(F32)
        part = wide * wide
        part = part[:, :128] + part[:, 128:]
        squares = part if squares is None else squares + part
    scale = lax.rsqrt(jnp.sum(squares, axis=-1, keepdims=True) / 2048.0 + NORM_EPS)
    for number, piece in enumerate(pieces):
        place = piece_ref[number]
        gain = gain_ref[pl.ds(place, 1), :]
        value = (piece.astype(F32) * scale * gain).astype(BF16)
        normed[:, pl.ds(pl.multiple_of(place * 256, 256), 256)] = value
    kv_out[...] = dot(normed[...], jnp.concatenate([wkp[...], wvp[...]], axis=1)).astype(BF16)
    q_out[...] = dot(normed[...], wq[...]).astype(BF16)


def same_head():
    return (row_ids((128, 128)) < HD) == (lane_ids((128, 128)) < HD)


def diagonal_mask():
    return row_ids((128, 128)) == lane_ids((128, 128))


def compose(earlier, later, same):
    return exact(earlier, jnp.where(same, later, 0.0)) + jnp.where(same, 0.0, later)


def chunk_kernel(
    normed, wr, wk, wv, wd, up_ref, base_ref, shift_ref, rate_ref,
    lower_out, reading_out, rhs_out, turned_out, reads_out, ends_out, last_out,
):
    both = dot(normed[...], jnp.concatenate([wr[...], wk[...]], axis=1))
    all_reads = both[:, :128].astype(BF16)
    all_keys = both[:, 128:].astype(BF16)
    both = dot(normed[...], jnp.concatenate([wv[...], wd[...]], axis=1))
    all_values = both[:, :128].astype(BF16)
    low = jnp.tanh(both[:, 128:]).astype(BF16)
    pre = dot(low, up_ref[...]) + base_ref[...]
    all_decay = -DECAY_SCALE * jax.nn.sigmoid(pre) + shift_ref[...]
    rows = normed.shape[0]
    count = rows // SPAN
    ones_block = jnp.where(same_head(), 1.0, 0.0).astype(F32)
    first = lane_ids((SPAN, 128)) < HD
    t_ids = row_ids((SPAN, 128))
    s_ids = lane_ids((SPAN, 128)) % HD
    strict = s_ids < t_ids
    causal = s_ids <= t_ids
    tri = jnp.where(row_ids((SPAN, SPAN)) >= lane_ids((SPAN, SPAN)), 1.0, 0.0).astype(F32)
    keep = (first, jnp.logical_not(first))
    zero = jnp.zeros((SPAN, 128), F32)
    for c in range(count):
        at = slice(c * SPAN, (c + 1) * SPAN)
        decay = all_decay[at, :]
        running = exact(tri, decay)
        before = running - decay
        middle = running[SPAN // 2 - 1 : SPAN // 2, :]
        ending = running[SPAN - 1 : SPAN, :]
        keys = all_keys[at, :].astype(F32)
        reads = all_reads[at, :].astype(F32)
        values = all_values[at, :].astype(F32)
        unit_keys = keys * lax.rsqrt(exact(keys * keys, ones_block) + KEY_EPS)
        erasing = unit_keys * rate_ref[...]
        grow = jnp.exp(middle - running)
        against = -unit_keys * jnp.exp(before - middle)
        read_scaled = reads * jnp.exp(running - middle)
        right = jnp.concatenate([erasing * grow, keys * grow], axis=0)
        left = jnp.concatenate(
            [jnp.where(k, side, 0.0) for k in keep for side in (against, read_scaled)], axis=0
        )
        scores = exact(left, right, NT)
        turned = pltpu.roll(values, HD, 1)
        to_end = jnp.exp(ending - running)
        ends_out[c] = jnp.concatenate([erasing * to_end, keys * to_end], axis=0)
        start = -unit_keys * jnp.exp(before)
        reads_out[c] = reads * jnp.exp(running)
        last_out[c] = jnp.broadcast_to(jnp.exp(ending), (8, 128))
        turned_out[c] = turned
        for h in range(2):
            lower = jnp.where(strict, scores[128 * h : 128 * h + SPAN], 0.0)
            lower_out[2 * c + h] = lower
            reading_out[2 * c + h] = jnp.where(causal, scores[128 * h + SPAN : 128 * h + 128], 0.0)
            side_values = jnp.where(keep[h], 0.0, turned)
            rhs_out[2 * c + h] = jnp.where(keep[h], start, 0.0) + exact(
                lower, jnp.concatenate([zero, side_values], axis=0)
            )


def recurrent_kernel(
    lower_ref, reading_ref, rhs_ref, turned_ref, reads_ref, ends_ref, last_ref, query_ref,
    read_out, local_out, message_out,
):
    count = turned_ref.shape[0]
    rows = count * SPAN
    same = same_head()
    diagonal = diagonal_mask()
    first = lane_ids((SPAN, 128)) < HD
    keep = (first, jnp.logical_not(first))
    solved = []
    group = 4
    for base in range(0, 2 * count, group):
        lowers = [lower_ref[base + n] for n in range(group)]
        state = [[rhs_ref[base + n, 8 * b : 8 * b + 8] for b in range(SPAN // 8)] for n in range(group)]
        for s in range(SPAN - 1):
            for n in range(group):
                row = state[n][s // 8][s % 8 : s % 8 + 1]
                for b in range(s // 8 if s % 8 < 7 else s // 8 + 1, SPAN // 8):
                    state[n][b] = state[n][b] + lowers[n][8 * b : 8 * b + 8, s : s + 1] * row
        solved += [jnp.concatenate(one, axis=0) for one in state]
    prefix = jnp.where(diagonal, 1.0, 0.0).astype(F32)
    for c in range(count):
        got, moved = [], []
        for h in range(2):
            side_values = jnp.where(keep[h], 0.0, turned_ref[c])
            both = jnp.concatenate([solved[2 * c + h], side_values], axis=0)
            got.append(exact(reading_ref[2 * c + h], both))
            moved.append(exact(both, ends_ref[c], TN))
        lanes = lane_ids((128, 128)) < HD
        step = jnp.where(lanes, moved[0], moved[1]) + jnp.where(diagonal, last_ref[c, :1], 0.0)
        read_state = jnp.where(first, got[0], got[1]) + reads_ref[c]
        local = jnp.where(first, got[1], got[0])
        at = slice(c * SPAN, (c + 1) * SPAN)
        read_out[at, :] = exact(read_state, jnp.where(same, prefix, 0.0), NT)
        local_out[at, :] = local + exact(read_state, jnp.where(same, 0.0, prefix), NT)
        prefix = compose(prefix, step, same)
    message_out[:rows, :] = query_ref[...]
    message_out[rows:, :] = prefix.astype(BF16)


def along_x_kernel(place_ref, m0, m1, m2, m3, before_out, total_out, parts):
    rows = m0.shape[0] - 128
    same = same_head()
    identity = jnp.where(diagonal_mask(), 1.0, 0.0).astype(F32)
    mine = place_ref[1]
    for n, ref in enumerate((m0, m1, m2, m3)):
        parts[place_ref[10 + n]] = ref[rows:, :].astype(F32)
    total = compose(
        compose(parts[0], parts[1], same), compose(parts[2], parts[3], same), same
    ).astype(BF16)
    for n in range(8):
        total_out[n] = total
    kept = [jnp.where(j < mine, parts[j], identity) for j in range(3)]
    before_out[...] = compose(compose(kept[0], kept[1], same), kept[2], same)


def along_z_kernel(place_ref, parts_ref, before_ref, state_out):
    same = same_head()
    identity = jnp.where(diagonal_mask(), 1.0, 0.0).astype(F32)
    mine = place_ref[0]
    level = [jnp.where(j < mine, parts_ref[j].astype(F32), identity) for j in range(7)]
    level.append(before_ref[...])
    while len(level) > 1:
        level = [compose(level[i], level[i + 1], same) for i in range(0, len(level), 2)]
    state_out[...] = jnp.where(same, 0.0, level[0])


TALL = 144


def attention_kernel(blocks, is_first, is_last, *refs):
    place_ref, refs = refs[0], refs[1:]
    messages, refs = refs[:4], refs[4:]
    kvs, refs = refs[: len(blocks)], refs[len(blocks) :]
    if not is_first:
        (max_in, sum_in), refs = refs[:2], refs[2:]
    count = 4 if is_last else 2
    outs, refs = refs[:count], refs[count:]
    row_max, weighted, queries, keys, turned, scores, weights, rescales, units = refs
    rows = messages[0].shape[0] - 128
    my_z, my_x = place_ref[0], place_ref[1]
    first = lane_ids((rows, 128)) < HD
    for n, ref in enumerate(messages):
        scaled = (ref[:rows, :].astype(F32) * (HD**-0.5)).astype(BF16)
        queries[2 * n] = jnp.where(first, scaled, 0).astype(BF16)
        queries[2 * n + 1] = jnp.where(first, 0, scaled).astype(BF16)
    ones = jnp.where(row_ids((TALL - 128, rows)) == 0, 1.0, 0.0).astype(BF16)
    for n, ref in enumerate(kvs):
        keys[n] = ref[:, :128]
        turned[n, :128, :] = jnp.transpose(ref[:, 128:])
        turned[n, 128:, :] = ones
    if is_first:
        row_max[...] = jnp.full_like(row_max, NEGATIVE)
        weighted[...] = jnp.zeros_like(weighted)
    else:
        row_max[:8] = max_in[...]
        weighted[:8] = sum_in[...]

    def score(q, n, out):
        for m in range(2):
            out[m] = dot(keys[n], queries[2 * q + m], NT)

    def soften(slot, source, target, factors, diagonal=False):
        for m in range(2):
            i = 2 * slot + m
            got = source[m]
            if diagonal:
                allowed = row_ids((rows, rows)) <= lane_ids((rows, rows))
                got = jnp.where(allowed, got, NEGATIVE)
            old = row_max[i, :1, :]
            new = jnp.maximum(old, jnp.max(got, axis=0, keepdims=True))
            target[m] = jnp.exp(got - new).astype(BF16)
            factors[m] = jnp.broadcast_to(jnp.exp(old - new), (8, rows))
            row_max[i] = jnp.broadcast_to(new, (8, rows))

    def gather(slot, n, source, factors):
        for m in range(2):
            i = 2 * slot + m
            weighted[i] = weighted[i] * factors[m, :1, :] + dot(turned[n], source[m])

    def put(at, q, n, slot):
        units[0, at] = q
        units[1, at] = n
        units[2, at] = slot

    put(0, 0, 0, 4)
    total = jnp.int32(1)
    for n, number in enumerate(blocks):
        for q in range(4):
            put(total, q, n, q)
            wanted = place_ref[10 + q] > my_x if number == 0 else place_ref[2 + number] < my_z
            total = total + wanted.astype(jnp.int32)
    for extra in range(4):
        put(total + extra, 0, 0, 4)

    if is_first:
        score(0, 0, scores[0])
        soften(0, scores[0], weights[0], rescales[0], True)
        gather(0, 0, weights[0], rescales[0])

    @pl.when(total > 1)
    def _():
        score(units[0, 1], units[1, 1], scores[1])

        def step(at, now, other):
            score(units[0, at + 1], units[1, at + 1], scores[other])
            soften(units[2, at], scores[now], weights[now], rescales[now])
            gather(units[2, at - 1], units[1, at - 1], weights[other], rescales[other])

        def two(t, carry):
            step(2 * t + 1, 1, 0)
            step(2 * t + 2, 0, 1)
            return carry

        lax.fori_loop(0, (total + 1) // 2, two, 0)

    if is_last:
        for q, out in enumerate(outs):
            for m in range(2):
                i = 2 * q + m
                row_sum = weighted[i, 128:129, :]
                some = row_sum > 0.0
                safe = jnp.where(some, row_sum, 1.0)
                out[m, :128, :] = (weighted[i, :128, :] * (1.0 / safe)).astype(BF16)
                logs = jnp.where(some, row_max[i, :1, :] + jnp.log(safe), NEGATIVE)
                high = logs.astype(BF16).astype(F32)
                middle = (logs - high).astype(BF16).astype(F32)
                low = logs - high - middle
                tail = [high, middle, low, jnp.zeros((TALL - 131, rows), F32)]
                out[m, 128:, :] = jnp.concatenate(tail, axis=0).astype(BF16)
    else:
        outs[0][...] = row_max[:8]
        outs[1][...] = weighted[:8]


def finish_kernel(
    place_ref, lambda_ref, p0, p1, p2, p3, read_ref, local_ref, state_ref, wr_ref, wa_ref,
    mine_out, other_out, logs_out,
):
    rows = read_ref.shape[0]
    parts = (p0, p1, p2, p3)
    maps = []
    for m in range(2):
        logs = []
        for p in parts:
            tail = p[m, 128:, :].astype(F32)
            logs.append(tail[:1] + tail[1:2] + tail[2:3])
        top = functools.reduce(jnp.maximum, logs)
        shares = [jnp.exp(a - top) for a in logs]
        total = functools.reduce(jnp.add, shares)
        logs_out[m : m + 1, :] = top + jnp.log(total)
        got = None
        for p, share in zip(parts, shares):
            term = p[m, :128, :].astype(F32) * (share / total)
            got = term if got is None else got + term
        maps.append(got)
    head = maps[0] - lambda_ref[0] * maps[1]
    head = head * lax.rsqrt(jnp.mean(head * head, axis=0, keepdims=True) + HEAD_EPS)
    att_mix = jnp.transpose(head.astype(BF16))
    recurrent = local_ref[...] + exact(read_ref[...], state_ref[...], NT)
    recurrent = pltpu.roll(recurrent, HD, 1)
    first = lane_ids((rows, 128)) < HD

    def per_head(values):
        low = jnp.sum(jnp.where(first, values, 0.0), axis=-1, keepdims=True)
        high = jnp.sum(jnp.where(first, 0.0, values), axis=-1, keepdims=True)
        return jnp.where(first, low, high) / HD

    centered = recurrent - per_head(recurrent)
    rec_mix = (centered * lax.rsqrt(per_head(centered * centered) + GROUP_EPS)).astype(BF16)
    mix = jnp.concatenate([rec_mix, att_mix], axis=1)
    core = place_ref[0]
    for n in range(8):
        at = slice(256 * n, 256 * n + 256)
        weight = jnp.concatenate([wr_ref[:, at], wa_ref[:, at]], axis=0)
        got = dot(mix, weight).astype(BF16)
        for y in range(4):
            even = got[96 * y : 96 * y + 48]
            odd = got[96 * y + 48 : 96 * y + 96]
            mine_out[y, :, at] = jnp.where(core == 0, even, odd)
            other_out[y, :, at] = jnp.where(core == 0, odd, even)


def rms_rows(values, gain):
    return values * lax.rsqrt(jnp.mean(values * values, axis=-1, keepdims=True) + NORM_EPS) * gain


def per_device(
    hidden_in, in_gain, receptance_weight, key_weight, value_weight, decay_down, decay_up,
    decay_base, decay_shift, learn_rate, query_pair, key_pair, value_pair, mix_lambda,
    out_recurrent, out_attention, out_gain,
):
    permute = lax.ppermute
    together = lax.optimization_barrier
    z, x, y, core = (lax.axis_index(a) for a in ("z", "x", "y", "c"))
    rows = hidden_in.shape[0]
    half = rows // 2
    count = rows // SPAN
    shaped = jax.ShapeDtypeStruct

    up = permute(hidden_in, "y", ring(4, 1))
    down = permute(hidden_in, "y", ring(4, -1))
    far_a = permute(up[:half], "y", ring(4, 1))
    far_b = permute(down[half:], "y", ring(4, -1))
    mine = [hidden_in, up, down, far_a, far_b]
    theirs = [permute(a, "c", ring(2, 1)) for a in mine]
    ys = jnp.stack([y, (y + 3) % 4, (y + 1) % 4, (y + 2) % 4])
    piece_at = jnp.concatenate([ys * 2 + core, ys * 2 + 1 - core]).astype(jnp.int32)
    places = jnp.stack(
        [z, x, z]
        + [a for s in (1, 2, 3) for a in ((z + 8 - s) % 8, (z + s) % 8)]
        + [(z + 4) % 8, x, (x + 3) % 4, (x + 1) % 4, (x + 2) % 4]
    ).astype(jnp.int32)

    normed, q, kv = call(
        project_kernel,
        (shaped((rows, 2048), BF16), shaped((rows, 128), BF16), shaped((rows, 256), BF16)),
        (piece_at,),
        (
            *mine, *theirs, in_gain.reshape(8, 256), query_pair.reshape(2048, 128),
            key_pair.reshape(2048, 128), value_pair.reshape(2048, 128),
        ),
        flops=2 * rows * 2048 * 896,
        name="project",
    )

    right = permute(kv, "z", ring(8, 1))
    left = permute(kv, "z", ring(8, -1))
    tile = (2 * count, SPAN, 128)
    chunked = call(
        chunk_kernel,
        (
            shaped(tile, F32), shaped(tile, F32), shaped(tile, F32), shaped((count, SPAN, 128), F32),
            shaped((count, SPAN, 128), F32), shaped((count, 128, 128), F32), shaped((count, 8, 128), F32),
        ),
        (),
        (
            normed, receptance_weight, key_weight, value_weight, decay_down, decay_up,
            decay_base.reshape(1, 128), decay_shift, learn_rate.reshape(1, 128),
        ),
        flops=6 * 10**9,
        name="chunks",
    )
    right1, left1, chunked, q = together((right, left, chunked, q))
    right = permute(right1, "z", ring(8, 1))
    left = permute(left1, "z", ring(8, -1))
    read, local, message = call(
        recurrent_kernel,
        (shaped((rows, 128), F32), shaped((rows, 128), F32), shaped((rows + 128, 128), BF16)),
        (),
        (*chunked, q),
        flops=6 * 10**9,
        name="recurrent",
    )
    right2, left2, message = together((right, left, message))
    messages = [
        message,
        permute(message, "x", ring(4, 1)),
        permute(message, "x", ring(4, -1)),
        permute(message, "x", ring(4, 2)),
    ]
    right = permute(right2, "z", ring(8, 1))
    left = permute(left2, "z", ring(8, -1))
    before, line = call(
        along_x_kernel,
        (shaped((128, 128), F32), shaped((8, 128, 128), BF16)),
        (places,), messages, scratch=(pltpu.VMEM((4, 128, 128), F32),), flops=10**8, name="along_x",
    )
    right3, left3, line, messages = together((right, left, line, messages))
    line_parts = lax.all_to_all(line, "z", 0, 0, tiled=True)
    right4 = permute(right3, "z", ring(8, 1))

    carry = (shaped((8, 8, rows), F32), shaped((8, TALL, rows), F32))
    payload = shaped((2, TALL, rows), BF16)

    def attend(blocks, arrays, carried, last=False):
        pair = lambda shape, kind: [pltpu.VMEM(shape, kind)] * 2
        return call(
            functools.partial(attention_kernel, blocks, not carried, last),
            (payload,) * 4 if last else carry,
            (places,),
            (*messages, *arrays, *carried),
            scratch=[
                pltpu.VMEM((10, 8, rows), F32), pltpu.VMEM((10, TALL, rows), F32),
                pltpu.VMEM((8, rows, 128), BF16), pltpu.VMEM((len(blocks), rows, 128), BF16),
                pltpu.VMEM((len(blocks), TALL, rows), BF16), pair((2, rows, rows), F32),
                pair((2, rows, rows), BF16), pair((2, 8, rows), F32), pltpu.SMEM((3, 32), jnp.int32),
            ],
            flops=2 * len(blocks) * 10**9,
            name=f"attention{len(blocks)}",
        )

    carried = attend((0, 1, 2, 3, 4), (kv, right1, left1, right2, left2), ())
    outs = attend((5, 6, 7), (right3, left3, right4), tuple(carried), last=True)
    back = [
        outs[0],
        permute(outs[1], "x", ring(4, -1)),
        permute(outs[2], "x", ring(4, 1)),
        permute(outs[3], "x", ring(4, 2)),
    ]
    state = call(
        along_z_kernel, shaped((128, 128), F32), (places,), (line_parts, before),
        flops=10**8, name="along_z",
    )
    ours, others, log_sums = call(
        finish_kernel,
        (shaped((4, rows // 8, 2048), BF16), shaped((4, rows // 8, 2048), BF16), shaped((2, rows), F32)),
        (core.reshape(1), mix_lambda),
        (*back, read, local, state, out_recurrent, out_attention),
        flops=10**9,
        name="finish",
    )
    theirs = permute(others, "c", ring(2, 1))
    summed = (ours.astype(F32) + theirs.astype(F32)).astype(BF16)
    parts = lax.all_to_all(summed, "y", 0, 0, tiled=True)
    projected = jnp.sum(parts.astype(F32), axis=0)
    layer_out = rms_rows(projected, out_gain).astype(BF16)
    return (layer_out, log_sums[None])


def solution(mesh):
    split = Mesh(mesh.devices.reshape(8, 4, 4, 2), ("z", "x", "y", "c"))
    sp, tp = ("z", "x"), ("y", "c")
    placed = (
        P(sp, tp), P(), P(None, tp), P(None, tp), P(None, tp), P(), P(None, tp), P(tp), P(sp, tp),
        P(tp), P(None, tp, None), P(None, tp, None), P(None, tp, None), P(tp), P(tp, None),
        P(tp, None), P(),
    )
    return jax.shard_map(
        per_device,
        mesh=split,
        in_specs=placed,
        out_specs=(P(("z", "x", "y", "c"), None), P(tp, None, sp)),
        check_vma=False,
    )
```

profile of v0, /device:TPU:224, one launch (start us, length us, event | category | flops | bytes accessed | tf_op | source)
XLA Modules:
  0.0 129.7 jit_solution(2287242379240177244)
XLA Ops:
  0.6 1.7 %collective-permute-start = (bf16[384,256]{1,0:T(8,128)(2,1)}, bf16[384,256]{1,0:T(8,128)(2,1)S(1)}, u32[]{:S(2)}, u32[]{:S(2)}) collective-permute-start(bf16[384,256]{1,0:T(8,128)(2,1)} %h0.1), channel_id=1, source_target_pairs={{0,2},{2,4},{4,6},{6,0},{1,3},{3,5},{5,7},{7,1},{8,10},{10,12},{12... | collective-permute-start | bytes 589832 | tf_op jit(solution)/shard_map/ppermute | solution.py:401
  2.3 1.7 %collective-permute-start.1 = (bf16[384,256]{1,0:T(8,128)(2,1)}, bf16[384,256]{1,0:T(8,128)(2,1)S(1)}, u32[]{:S(2)}, u32[]{:S(2)}) collective-permute-start(bf16[384,256]{1,0:T(8,128)(2,1)} %h0.1), channel_id=1, source_target_pairs={{0,6},{2,0},{4,2},{6,4},{1,7},{3,1},{5,3},{7,5},{8,14},{10,8},{12,... | collective-permute-start | bytes 589832 | tf_op jit(solution)/shard_map/ppermute | solution.py:402
  4.0 4.8 %collective-permute-done.h1 = bf16[384,256]{1,0:T(8,128)(2,1)S(1)} collective-permute-done((bf16[384,256]{1,0:T(8,128)(2,1)}, bf16[384,256]{1,0:T(8,128)(2,1)S(1)}, u32[]{:S(2)}, u32[]{:S(2)}) %collective-permute-start) | collective-permute-done | bytes 196640 | tf_op jit(solution)/shard_map/ppermute | solution.py:401
  9.2 3.0 %collective-permute-start.3 = (bf16[192,256]{1,0:T(8,128)(2,1)S(1)}, bf16[192,256]{1,0:T(8,128)(2,1)S(1)}, u32[]{:S(2)}, u32[]{:S(2)}) collective-permute-start(bf16[192,256]{1,0:T(8,128)(2,1)S(1)} %slice.9), channel_id=1, source_target_pairs={{0,6},{2,0},{4,2},{6,4},{1,7},{3,1},{5,3},{7,5},{8,14},{10,8},{12,... | collective-permute-start | bytes 294920 | tf_op jit(solution)/shard_map/ppermute | solution.py:404
  17.0 4.5 %project.1 = (bf16[384,2048]{1,0:T(8,128)(2,1)}, bf16[384,128]{1,0:T(8,128)(2,1)}, bf16[384,256]{1,0:T(8,128)(2,1)}) custom-call(s32[8]{0:T(128)} %pad_add_fusion.piece_ref, bf16[384,256]{1,0:T(8,128)(2,1)} %h0.1, bf16[384,256]{1,0:T(8,128)(2,1)} %copy-done.4, bf16[384,256]{1,0:T(8,128)(2,1)} %copy-done.5, bf16[192,256]{1,0:T(8,128)(2,1)} %copy-done.20, ...), custom_call_target="tpu_custom_call" | custom-call | flops 1409286144 | bytes 1409286 | tf_op jit(solution)/shard_map/project/pallas_call | solution.py:30
  22.5 2.2 %collective-permute-start.9 = (bf16[384,256]{1,0:T(8,128)(2,1)}, bf16[384,256]{1,0:T(8,128)(2,1)S(1)}, u32[]{:S(2)}, u32[]{:S(2)}) collective-permute-start(bf16[384,256]{1,0:T(8,128)(2,1)} %get-tuple-element.46.refs_5_), channel_id=1, source_target_pairs={{0,32},{32,64},{64,96},{96,128},{128,160},{160,192},{192,224},{224... | collective-permute-start | bytes 589832 | tf_op jit(solution)/shard_map/ppermute | solution.py:427
  24.8 7.4 %chunks.1 = (f32[12,64,128]{2,1,0:T(8,128)}, f32[12,64,128]{2,1,0:T(8,128)}, f32[12,64,128]{2,1,0:T(8,128)}, f32[6,64,128]{2,1,0:T(8,128)}, f32[6,64,128]{2,1,0:...) custom-call(bf16[384,2048]{1,0:T(8,128)(2,1)} %get-tuple-element.47.normed, bf16[2048,128]{1,0:T(8,128)(2,1)} %wr.1, ...), custom_call_target="tpu_custom_call" | custom-call | flops 6000000000 | bytes 6000000 | tf_op jit(solution)/shard_map/chunks/pallas_call | solution.py:30
  34.2 9.3 %recurrent.1 = (f32[384,128]{1,0:T(8,128)}, f32[384,128]{1,0:T(8,128)}, bf16[512,128]{1,0:T(8,128)(2,1)}) custom-call(f32[12,64,128]{2,1,0:T(8,128)} %get-tuple-element.58.lower_ref, f32[12,64,128]{2,1,0:T(8,128)} %get-tuple-element.59.reading_ref, f32[12,64,128]{2,1,0:T(8,128)} %get-tuple-element.60.rhs_ref, f32[6,64,128]{2,1,0:T(8,128)} %get-tuple-element.61.turned_ref, ...), custom_call_target="tpu_custom_call" | custom-call | flops 6000000000 | bytes 6000000 | tf_op jit(solution)/shard_map/recurrent/pallas_call | solution.py:30
  43.6 2.4 %collective-permute-start.13 = (bf16[384,256]{1,0:T(8,128)(2,1)S(1)}, bf16[384,256]{1,0:T(8,128)(2,1)S(1)}, u32[]{:S(2)}, u32[]{:S(2)}) collective-permute-start(bf16[384,256]{1,0:T(8,128)(2,1)S(1)} %collective-permute-done.11.refs_8_), channel_id=1, source_target_pairs={{0,32},{32,64},{64,96},{96,128},{128,160},{160,192},{192,224},{224... | collective-permute-start | bytes 589832 | tf_op jit(solution)/shard_map/ppermute | solution.py:462
  46.0 1.5 %collective-permute-start.15 = (bf16[512,128]{1,0:T(8,128)(2,1)}, bf16[512,128]{1,0:T(8,128)(2,1)S(1)}, u32[]{:S(2)}, u32[]{:S(2)}) collective-permute-start(bf16[512,128]{1,0:T(8,128)(2,1)} %get-tuple-element.71.m0.refs_1_), channel_id=1, source_target_pairs={{0,8},{8,16},{16,24},{24,0},{1,9},{9,17},{17,25},{25,1},{2,10},{10... | collective-permute-start | bytes 393224 | tf_op jit(solution)/shard_map/ppermute | solution.py:458
  47.4 1.7 %collective-permute-start.16 = (bf16[512,128]{1,0:T(8,128)(2,1)}, bf16[512,128]{1,0:T(8,128)(2,1)S(1)}, u32[]{:S(2)}, u32[]{:S(2)}) collective-permute-start(bf16[512,128]{1,0:T(8,128)(2,1)} %get-tuple-element.71.m0.refs_1_), channel_id=1, source_target_pairs={{0,24},{8,0},{16,8},{24,16},{1,25},{9,1},{17,9},{25,17},{2,26},{10... | collective-permute-start | bytes 393224 | tf_op jit(solution)/shard_map/ppermute | solution.py:459
  49.2 1.8 %collective-permute-start.17 = (bf16[512,128]{1,0:T(8,128)(2,1)}, bf16[512,128]{1,0:T(8,128)(2,1)S(1)}, u32[]{:S(2)}, u32[]{:S(2)}) collective-permute-start(bf16[512,128]{1,0:T(8,128)(2,1)} %get-tuple-element.71.m0.refs_1_), channel_id=1, source_target_pairs={{0,16},{8,24},{16,0},{24,8},{1,17},{9,25},{17,1},{25,9},{2,18},{10... | collective-permute-start | bytes 393224 | tf_op jit(solution)/shard_map/ppermute | solution.py:460
  51.7 1.7 %collective-permute-done.15.m1.refs_2_ = bf16[512,128]{1,0:T(8,128)(2,1)S(1)} collective-permute-done((bf16[512,128]{1,0:T(8,128)(2,1)}, bf16[512,128]{1,0:T(8,128)(2,1)S(1)}, u32[]{:S(2)}, u32[]{:S(2)}) %collective-permute-start.15) | collective-permute-done | bytes 131104 | tf_op jit(solution)/shard_map/ppermute | solution.py:458
  53.4 2.4 %collective-permute-done.17.m3.refs_4_ = bf16[512,128]{1,0:T(8,128)(2,1)S(1)} collective-permute-done((bf16[512,128]{1,0:T(8,128)(2,1)}, bf16[512,128]{1,0:T(8,128)(2,1)S(1)}, u32[]{:S(2)}, u32[]{:S(2)}) %collective-permute-start.17) | collective-permute-done | bytes 131104 | tf_op jit(solution)/shard_map/ppermute | solution.py:460
  56.5 2.4 %along_x.1 = (f32[128,128]{1,0:T(8,128)}, bf16[8,128,128]{2,1,0:T(8,128)(2,1)}) custom-call(s32[14]{0:T(128)} %stack.68.place_ref.refs_0_, bf16[512,128]{1,0:T(8,128)(2,1)} %get-tuple-element.71.m0.refs_1_, bf16[512,128]{1,0:T(8,128)(2,1)} %copy-done.1, bf16[512,128]{1,0:T(8,128)(2,1)} %copy-done.2, bf16[512,128]{1,0:T(8,128)(2,1)} %copy-done.3), custom_call_target="tpu_custom_call" | custom-call | flops 100000000 | bytes 100000 | tf_op jit(solution)/shard_map/along_x/pallas_call | solution.py:30
  58.9 7.0 %all-to-all-start = ((bf16[8,128,128]{2,1,0:T(8,128)(2,1)}), bf16[8,128,128]{2,1,0:T(8,128)(2,1)S(1)}, u32[]{:S(2)}, u32[]{:S(2)}) async-start(bf16[8,128,128]{2,1,0:T(8,128)(2,1)} %get-tuple-element.85), calls=%async_computation | async-start | bytes 524288 | tf_op jit(solution)/shard_map/all_to_all | solution.py:470
  66.0 14.5 %attention5.1 = (f32[8,8,384]{2,1,0:T(8,128)}, f32[8,144,384]{2,1,0:T(8,128)}) custom-call(s32[14]{0:T(128)} %stack.68.place_ref.refs_0_, bf16[512,128]{1,0:T(8,128)(2,1)} %get-tuple-element.71.m0.refs_1_, bf16[512,128]{1,0:T(8,128)(2,1)} %copy-done.1, bf16[512,128]{1,0:T(8,128)(2,1)} %copy-done.2, bf16[512,128]{1,0:T(8,128)(2,1)} %copy-done.3, ...), custom_call_target="tpu_custom_call" | custom-call | flops 10000000000 | bytes 10000000 | tf_op jit(solution)/shard_map/attention5/pallas_call | solution.py:30
  81.2 10.9 %attention3.1 = (bf16[2,144,384]{2,1,0:T(8,128)(2,1)}, bf16[2,144,384]{2,1,0:T(8,128)(2,1)}, bf16[2,144,384]{2,1,0:T(8,128)(2,1)}, bf16[2,144,384]{2,1,0:T(8,128)(2,1)}) custom-call(s32[14]{0:T(128)} %stack.68.place_ref.refs_0_, bf16[512,128]{1,0:T(8,128)(2,1)} %get-tuple-element.71.m0.refs_1_, bf16[512,128]{1,0:T(8,128)(2,1)} %copy-done.1, ...), custom_call_target="tpu_custom_call" | custom-call | flops 6000000000 | bytes 6000000 | tf_op jit(solution)/shard_map/attention3/pallas_call | solution.py:30
  96.3 2.5 %along_z.1.state_ref = f32[128,128]{1,0:T(8,128)} custom-call(s32[14]{0:T(128)} %stack.68.place_ref.refs_0_, bf16[8,128,128]{2,1,0:T(8,128)(2,1)} %copy-done, f32[128,128]{1,0:T(8,128)} %get-tuple-element.86.before_ref), custom_call_target="tpu_custom_call" | custom-call | flops 100000000 | bytes 100000 | tf_op jit(solution)/shard_map/along_z/pallas_call | solution.py:30
  99.6 3.9 %collective-permute-done.20.p2 = bf16[2,144,384]{2,1,0:T(8,128)(2,1)S(1)} collective-permute-done((bf16[2,144,384]{2,1,0:T(8,128)(2,1)}, bf16[2,144,384]{2,1,0:T(8,128)(2,1)S(1)}, u32[]{:S(2)}, u32[]{:S(2)}) %collective-permute-start.20) | collective-permute-done | bytes 221216 | tf_op jit(solution)/shard_map/ppermute | solution.py:498
  104.2 4.4 %finish.1 = (bf16[4,48,2048]{2,1,0:T(8,128)(2,1)}, bf16[4,48,2048]{2,1,0:T(8,128)(2,1)}, f32[2,384]{1,0:T(2,128)}) custom-call(s32[1]{0:T(128)} %bitcast.place_ref, f32[1]{0:T(128)S(6)} %copy.19.lambda_ref, bf16[2,144,384]{2,1,0:T(8,128)(2,1)} %get-tuple-element.79.p0, bf16[2,144,384]{2,1,0:T(8,128)(2,1)} %copy-done.7, bf16[2,144,384]{2,1,0:T(8,128)(2,1)} %copy-done.8, ...), custom_call_target="tpu_custom_call" | custom-call | flops 1000000000 | bytes 1000000 | tf_op jit(solution)/shard_map/finish/pallas_call | solution.py:30
  108.6 2.5 %collective-permute-done.22 = bf16[4,48,2048]{2,1,0:T(8,128)(2,1)S(1)} collective-permute-done((bf16[4,48,2048]{2,1,0:T(8,128)(2,1)}, bf16[4,48,2048]{2,1,0:T(8,128)(2,1)S(1)}, u32[]{:S(2)}, u32[]{:S(2)}) %collective-permute-start.22) | collective-permute-done | bytes 786464 | tf_op jit(solution)/shard_map/ppermute | solution.py:513
  111.1 1.4 %add_convert_fusion = bf16[4,48,2048]{2,1,0:T(8,128)(2,1)S(1)} fusion(bf16[4,48,2048]{2,1,0:T(8,128)(2,1)S(1)} %collective-permute-done.22, bf16[4,48,2048]{2,1,0:T(8,128)(2,1)} %get-tuple-element.87), kind=kLoop, calls=%fused_computation.1 | loop fusion | flops 1572864 | bytes 2359296 | tf_op jit(solution)/shard_map/convert_element_type | solution.py:514
  112.5 16.2 %all_to_all.10 = bf16[4,48,2048]{2,1,0:T(8,128)(2,1)S(1)} all-to-all(bf16[4,48,2048]{2,1,0:T(8,128)(2,1)S(1)} %add_convert_fusion), channel_id=1, replica_groups=mesh['z'=8,'x'=4,'y'=4,'c'=2] {'y'}, dimensions={0} | all-to-all | bytes 1572864 | tf_op jit(solution)/shard_map/all_to_all | solution.py:515
  (93 shorter events, 16.5 us)
Async XLA Ops:
  0.6 8.2 %collective-permute-start = (bf16[384,256]{1,0:T(8,128)(2,1)}, bf16[384,256]{1,0:T(8,128)(2,1)S(1)}, u32[]{:S(2)}, u32[]{:S(2)}) collective-permute-start(bf16[384,256]{1,0:T(8,128)(2,1)} %h0.1), channel_id=1, source_target_pairs={{0,2},{2,4},{4,6},{6,0},{1,3},{3,5},{5,7},{7,1},{8,10},{10,12},{12... | collective-permute-start | bytes 589832 | tf_op jit(solution)/shard_map/ppermute | solution.py:401
  2.3 6.9 %collective-permute-start.1 = (bf16[384,256]{1,0:T(8,128)(2,1)}, bf16[384,256]{1,0:T(8,128)(2,1)S(1)}, u32[]{:S(2)}, u32[]{:S(2)}) collective-permute-start(bf16[384,256]{1,0:T(8,128)(2,1)} %h0.1), channel_id=1, source_target_pairs={{0,6},{2,0},{4,2},{6,4},{1,7},{3,1},{5,3},{7,5},{8,14},{10,8},{12,... | collective-permute-start | bytes 589832 | tf_op jit(solution)/shard_map/ppermute | solution.py:402
  3.9 11.9 %collective-permute-start.4 = (bf16[384,256]{1,0:T(8,128)(2,1)}, bf16[384,256]{1,0:T(8,128)(2,1)S(1)}, u32[]{:S(2)}, u32[]{:S(2)}) collective-permute-start(bf16[384,256]{1,0:T(8,128)(2,1)} %h0.1), channel_id=1, source_target_pairs={{0,1},{1,0},{2,3},{3,2},{4,5},{5,4},{6,7},{7,6},{8,9},{9,8},{10,11... | collective-permute-start | bytes 589832 | tf_op jit(solution)/shard_map/ppermute | solution.py:406
  8.8 5.9 %collective-permute-start.2 = (bf16[192,256]{1,0:T(8,128)(2,1)S(1)}, bf16[192,256]{1,0:T(8,128)(2,1)S(1)}, u32[]{:S(2)}, u32[]{:S(2)}) collective-permute-start(bf16[192,256]{1,0:T(8,128)(2,1)S(1)} %slice.8), channel_id=1, source_target_pairs={{0,2},{2,4},{4,6},{6,0},{1,3},{3,5},{5,7},{7,1},{8,10},{10,12},{12... | collective-permute-start | bytes 294920 | tf_op jit(solution)/shard_map/ppermute | solution.py:403
  9.2 5.5 %collective-permute-start.3 = (bf16[192,256]{1,0:T(8,128)(2,1)S(1)}, bf16[192,256]{1,0:T(8,128)(2,1)S(1)}, u32[]{:S(2)}, u32[]{:S(2)}) collective-permute-start(bf16[192,256]{1,0:T(8,128)(2,1)S(1)} %slice.9), channel_id=1, source_target_pairs={{0,6},{2,0},{4,2},{6,4},{1,7},{3,1},{5,3},{7,5},{8,14},{10,8},{12,... | collective-permute-start | bytes 294920 | tf_op jit(solution)/shard_map/ppermute | solution.py:404
  12.3 4.0 %collective-permute-start.5 = (bf16[384,256]{1,0:T(8,128)(2,1)S(1)}, bf16[384,256]{1,0:T(8,128)(2,1)S(1)}, u32[]{:S(2)}, u32[]{:S(2)}) collective-permute-start(bf16[384,256]{1,0:T(8,128)(2,1)S(1)} %collective-permute-done.h1), channel_id=1, source_target_pairs={{0,1},{1,0},{2,3},{3,2},{4,5},{5,4},{6,7},{7,6},{8,9},{9,8},{10,11... | collective-permute-start | bytes 589832 | tf_op jit(solution)/shard_map/ppermute | solution.py:406
  12.3 4.0 %collective-permute-start.6 = (bf16[384,256]{1,0:T(8,128)(2,1)S(1)}, bf16[384,256]{1,0:T(8,128)(2,1)S(1)}, u32[]{:S(2)}, u32[]{:S(2)}) collective-permute-start(bf16[384,256]{1,0:T(8,128)(2,1)S(1)} %collective-permute-done.1.h2), channel_id=1, source_target_pairs={{0,1},{1,0},{2,3},{3,2},{4,5},{5,4},{6,7},{7,6},{8,9},{9,8},{10,11... | collective-permute-start | bytes 589832 | tf_op jit(solution)/shard_map/ppermute | solution.py:406
  14.8 1.3 %collective-permute-start.7 = (bf16[192,256]{1,0:T(8,128)(2,1)S(1)}, bf16[192,256]{1,0:T(8,128)(2,1)S(1)}, u32[]{:S(2)}, u32[]{:S(2)}) collective-permute-start(bf16[192,256]{1,0:T(8,128)(2,1)S(1)} %collective-permute-done.2.h3), channel_id=1, source_target_pairs={{0,1},{1,0},{2,3},{3,2},{4,5},{5,4},{6,7},{7,6},{8,9},{9,8},{10,11... | collective-permute-start | bytes 294920 | tf_op jit(solution)/shard_map/ppermute | solution.py:406
  14.8 1.4 %collective-permute-start.8 = (bf16[192,256]{1,0:T(8,128)(2,1)S(1)}, bf16[192,256]{1,0:T(8,128)(2,1)S(1)}, u32[]{:S(2)}, u32[]{:S(2)}) collective-permute-start(bf16[192,256]{1,0:T(8,128)(2,1)S(1)} %collective-permute-done.3.h4), channel_id=1, source_target_pairs={{0,1},{1,0},{2,3},{3,2},{4,5},{5,4},{6,7},{7,6},{8,9},{9,8},{10,11... | collective-permute-start | bytes 294920 | tf_op jit(solution)/shard_map/ppermute | solution.py:406
  21.5 10.6 %collective-permute-start.10 = (bf16[384,256]{1,0:T(8,128)(2,1)}, bf16[384,256]{1,0:T(8,128)(2,1)S(1)}, u32[]{:S(2)}, u32[]{:S(2)}) collective-permute-start(bf16[384,256]{1,0:T(8,128)(2,1)} %get-tuple-element.46.refs_5_), channel_id=1, source_target_pairs={{0,224},{32,0},{64,32},{96,64},{128,96},{160,128},{192,160},{224,1... | collective-permute-start | bytes 589832 | tf_op jit(solution)/shard_map/ppermute | solution.py:428
  22.5 9.6 %collective-permute-start.9 = (bf16[384,256]{1,0:T(8,128)(2,1)}, bf16[384,256]{1,0:T(8,128)(2,1)S(1)}, u32[]{:S(2)}, u32[]{:S(2)}) collective-permute-start(bf16[384,256]{1,0:T(8,128)(2,1)} %get-tuple-element.46.refs_5_), channel_id=1, source_target_pairs={{0,32},{32,64},{64,96},{96,128},{128,160},{160,192},{192,224},{224... | collective-permute-start | bytes 589832 | tf_op jit(solution)/shard_map/ppermute | solution.py:427
  32.1 11.4 %collective-permute-start.11 = (bf16[384,256]{1,0:T(8,128)(2,1)S(1)}, bf16[384,256]{1,0:T(8,128)(2,1)S(1)}, u32[]{:S(2)}, u32[]{:S(2)}) collective-permute-start(bf16[384,256]{1,0:T(8,128)(2,1)S(1)} %collective-permute-done.9.refs_6_), channel_id=1, source_target_pairs={{0,32},{32,64},{64,96},{96,128},{128,160},{160,192},{192,224},{224... | collective-permute-start | bytes 589832 | tf_op jit(solution)/shard_map/ppermute | solution.py:445
  33.1 10.5 %collective-permute-start.12 = (bf16[384,256]{1,0:T(8,128)(2,1)S(1)}, bf16[384,256]{1,0:T(8,128)(2,1)S(1)}, u32[]{:S(2)}, u32[]{:S(2)}) collective-permute-start(bf16[384,256]{1,0:T(8,128)(2,1)S(1)} %collective-permute-done.10.refs_7_), channel_id=1, source_target_pairs={{0,224},{32,0},{64,32},{96,64},{128,96},{160,128},{192,160},{224,1... | collective-permute-start | bytes 589832 | tf_op jit(solution)/shard_map/ppermute | solution.py:446
  43.6 15.3 %collective-permute-start.13 = (bf16[384,256]{1,0:T(8,128)(2,1)S(1)}, bf16[384,256]{1,0:T(8,128)(2,1)S(1)}, u32[]{:S(2)}, u32[]{:S(2)}) collective-permute-start(bf16[384,256]{1,0:T(8,128)(2,1)S(1)} %collective-permute-done.11.refs_8_), channel_id=1, source_target_pairs={{0,32},{32,64},{64,96},{96,128},{128,160},{160,192},{192,224},{224... | collective-permute-start | bytes 589832 | tf_op jit(solution)/shard_map/ppermute | solution.py:462
  45.9 13.0 %collective-permute-start.14 = (bf16[384,256]{1,0:T(8,128)(2,1)S(1)}, bf16[384,256]{1,0:T(8,128)(2,1)S(1)}, u32[]{:S(2)}, u32[]{:S(2)}) collective-permute-start(bf16[384,256]{1,0:T(8,128)(2,1)S(1)} %collective-permute-done.12.refs_9_), channel_id=1, source_target_pairs={{0,224},{32,0},{64,32},{96,64},{128,96},{160,128},{192,160},{224,1... | collective-permute-start | bytes 589832 | tf_op jit(solution)/shard_map/ppermute | solution.py:463
  46.0 7.5 %collective-permute-start.15 = (bf16[512,128]{1,0:T(8,128)(2,1)}, bf16[512,128]{1,0:T(8,128)(2,1)S(1)}, u32[]{:S(2)}, u32[]{:S(2)}) collective-permute-start(bf16[512,128]{1,0:T(8,128)(2,1)} %get-tuple-element.71.m0.refs_1_), channel_id=1, source_target_pairs={{0,8},{8,16},{16,24},{24,0},{1,9},{9,17},{17,25},{25,1},{2,10},{10... | collective-permute-start | bytes 393224 | tf_op jit(solution)/shard_map/ppermute | solution.py:458
  47.4 6.0 %collective-permute-start.16 = (bf16[512,128]{1,0:T(8,128)(2,1)}, bf16[512,128]{1,0:T(8,128)(2,1)S(1)}, u32[]{:S(2)}, u32[]{:S(2)}) collective-permute-start(bf16[512,128]{1,0:T(8,128)(2,1)} %get-tuple-element.71.m0.refs_1_), channel_id=1, source_target_pairs={{0,24},{8,0},{16,8},{24,16},{1,25},{9,1},{17,9},{25,17},{2,26},{10... | collective-permute-start | bytes 393224 | tf_op jit(solution)/shard_map/ppermute | solution.py:459
  49.2 6.7 %collective-permute-start.17 = (bf16[512,128]{1,0:T(8,128)(2,1)}, bf16[512,128]{1,0:T(8,128)(2,1)S(1)}, u32[]{:S(2)}, u32[]{:S(2)}) collective-permute-start(bf16[512,128]{1,0:T(8,128)(2,1)} %get-tuple-element.71.m0.refs_1_), channel_id=1, source_target_pairs={{0,16},{8,24},{16,0},{24,8},{1,17},{9,25},{17,1},{25,9},{2,18},{10... | collective-permute-start | bytes 393224 | tf_op jit(solution)/shard_map/ppermute | solution.py:460
  58.9 36.7 %all-to-all-start = ((bf16[8,128,128]{2,1,0:T(8,128)(2,1)}), bf16[8,128,128]{2,1,0:T(8,128)(2,1)S(1)}, u32[]{:S(2)}, u32[]{:S(2)}) async-start(bf16[8,128,128]{2,1,0:T(8,128)(2,1)} %get-tuple-element.85), calls=%async_computation | async-start | bytes 524288 | tf_op jit(solution)/shard_map/all_to_all | solution.py:470
  66.0 14.5 %collective-permute-start.18 = (bf16[384,256]{1,0:T(8,128)(2,1)S(1)}, bf16[384,256]{1,0:T(8,128)(2,1)S(1)}, u32[]{:S(2)}, u32[]{:S(2)}) collective-permute-start(bf16[384,256]{1,0:T(8,128)(2,1)S(1)} %collective-permute-done.13.refs_5_), channel_id=1, source_target_pairs={{0,32},{32,64},{64,96},{96,128},{128,160},{160,192},{192,224},{224... | collective-permute-start | bytes 589832 | tf_op jit(solution)/shard_map/ppermute | solution.py:471
  92.2 7.4 %collective-permute-start.19 = (bf16[2,144,384]{2,1,0:T(8,128)(2,1)}, bf16[2,144,384]{2,1,0:T(8,128)(2,1)S(1)}, u32[]{:S(2)}, u32[]{:S(2)}) collective-permute-start(bf16[2,144,384]{2,1,0:T(8,128)(2,1)} %get-tuple-element.80), channel_id=1, source_target_pairs={{0,24},{8,0},{16,8},{24,16},{1,25},{9,1},{17,9},{25,17},{2,26},{10... | collective-permute-start | bytes 663560 | tf_op jit(solution)/shard_map/ppermute | solution.py:497
  93.4 10.1 %collective-permute-start.20 = (bf16[2,144,384]{2,1,0:T(8,128)(2,1)}, bf16[2,144,384]{2,1,0:T(8,128)(2,1)S(1)}, u32[]{:S(2)}, u32[]{:S(2)}) collective-permute-start(bf16[2,144,384]{2,1,0:T(8,128)(2,1)} %get-tuple-element.81), channel_id=1, source_target_pairs={{0,8},{8,16},{16,24},{24,0},{1,9},{9,17},{17,25},{25,1},{2,10},{10... | collective-permute-start | bytes 663560 | tf_op jit(solution)/shard_map/ppermute | solution.py:498
  94.2 9.3 %collective-permute-start.21 = (bf16[2,144,384]{2,1,0:T(8,128)(2,1)}, bf16[2,144,384]{2,1,0:T(8,128)(2,1)S(1)}, u32[]{:S(2)}, u32[]{:S(2)}) collective-permute-start(bf16[2,144,384]{2,1,0:T(8,128)(2,1)} %get-tuple-element.82), channel_id=1, source_target_pairs={{0,16},{8,24},{16,0},{24,8},{1,17},{9,25},{17,1},{25,9},{2,18},{10... | collective-permute-start | bytes 663560 | tf_op jit(solution)/shard_map/ppermute | solution.py:499
  108.6 2.5 %collective-permute-start.22 = (bf16[4,48,2048]{2,1,0:T(8,128)(2,1)}, bf16[4,48,2048]{2,1,0:T(8,128)(2,1)S(1)}, u32[]{:S(2)}, u32[]{:S(2)}) collective-permute-start(bf16[4,48,2048]{2,1,0:T(8,128)(2,1)} %get-tuple-element.88), channel_id=1, source_target_pairs={{0,1},{1,0},{2,3},{3,2},{4,5},{5,4},{6,7},{7,6},{8,9},{9,8},{10,11... | collective-permute-start | bytes 2359304 | tf_op jit(solution)/shard_map/ppermute | solution.py:513
  (24 other events, 160.6 us)
where the time goes:
time: 130 us
  Pallas kernels  55.8 us (43%)
  starting transfers between devices  30.3 us (23%)
  waiting for transfers between devices  17.2 us (13%)
  blocking collectives  16.2 us (12%)
  local copies, waits for them, and re-layouts  5.59 us (4%)
  other arithmetic  3.11 us (2%)
  between operations  1.53 us (1%)
    pallas_call x8, Pallas kernels, call(): pl.pallas_call(kernel, out_shape=outs, in_specs=[pl.BlockSpec(memory_spac...  55.8 us
    all_to_all x1, blocking collectives, per_device(): parts = lax.all_to_all(summed, 'y', 0, 0, tiled=True)  16.2 us
    all_to_all x1, starting transfers between devices, per_device(): line_parts = lax.all_to_all(line, 'z', 0, 0, tiled=True)  7.04 us
    ppermute x1, waiting for transfers between devices, per_device(): up = permute(hidden_in, 'y', ring(4, 1))  4.81 us
    ppermute x1, waiting for transfers between devices, per_device(): permute(outs[2], 'x', ring(4, 1))  3.85 us
    unnamed x48, local copies, waits for them, and re-layouts  3.61 us
    ppermute x1, starting transfers between devices, per_device(): far_b = permute(down[half:], 'y', ring(4, -1))  3.01 us
  transfers between devices with their start and end apart: 24, of which 9 were waited for; matrix products, arithmetic and copies ran while one was open for 2% of the time, Pallas kernels for 36%

commit v1 on v0

--- a/solution.py
+++ b/solution.py
@@ -12,7 +12,6 @@
 HD = 64
 F32 = jnp.float32
 BF16 = jnp.bfloat16
-HIGHEST = lax.Precision.HIGHEST
 DECAY_SCALE = math.exp(-0.5)
 NORM_EPS = 1e-06
 GROUP_EPS = 0.00064
@@ -20,13 +19,15 @@
 KEY_EPS = 1e-06
 NEGATIVE = -1e30
 SPAN = 64
-VMEM_LIMIT = 60 * 1024 * 1024
+GROUP = 12
+MIB = 1024 * 1024
+GRANT = 28
 NT = (((1,), (1,)), ((), ()))
 TN = (((0,), (0,)), ((), ()))
 NN = (((1,), (0,)), ((), ()))
 
 
-def call(kernel, outs, scalars, arrays, scratch=(), flops=0, name=None):
+def call(kernel, outs, scalars, arrays, scratch=(), flops=0, grant=GRANT, name=None):
     return pl.pallas_call(
         kernel,
         out_shape=outs,
@@ -34,18 +35,31 @@
         + [pl.BlockSpec(memory_space=pltpu.VMEM)] * len(arrays),
         out_specs=jax.tree.map(lambda _: pl.BlockSpec(memory_space=pltpu.VMEM), outs),
         scratch_shapes=list(scratch),
-        compiler_params=pltpu.CompilerParams(vmem_limit_bytes=VMEM_LIMIT),
+        compiler_params=pltpu.CompilerParams(vmem_limit_bytes=grant * MIB),
         cost_estimate=pl.CostEstimate(flops=flops, bytes_accessed=flops // 1000, transcendentals=0),
         name=name,
     )(*scalars, *arrays)
 
 
-def dot(left, right, dims=NN, precision=None):
-    return lax.dot_general(left, right, dims, precision=precision, preferred_element_type=F32)
+def dot(left, right, dims=NN):
+    return lax.dot_general(left, right, dims, preferred_element_type=F32)
+
+
+def halves(value):
+    if value.dtype == BF16:
+        return (value,)
+    high = value.astype(BF16)
+    return (high, (value - high.astype(F32)).astype(BF16))
 
 
 def exact(left, right, dims=NN):
-    return dot(left, right, dims, HIGHEST)
+    left, right = halves(left), halves(right)
+    total = dot(left[0], right[0], dims)
+    for more in left[1:]:
+        total = total + dot(more, right[0], dims)
+    for more in right[1:]:
+        total = total + dot(left[0], more, dims)
+    return total
 
 
 def ring(size, shift):
@@ -62,13 +76,15 @@
 
 def project_kernel(
     piece_ref,
-    h0, h1, h2, h3, h4, g0, g1, g2, g3, g4,
-    gain_ref, wq, wkp, wvp,
+    own, h1, h2, h3, h4, g0, g1, g2, g3, g4, gain_ref, weights,
     normed, q_out, kv_out,
 ):
-    pieces = []
-    for own, up, down, far_a, far_b in ((h0, h1, h2, h3, h4), (g0, g1, g2, g3, g4)):
-        pieces += [own[...], up[...], down[...], jnp.concatenate([far_a[...], far_b[...]], axis=0)]
+    half = own.shape[0] // 2
+    pieces = [
+        h1[...], h2[...], jnp.concatenate([h3[...], h4[...]], axis=0),
+        g0[...], g1[...], g2[...], jnp.concatenate([g3[...], g4[...]], axis=0),
+        jnp.concatenate([own[half:], own[:half]], axis=0),
+    ]
     squares = None
     for piece in pieces:
         wide = piece.astype(F32)
@@ -81,8 +97,8 @@
         gain = gain_ref[pl.ds(place, 1), :]
         value = (piece.astype(F32) * scale * gain).astype(BF16)
         normed[:, pl.ds(pl.multiple_of(place * 256, 256), 256)] = value
-    kv_out[...] = dot(normed[...], jnp.concatenate([wkp[...], wvp[...]], axis=1)).astype(BF16)
-    q_out[...] = dot(normed[...], wq[...]).astype(BF16)
+    kv_out[...] = dot(normed[...], weights[:, :256]).astype(BF16)
+    q_out[...] = dot(normed[...], weights[:, 256:]).astype(BF16)
 
 
 def same_head():
@@ -94,7 +110,8 @@
 
 
 def compose(earlier, later, same):
-    return exact(earlier, jnp.where(same, later, 0.0)) + jnp.where(same, 0.0, later)
+    zero = jnp.zeros_like(later)
+    return exact(earlier, jnp.where(same, later, zero)) + jnp.where(same, zero, later).astype(F32)
 
 
 def chunk_kernel(
@@ -111,13 +128,13 @@
     all_decay = -DECAY_SCALE * jax.nn.sigmoid(pre) + shift_ref[...]
     rows = normed.shape[0]
     count = rows // SPAN
-    ones_block = jnp.where(same_head(), 1.0, 0.0).astype(F32)
+    ones_block = jnp.where(same_head(), 1.0, 0.0).astype(BF16)
     first = lane_ids((SPAN, 128)) < HD
     t_ids = row_ids((SPAN, 128))
     s_ids = lane_ids((SPAN, 128)) % HD
     strict = s_ids < t_ids
     causal = s_ids <= t_ids
-    tri = jnp.where(row_ids((SPAN, SPAN)) >= lane_ids((SPAN, SPAN)), 1.0, 0.0).astype(F32)
+    tri = jnp.where(row_ids((SPAN, SPAN)) >= lane_ids((SPAN, SPAN)), 1.0, 0.0).astype(BF16)
     keep = (first, jnp.logical_not(first))
     zero = jnp.zeros((SPAN, 128), F32)
     for c in range(count):
@@ -153,7 +170,7 @@
             reading_out[2 * c + h] = jnp.where(causal, scores[128 * h + SPAN : 128 * h + 128], 0.0)
             side_values = jnp.where(keep[h], 0.0, turned)
             rhs_out[2 * c + h] = jnp.where(keep[h], start, 0.0) + exact(
-                lower, jnp.concatenate([zero, side_values], axis=0)
+                lower, jnp.concatenate([zero, side_values], axis=0).astype(BF16)
             )
 
 
@@ -168,7 +185,7 @@
     first = lane_ids((SPAN, 128)) < HD
     keep = (first, jnp.logical_not(first))
     solved = []
-    group = 4
+    group = GROUP
     for base in range(0, 2 * count, group):
         lowers = [lower_ref[base + n] for n in range(group)]
         state = [[rhs_ref[base + n, 8 * b : 8 * b + 8] for b in range(SPAN // 8)] for n in range(group)]
@@ -201,24 +218,26 @@
 def along_x_kernel(place_ref, m0, m1, m2, m3, before_out, total_out, parts):
     rows = m0.shape[0] - 128
     same = same_head()
-    identity = jnp.where(diagonal_mask(), 1.0, 0.0).astype(F32)
+    identity = jnp.where(diagonal_mask(), 1.0, 0.0).astype(BF16)
     mine = place_ref[1]
     for n, ref in enumerate((m0, m1, m2, m3)):
-        parts[place_ref[10 + n]] = ref[rows:, :].astype(F32)
-    total = compose(
-        compose(parts[0], parts[1], same), compose(parts[2], parts[3], same), same
-    ).astype(BF16)
+        parts[place_ref[10 + n]] = ref[rows:, :]
+    total = parts[0]
+    for j in range(1, 4):
+        total = compose(total, parts[j], same)
     for n in range(8):
-        total_out[n] = total
-    kept = [jnp.where(j < mine, parts[j], identity) for j in range(3)]
-    before_out[...] = compose(compose(kept[0], kept[1], same), kept[2], same)
+        total_out[n] = total.astype(BF16)
+    before = jnp.where(mine > 0, parts[0], identity)
+    for j in range(1, 3):
+        before = compose(before, jnp.where(j < mine, parts[j], identity), same)
+    before_out[...] = before
 
 
 def along_z_kernel(place_ref, parts_ref, before_ref, state_out):
     same = same_head()
-    identity = jnp.where(diagonal_mask(), 1.0, 0.0).astype(F32)
+    identity = jnp.where(diagonal_mask(), 1.0, 0.0).astype(BF16)
     mine = place_ref[0]
-    level = [jnp.where(j < mine, parts_ref[j].astype(F32), identity) for j in range(7)]
+    level = [jnp.where(j < mine, parts_ref[j], identity) for j in range(7)]
     level.append(before_ref[...])
     while len(level) > 1:
         level = [compose(level[i], level[i + 1], same) for i in range(0, len(level), 2)]
@@ -228,109 +247,105 @@
 TALL = 144
 
 
-def attention_kernel(blocks, is_first, is_last, *refs):
-    place_ref, refs = refs[0], refs[1:]
-    messages, refs = refs[:4], refs[4:]
-    kvs, refs = refs[: len(blocks)], refs[len(blocks) :]
-    if not is_first:
-        (max_in, sum_in), refs = refs[:2], refs[2:]
-    count = 4 if is_last else 2
-    outs, refs = refs[:count], refs[count:]
-    row_max, weighted, queries, keys, turned, scores, weights, rescales, units = refs
-    rows = messages[0].shape[0] - 128
+def attention_kernel(
+    place_ref, m0, m1, m2, m3, *refs
+):
+    kvs, outs = refs[:8], refs[8:12]
+    row_max, weighted, queries, keys, turned, scores, weights, rescales, units = refs[12:]
+    rows = m0.shape[0] - 128
+    wide = 2 * rows
     my_z, my_x = place_ref[0], place_ref[1]
     first = lane_ids((rows, 128)) < HD
-    for n, ref in enumerate(messages):
+    for n, ref in enumerate((m0, m1, m2, m3)):
         scaled = (ref[:rows, :].astype(F32) * (HD**-0.5)).astype(BF16)
-        queries[2 * n] = jnp.where(first, scaled, 0).astype(BF16)
-        queries[2 * n + 1] = jnp.where(first, 0, scaled).astype(BF16)
+        at = slice((n % 2) * rows, (n % 2 + 1) * rows)
+        queries[2 * (n // 2), at, :] = jnp.where(first, scaled, 0).astype(BF16)
+        queries[2 * (n // 2) + 1, at, :] = jnp.where(first, 0, scaled).astype(BF16)
     ones = jnp.where(row_ids((TALL - 128, rows)) == 0, 1.0, 0.0).astype(BF16)
     for n, ref in enumerate(kvs):
         keys[n] = ref[:, :128]
         turned[n, :128, :] = jnp.transpose(ref[:, 128:])
         turned[n, 128:, :] = ones
-    if is_first:
-        row_max[...] = jnp.full_like(row_max, NEGATIVE)
-        weighted[...] = jnp.zeros_like(weighted)
-    else:
-        row_max[:8] = max_in[...]
-        weighted[:8] = sum_in[...]
-
-    def score(q, n, out):
+    row_max[...] = jnp.full_like(row_max, NEGATIVE)
+    weighted[...] = jnp.zeros_like(weighted)
+
+    def score(pair, n, out):
         for m in range(2):
-            out[m] = dot(keys[n], queries[2 * q + m], NT)
-
-    def soften(slot, source, target, factors, diagonal=False):
+            out[m] = dot(keys[n], queries[2 * pair + m], NT)
+
+    def soften(slot, source, target, factors, limit=None):
         for m in range(2):
             i = 2 * slot + m
             got = source[m]
-            if diagonal:
-                allowed = row_ids((rows, rows)) <= lane_ids((rows, rows))
-                got = jnp.where(allowed, got, NEGATIVE)
+            if limit is not None:
+                got = jnp.where(row_ids((rows, wide)) <= limit, got, NEGATIVE)
             old = row_max[i, :1, :]
             new = jnp.maximum(old, jnp.max(got, axis=0, keepdims=True))
             target[m] = jnp.exp(got - new).astype(BF16)
-            factors[m] = jnp.broadcast_to(jnp.exp(old - new), (8, rows))
-            row_max[i] = jnp.broadcast_to(new, (8, rows))
+            factors[m] = jnp.broadcast_to(jnp.exp(old - new), (8, wide))
+            row_max[i] = jnp.broadcast_to(new, (8, wide))
 
     def gather(slot, n, source, factors):
         for m in range(2):
             i = 2 * slot + m
             weighted[i] = weighted[i] * factors[m, :1, :] + dot(turned[n], source[m])
 
-    def put(at, q, n, slot):
-        units[0, at] = q
+    def put(at, pair, n, slot):
+        units[0, at] = pair
         units[1, at] = n
         units[2, at] = slot
 
-    put(0, 0, 0, 4)
+    put(0, 1, 0, 1)
     total = jnp.int32(1)
-    for n, number in enumerate(blocks):
-        for q in range(4):
-            put(total, q, n, q)
-            wanted = place_ref[10 + q] > my_x if number == 0 else place_ref[2 + number] < my_z
+    for n in range(1, 8):
+        wanted = place_ref[2 + n] < my_z
+        for pair in range(2):
+            put(total, pair, n, pair)
             total = total + wanted.astype(jnp.int32)
     for extra in range(4):
-        put(total + extra, 0, 0, 4)
-
-    if is_first:
-        score(0, 0, scores[0])
-        soften(0, scores[0], weights[0], rescales[0], True)
-        gather(0, 0, weights[0], rescales[0])
-
-    @pl.when(total > 1)
-    def _():
-        score(units[0, 1], units[1, 1], scores[1])
-
-        def step(at, now, other):
-            score(units[0, at + 1], units[1, at + 1], scores[other])
-            soften(units[2, at], scores[now], weights[now], rescales[now])
-            gather(units[2, at - 1], units[1, at - 1], weights[other], rescales[other])
-
-        def two(t, carry):
-            step(2 * t + 1, 1, 0)
-            step(2 * t + 2, 0, 1)
-            return carry
-
-        lax.fori_loop(0, (total + 1) // 2, two, 0)
-
-    if is_last:
-        for q, out in enumerate(outs):
-            for m in range(2):
-                i = 2 * q + m
-                row_sum = weighted[i, 128:129, :]
-                some = row_sum > 0.0
-                safe = jnp.where(some, row_sum, 1.0)
-                out[m, :128, :] = (weighted[i, :128, :] * (1.0 / safe)).astype(BF16)
-                logs = jnp.where(some, row_max[i, :1, :] + jnp.log(safe), NEGATIVE)
-                high = logs.astype(BF16).astype(F32)
-                middle = (logs - high).astype(BF16).astype(F32)
-                low = logs - high - middle
-                tail = [high, middle, low, jnp.zeros((TALL - 131, rows), F32)]
-                out[m, 128:, :] = jnp.concatenate(tail, axis=0).astype(BF16)
-    else:
-        outs[0][...] = row_max[:8]
-        outs[1][...] = weighted[:8]
+        put(total + extra, 0, 0, 2)
+
+    column = lane_ids((1, wide))
+    within = jnp.where(column < rows, column, column - rows)
+
+    def limit(pair):
+        x_of = jnp.where(column < rows, place_ref[10 + 2 * pair], place_ref[11 + 2 * pair])
+        return jnp.where(x_of > my_x, rows, jnp.where(x_of == my_x, within, -1))
+
+    score(0, 0, scores[0])
+    score(1, 0, scores[1])
+    soften(0, scores[0], weights[0], rescales[0], limit(0))
+    score(units[0, 1], units[1, 1], scores[0])
+    soften(1, scores[1], weights[1], rescales[1], limit(1))
+    gather(0, 0, weights[0], rescales[0])
+
+    def step(at, now, other):
+        score(units[0, at + 1], units[1, at + 1], scores[other])
+        soften(units[2, at], scores[now], weights[now], rescales[now])
+        gather(units[2, at - 1], units[1, at - 1], weights[other], rescales[other])
+
+    def two(t, carry):
+        step(2 * t + 1, 0, 1)
+        step(2 * t + 2, 1, 0)
+        return carry
+
+    lax.fori_loop(0, (total + 1) // 2, two, 0)
+
+    for n, out in enumerate(outs):
+        at = slice((n % 2) * rows, (n % 2 + 1) * rows)
+        for m in range(2):
+            i = 2 * (n // 2) + m
+            top = row_max[i, :1, at]
+            some = top > 0.5 * NEGATIVE
+            row_sum = jnp.where(some, weighted[i, 128:129, at], 1.0)
+            share = jnp.where(some, 1.0 / row_sum, 0.0)
+            out[m, :128, :] = (weighted[i, :128, at] * share).astype(BF16)
+            logs = jnp.where(some, top + jnp.log(row_sum), NEGATIVE)
+            high = logs.astype(BF16).astype(F32)
+            middle = (logs - high).astype(BF16).astype(F32)
+            low = logs - high - middle
+            tail = [high, middle, low, jnp.zeros((TALL - 131, rows), F32)]
+            out[m, 128:, :] = jnp.concatenate(tail, axis=0).astype(BF16)
 
 
 def finish_kernel(
@@ -402,24 +417,25 @@
     down = permute(hidden_in, "y", ring(4, -1))
     far_a = permute(up[:half], "y", ring(4, 1))
     far_b = permute(down[half:], "y", ring(4, -1))
-    mine = [hidden_in, up, down, far_a, far_b]
-    theirs = [permute(a, "c", ring(2, 1)) for a in mine]
-    ys = jnp.stack([y, (y + 3) % 4, (y + 1) % 4, (y + 2) % 4])
-    piece_at = jnp.concatenate([ys * 2 + core, ys * 2 + 1 - core]).astype(jnp.int32)
+    mine = [up, down, far_a, far_b]
+    theirs = [permute(a, "c", ring(2, 1)) for a in (hidden_in, *mine)]
+    ys = [(y + 3) % 4, (y + 1) % 4, (y + 2) % 4, y]
+    piece_at = jnp.stack(
+        [2 * a + core for a in ys[:3]] + [2 * a + 1 - core for a in (y, *ys[:3])] + [2 * y + core]
+    ).astype(jnp.int32)
     places = jnp.stack(
         [z, x, z]
         + [a for s in (1, 2, 3) for a in ((z + 8 - s) % 8, (z + s) % 8)]
         + [(z + 4) % 8, x, (x + 3) % 4, (x + 1) % 4, (x + 2) % 4]
     ).astype(jnp.int32)
 
+    turned_in = jnp.concatenate([hidden_in[half:], hidden_in[:half]], axis=0)
+    pair_weights = jnp.concatenate([key_pair, value_pair, query_pair], axis=2).reshape(2048, 384)
     normed, q, kv = call(
         project_kernel,
         (shaped((rows, 2048), BF16), shaped((rows, 128), BF16), shaped((rows, 256), BF16)),
         (piece_at,),
-        (
-            *mine, *theirs, in_gain.reshape(8, 256), query_pair.reshape(2048, 128),
-            key_pair.reshape(2048, 128), value_pair.reshape(2048, 128),
-        ),
+        (turned_in, *mine, *theirs, in_gain.reshape(8, 256), pair_weights),
         flops=2 * rows * 2048 * 896,
         name="project",
     )
@@ -453,45 +469,43 @@
         name="recurrent",
     )
     right2, left2, message = together((right, left, message))
+    right = permute(right2, "z", ring(8, 1))
+    left = permute(left2, "z", ring(8, -1))
     messages = [
         message,
         permute(message, "x", ring(4, 1)),
         permute(message, "x", ring(4, -1)),
         permute(message, "x", ring(4, 2)),
     ]
-    right = permute(right2, "z", ring(8, 1))
-    left = permute(left2, "z", ring(8, -1))
+    right3, left3, messages = together((right, left, messages))
+    right4 = permute(right3, "z", ring(8, 1))
     before, line = call(
         along_x_kernel,
         (shaped((128, 128), F32), shaped((8, 128, 128), BF16)),
-        (places,), messages, scratch=(pltpu.VMEM((4, 128, 128), F32),), flops=10**8, name="along_x",
-    )
-    right3, left3, line, messages = together((right, left, line, messages))
+        (places,), messages, scratch=(pltpu.VMEM((4, 128, 128), BF16),), flops=10**8, name="along_x",
+    )
     line_parts = lax.all_to_all(line, "z", 0, 0, tiled=True)
-    right4 = permute(right3, "z", ring(8, 1))
-
-    carry = (shaped((8, 8, rows), F32), shaped((8, TALL, rows), F32))
+
     payload = shaped((2, TALL, rows), BF16)
-
-    def attend(blocks, arrays, carried, last=False):
-        pair = lambda shape, kind: [pltpu.VMEM(shape, kind)] * 2
-        return call(
-            functools.partial(attention_kernel, blocks, not carried, last),
-            (payload,) * 4 if last else carry,
-            (places,),
-            (*messages, *arrays, *carried),
-            scratch=[
-                pltpu.VMEM((10, 8, rows), F32), pltpu.VMEM((10, TALL, rows), F32),
-                pltpu.VMEM((8, rows, 128), BF16), pltpu.VMEM((len(blocks), rows, 128), BF16),
-                pltpu.VMEM((len(blocks), TALL, rows), BF16), pair((2, rows, rows), F32),
-                pair((2, rows, rows), BF16), pair((2, 8, rows), F32), pltpu.SMEM((3, 32), jnp.int32),
-            ],
-            flops=2 * len(blocks) * 10**9,
-            name=f"attention{len(blocks)}",
-        )
-
-    carried = attend((0, 1, 2, 3, 4), (kv, right1, left1, right2, left2), ())
-    outs = attend((5, 6, 7), (right3, left3, right4), tuple(carried), last=True)
+    wide = 2 * rows
+
+    def pair(shape, kind):
+        return [pltpu.VMEM(shape, kind)] * 2
+
+    outs = call(
+        attention_kernel,
+        (payload,) * 4,
+        (places,),
+        (*messages, kv, right1, left1, right2, left2, right3, left3, right4),
+        scratch=[
+            pltpu.VMEM((6, 8, wide), F32), pltpu.VMEM((6, TALL, wide), F32),
+            pltpu.VMEM((4, wide, 128), BF16), pltpu.VMEM((8, rows, 128), BF16),
+            pltpu.VMEM((8, TALL, rows), BF16), pair((2, rows, wide), F32),
+            pair((2, rows, wide), BF16), pair((2, 8, wide), F32), pltpu.SMEM((3, 32), jnp.int32),
+        ],
+        flops=16 * 10**9,
+        name="attention",
+    )
     back = [
         outs[0],
         permute(outs[1], "x", ring(4, -1)),

time: 130 us -> 117 us (0.900)
  Pallas kernels: 55.8 us -> 33.1 us
  starting transfers between devices: 30.3 us -> 33.8 us
  local copies, waits for them, and re-layouts: 5.59 us -> 8.57 us
  waiting for transfers between devices: 17.2 us -> 19.8 us
    pallas_call x8 -> x7, Pallas kernels: 55.8 us -> 33.1 us  [call(): pl.pallas_call(kernel, out_shape=outs, in_specs=[pl.BlockSpec(memory_spac...]
    unnamed x48 -> x50, local copies, waits for them, and re-layouts: 3.61 us -> 8.36 us
    ppermute x1, starting transfers between devices: 0.02 us -> 3.31 us  [per_device(): right4 = permute(right3, 'z', ring(8, 1))]
    all_to_all x1, starting transfers between devices: 7.04 us -> 4.51 us  [per_device(): line_parts = lax.all_to_all(line, 'z', 0, 0, tiled=True)]
    ppermute x1, starting transfers between devices: 0.92 us -> 2.95 us  [per_device(): right = permute(right1, 'z', ring(8, 1))]
    reshape x0 -> x1, other arithmetic: none -> 1.56 us  [per_device(): jnp.concatenate([key_pair, value_pair, query_pair], axis=2)]
    ppermute x1, waiting for transfers between devices: 4.81 us -> 3.32 us  [per_device(): up = permute(hidden_in, 'y', ring(4, 1))]
  transfers between devices with their start and end apart: 24 -> 24, of which waited for: 9 -> 11; matrix products, arithmetic and copies ran while one was open for 2% -> 2% of each run, Pallas kernels for 36% -> 25%
where the time goes in v1:
time: 117 us; the launch traced here: 116 us
  starting transfers between devices  33.8 us (29%)
  Pallas kernels  33.1 us (28%)
  waiting for transfers between devices  19.8 us (17%)
  blocking collectives  16.6 us (14%)
  local copies, waits for them, and re-layouts  8.57 us (7%)
  other arithmetic  2.89 us (2%)
  between operations  1.66 us (1%)
    pallas_call x7, Pallas kernels, call(): pl.pallas_call(kernel, out_shape=outs, in_specs=[pl.BlockSpec(memory_spac...  33.1 us
    all_to_all x1, blocking collectives, per_device(): parts = lax.all_to_all(summed, 'y', 0, 0, tiled=True)  16.6 us
    unnamed x50, local copies, waits for them, and re-layouts  8.36 us
    ppermute x1, waiting for transfers between devices, per_device(): permute(outs[2], 'x', ring(4, 1))  5.03 us
    all_to_all x1, starting transfers between devices, per_device(): line_parts = lax.all_to_all(line, 'z', 0, 0, tiled=True)  4.51 us
    ppermute x1, waiting for transfers between devices, per_device(): up = permute(hidden_in, 'y', ring(4, 1))  3.32 us
    ppermute x1, starting transfers between devices, per_device(): right4 = permute(right3, 'z', ring(8, 1))  3.31 us
    ppermute x1, starting transfers between devices, per_device(): right = permute(right2, 'z', ring(8, 1))  3.08 us
  transfers between devices with their start and end apart: 24, of which 11 were waited for; matrix products, arithmetic and copies ran while one was open for 2% of the time, Pallas kernels for 25%

profile of v1, /device:TPU:224, one launch (start us, length us, event | category | flops | bytes accessed | tf_op | source)
XLA Modules:
  0.0 116.4 jit_solution(17434600130916983701)
XLA Ops:
  0.7 1.7 %collective-permute-start = (bf16[384,256]{1,0:T(8,128)(2,1)}, bf16[384,256]{1,0:T(8,128)(2,1)S(1)}, u32[]{:S(2)}, u32[]{:S(2)}) collective-permute-start(bf16[384,256]{1,0:T(8,128)(2,1)} %param.17), channel_id=1, source_target_pairs={{0,2},{2,4},{4,6},{6,0},{1,3},{3,5},{5,7},{7,1},{8,10},{10,12},{12... | collective-permute-start | bytes 589832 | tf_op jit(solution)/shard_map/ppermute | solution.py:416
  2.3 1.7 %collective-permute-start.1 = (bf16[384,256]{1,0:T(8,128)(2,1)}, bf16[384,256]{1,0:T(8,128)(2,1)S(1)}, u32[]{:S(2)}, u32[]{:S(2)}) collective-permute-start(bf16[384,256]{1,0:T(8,128)(2,1)} %param.17), channel_id=1, source_target_pairs={{0,6},{2,0},{4,2},{6,4},{1,7},{3,1},{5,3},{7,5},{8,14},{10,8},{12,... | collective-permute-start | bytes 589832 | tf_op jit(solution)/shard_map/ppermute | solution.py:417
  5.5 3.3 %collective-permute-done.h1 = bf16[384,256]{1,0:T(8,128)(2,1)S(1)} collective-permute-done((bf16[384,256]{1,0:T(8,128)(2,1)}, bf16[384,256]{1,0:T(8,128)(2,1)S(1)}, u32[]{:S(2)}, u32[]{:S(2)}) %collective-permute-start) | collective-permute-done | bytes 196640 | tf_op jit(solution)/shard_map/ppermute | solution.py:416
  9.3 3.0 %collective-permute-start.3 = (bf16[192,256]{1,0:T(8,128)(2,1)S(1)}, bf16[192,256]{1,0:T(8,128)(2,1)S(1)}, u32[]{:S(2)}, u32[]{:S(2)}) collective-permute-start(bf16[192,256]{1,0:T(8,128)(2,1)S(1)} %slice.17), channel_id=1, source_target_pairs={{0,6},{2,0},{4,2},{6,4},{1,7},{3,1},{5,3},{7,5},{8,14},{10,8},{12,... | collective-permute-start | bytes 294920 | tf_op jit(solution)/shard_map/ppermute | solution.py:419
  13.0 1.8 %collective-permute-done.2.h3 = bf16[192,256]{1,0:T(8,128)(2,1)S(1)} collective-permute-done((bf16[192,256]{1,0:T(8,128)(2,1)S(1)}, bf16[192,256]{1,0:T(8,128)(2,1)S(1)}, u32[]{:S(2)}, u32[]{:S(2)}) %collective-permute-start.2) | collective-permute-done | bytes 98336 | tf_op jit(solution)/shard_map/ppermute | solution.py:418
  16.2 2.3 %project.1 = (bf16[384,2048]{1,0:T(8,128)(2,1)S(1)}, bf16[384,128]{1,0:T(8,128)(2,1)S(1)}, bf16[384,256]{1,0:T(8,128)(2,1)S(1)}) custom-call(s32[8]{0:T(128)S(1)} %stack.89.piece_ref, bf16[384,256]{1,0:T(8,128)(2,1)S(1)} %pad_maximum_fusion.own, bf16[384,256]{1,0:T(8,128)(2,1)S(1)} %collective-permute-done.h1, ...), custom_call_target="tpu_custom_call" | custom-call | flops 1409286144 | bytes 1409286 | tf_op jit(solution)/shard_map/project/pallas_call | solution.py:31
  19.6 2.2 %collective-permute-start.9 = (bf16[384,256]{1,0:T(8,128)(2,1)S(1)}, bf16[384,256]{1,0:T(8,128)(2,1)S(1)}, u32[]{:S(2)}, u32[]{:S(2)}) collective-permute-start(bf16[384,256]{1,0:T(8,128)(2,1)S(1)} %get-tuple-element.43.refs_0_), channel_id=1, source_target_pairs={{0,32},{32,64},{64,96},{96,128},{128,160},{160,192},{192,224},{224... | collective-permute-start | bytes 589832 | tf_op jit(solution)/shard_map/ppermute | solution.py:443
  21.9 3.8 %chunks.1 = (f32[12,64,128]{2,1,0:T(8,128)S(1)}, f32[12,64,128]{2,1,0:T(8,128)S(1)}, f32[12,64,128]{2,1,0:T(8,128)S(1)}, f32[6,64,128]{2,1,0:T(8,128)S(1)}, f32[...) custom-call(bf16[384,2048]{1,0:T(8,128)(2,1)S(1)} %get-tuple-element.44.normed, ...), custom_call_target="tpu_custom_call" | custom-call | flops 6000000000 | bytes 6000000 | tf_op jit(solution)/shard_map/chunks/pallas_call | solution.py:31
  27.0 3.0 %collective-permute-start.11 = (bf16[384,256]{1,0:T(8,128)(2,1)S(1)}, bf16[384,256]{1,0:T(8,128)(2,1)S(1)}, u32[]{:S(2)}, u32[]{:S(2)}) collective-permute-start(bf16[384,256]{1,0:T(8,128)(2,1)S(1)} %collective-permute-done.9.refs_1_), channel_id=1, source_target_pairs={{0,32},{32,64},{64,96},{96,128},{128,160},{160,192},{192,224},{224... | collective-permute-start | bytes 589832 | tf_op jit(solution)/shard_map/ppermute | solution.py:461
  30.0 5.4 %recurrent.1 = (f32[384,128]{1,0:T(8,128)S(1)}, f32[384,128]{1,0:T(8,128)S(1)}, bf16[512,128]{1,0:T(8,128)(2,1)S(1)}) custom-call(f32[12,64,128]{2,1,0:T(8,128)S(1)} %get-tuple-element.55.lower_ref, f32[12,64,128]{2,1,0:T(8,128)S(1)} %get-tuple-element.56.reading_ref, f32[12,64,128]{2,1,0:T(8,128)S(1)} %get-tuple-element.57.rhs_ref, ...), custom_call_target="tpu_custom_call" | custom-call | flops 6000000000 | bytes 6000000 | tf_op jit(solution)/shard_map/recurrent/pallas_call | solution.py:31
  36.9 3.1 %collective-permute-start.13 = (bf16[384,256]{1,0:T(8,128)(2,1)S(1)}, bf16[384,256]{1,0:T(8,128)(2,1)S(1)}, u32[]{:S(2)}, u32[]{:S(2)}) collective-permute-start(bf16[384,256]{1,0:T(8,128)(2,1)S(1)} %collective-permute-done.11.refs_3_), channel_id=1, source_target_pairs={{0,32},{32,64},{64,96},{96,128},{128,160},{160,192},{192,224},{224... | collective-permute-start | bytes 589832 | tf_op jit(solution)/shard_map/ppermute | solution.py:472
  41.5 1.7 %collective-permute-start.16 = (bf16[512,128]{1,0:T(8,128)(2,1)S(1)}, bf16[512,128]{1,0:T(8,128)(2,1)S(1)}, u32[]{:S(2)}, u32[]{:S(2)}) collective-permute-start(bf16[512,128]{1,0:T(8,128)(2,1)S(1)} %get-tuple-element.67.m0), channel_id=1, source_target_pairs={{0,24},{8,0},{16,8},{24,16},{1,25},{9,1},{17,9},{25,17},{2,26},{10... | collective-permute-start | bytes 393224 | tf_op jit(solution)/shard_map/ppermute | solution.py:477
  43.2 1.8 %collective-permute-start.17 = (bf16[512,128]{1,0:T(8,128)(2,1)S(1)}, bf16[512,128]{1,0:T(8,128)(2,1)S(1)}, u32[]{:S(2)}, u32[]{:S(2)}) collective-permute-start(bf16[512,128]{1,0:T(8,128)(2,1)S(1)} %get-tuple-element.67.m0), channel_id=1, source_target_pairs={{0,16},{8,24},{16,0},{24,8},{1,17},{9,25},{17,1},{25,9},{2,18},{10... | collective-permute-start | bytes 393224 | tf_op jit(solution)/shard_map/ppermute | solution.py:478
  45.1 2.5 %collective-permute-done.15.m1 = bf16[512,128]{1,0:T(8,128)(2,1)S(1)} collective-permute-done((bf16[512,128]{1,0:T(8,128)(2,1)S(1)}, bf16[512,128]{1,0:T(8,128)(2,1)S(1)}, u32[]{:S(2)}, u32[]{:S(2)}) %collective-permute-start.15) | collective-permute-done | bytes 131104 | tf_op jit(solution)/shard_map/ppermute | solution.py:476
  47.6 2.1 %collective-permute-done.17.m3 = bf16[512,128]{1,0:T(8,128)(2,1)S(1)} collective-permute-done((bf16[512,128]{1,0:T(8,128)(2,1)S(1)}, bf16[512,128]{1,0:T(8,128)(2,1)S(1)}, u32[]{:S(2)}, u32[]{:S(2)}) %collective-permute-start.17) | collective-permute-done | bytes 131104 | tf_op jit(solution)/shard_map/ppermute | solution.py:478
  49.7 3.3 %collective-permute-start.18 = (bf16[384,256]{1,0:T(8,128)(2,1)S(1)}, bf16[384,256]{1,0:T(8,128)(2,1)S(1)}, u32[]{:S(2)}, u32[]{:S(2)}) collective-permute-start(bf16[384,256]{1,0:T(8,128)(2,1)S(1)} %collective-permute-done.13.refs_5_), channel_id=1, source_target_pairs={{0,32},{32,64},{64,96},{96,128},{128,160},{160,192},{192,224},{224... | collective-permute-start | bytes 589832 | tf_op jit(solution)/shard_map/ppermute | solution.py:481
  53.1 1.7 %along_x.1 = (f32[128,128]{1,0:T(8,128)S(1)}, bf16[8,128,128]{2,1,0:T(8,128)(2,1)}) custom-call(s32[14]{0:T(128)S(1)} %stack.80.place_ref, bf16[512,128]{1,0:T(8,128)(2,1)S(1)} %get-tuple-element.67.m0, bf16[512,128]{1,0:T(8,128)(2,1)S(1)} %collective-permute-done.15.m1, bf16[512,128]{1,0:T(8,128)(2,1)S(1)} %collective-permute-done.16.m2, ...), custom_call_target="tpu_custom_call" | custom-call | flops 100000000 | bytes 100000 | tf_op jit(solution)/shard_map/along_x/pallas_call | solution.py:31
  54.8 4.5 %all-to-all-start = ((bf16[8,128,128]{2,1,0:T(8,128)(2,1)}), bf16[8,128,128]{2,1,0:T(8,128)(2,1)S(1)}, u32[]{:S(2)}, u32[]{:S(2)}) async-start(bf16[8,128,128]{2,1,0:T(8,128)(2,1)} %get-tuple-element.79), calls=%async_computation | async-start | bytes 524288 | tf_op jit(solution)/shard_map/all_to_all | solution.py:487
  62.8 16.8 %attention.1 = (bf16[2,144,384]{2,1,0:T(8,128)(2,1)S(1)}, bf16[2,144,384]{2,1,0:T(8,128)(2,1)S(1)}, bf16[2,144,384]{2,1,0:T(8,128)(2,1)S(1)}, bf16[2,144,384]{2,1,0:T(8,128)(2,1)S(1)}) custom-call(s32[14]{0:T(128)S(1)} %stack.80.place_ref, bf16[512,128]{1,0:T(8,128)(2,1)S(1)} %get-tuple-element.67.m0, bf16[512,128]{1,0:T(8,128)(2,1)S(1)} %collective-permute-done.15.m1, ...), custom_call_target="tpu_custom_call" | custom-call | flops 16000000000 | bytes 16000000 | tf_op jit(solution)/shard_map/attention/pallas_call | solution.py:31
  82.4 1.8 %collective-permute-start.21 = (bf16[2,144,384]{2,1,0:T(8,128)(2,1)S(1)}, bf16[2,144,384]{2,1,0:T(8,128)(2,1)S(1)}, u32[]{:S(2)}, u32[]{:S(2)}) collective-permute-start(bf16[2,144,384]{2,1,0:T(8,128)(2,1)S(1)} %get-tuple-element.76), channel_id=1, source_target_pairs={{0,16},{8,24},{16,0},{24,8},{1,17},{9,25},{17,1},{25,9},{2,18},{10... | collective-permute-start | bytes 663560 | tf_op jit(solution)/shard_map/ppermute | solution.py:513
  86.4 5.0 %collective-permute-done.20.p2 = bf16[2,144,384]{2,1,0:T(8,128)(2,1)S(1)} collective-permute-done((bf16[2,144,384]{2,1,0:T(8,128)(2,1)S(1)}, bf16[2,144,384]{2,1,0:T(8,128)(2,1)S(1)}, u32[]{:S(2)}, u32[]{:S(2)}) %collective-permute-start.20) | collective-permute-done | bytes 221216 | tf_op jit(solution)/shard_map/ppermute | solution.py:512
  94.2 2.0 %finish.1 = (bf16[4,48,2048]{2,1,0:T(8,128)(2,1)S(1)}, bf16[4,48,2048]{2,1,0:T(8,128)(2,1)S(1)}, f32[2,384]{1,0:T(2,128)}) custom-call(s32[1]{0:T(128)} %bitcast.place_ref, f32[1]{0:T(128)S(6)} %copy.19.lambda_ref, bf16[2,144,384]{2,1,0:T(8,128)(2,1)S(1)} %copy-done.17, bf16[2,144,384]{2,1,0:T(8,128)(2,1)S(1)} %collective-permute-done.19.p1, ...), custom_call_target="tpu_custom_call" | custom-call | flops 1000000000 | bytes 1000000 | tf_op jit(solution)/shard_map/finish/pallas_call | solution.py:31
  96.2 2.3 %collective-permute-done.22 = bf16[4,48,2048]{2,1,0:T(8,128)(2,1)S(1)} collective-permute-done((bf16[4,48,2048]{2,1,0:T(8,128)(2,1)S(1)}, bf16[4,48,2048]{2,1,0:T(8,128)(2,1)S(1)}, u32[]{:S(2)}, u32[]{:S(2)}) %collective-permute-start.22) | collective-permute-done | bytes 786464 | tf_op jit(solution)/shard_map/ppermute | solution.py:527
  98.8 16.6 %all_to_all.10 = bf16[4,48,2048]{2,1,0:T(8,128)(2,1)S(1)} all-to-all(bf16[4,48,2048]{2,1,0:T(8,128)(2,1)S(1)} %add_convert_fusion), channel_id=1, replica_groups=mesh['z'=8,'x'=4,'y'=4,'c'=2] {'y'}, dimensions={0} | all-to-all | bytes 1572864 | tf_op jit(solution)/shard_map/all_to_all | solution.py:529
  (95 shorter events, 21.3 us)
Async XLA Ops:
  0.7 8.2 %collective-permute-start = (bf16[384,256]{1,0:T(8,128)(2,1)}, bf16[384,256]{1,0:T(8,128)(2,1)S(1)}, u32[]{:S(2)}, u32[]{:S(2)}) collective-permute-start(bf16[384,256]{1,0:T(8,128)(2,1)} %param.17), channel_id=1, source_target_pairs={{0,2},{2,4},{4,6},{6,0},{1,3},{3,5},{5,7},{7,1},{8,10},{10,12},{12... | collective-permute-start | bytes 589832 | tf_op jit(solution)/shard_map/ppermute | solution.py:416
  2.3 6.9 %collective-permute-start.1 = (bf16[384,256]{1,0:T(8,128)(2,1)}, bf16[384,256]{1,0:T(8,128)(2,1)S(1)}, u32[]{:S(2)}, u32[]{:S(2)}) collective-permute-start(bf16[384,256]{1,0:T(8,128)(2,1)} %param.17), channel_id=1, source_target_pairs={{0,6},{2,0},{4,2},{6,4},{1,7},{3,1},{5,3},{7,5},{8,14},{10,8},{12,... | collective-permute-start | bytes 589832 | tf_op jit(solution)/shard_map/ppermute | solution.py:417
  4.0 11.4 %collective-permute-start.4 = (bf16[384,256]{1,0:T(8,128)(2,1)}, bf16[384,256]{1,0:T(8,128)(2,1)S(1)}, u32[]{:S(2)}, u32[]{:S(2)}) collective-permute-start(bf16[384,256]{1,0:T(8,128)(2,1)} %param.17), channel_id=1, source_target_pairs={{0,1},{1,0},{2,3},{3,2},{4,5},{5,4},{6,7},{7,6},{8,9},{9,8},{10,11... | collective-permute-start | bytes 589832 | tf_op jit(solution)/shard_map/ppermute | solution.py:421
  8.9 5.9 %collective-permute-start.2 = (bf16[192,256]{1,0:T(8,128)(2,1)S(1)}, bf16[192,256]{1,0:T(8,128)(2,1)S(1)}, u32[]{:S(2)}, u32[]{:S(2)}) collective-permute-start(bf16[192,256]{1,0:T(8,128)(2,1)S(1)} %slice.16), channel_id=1, source_target_pairs={{0,2},{2,4},{4,6},{6,0},{1,3},{3,5},{5,7},{7,1},{8,10},{10,12},{12... | collective-permute-start | bytes 294920 | tf_op jit(solution)/shard_map/ppermute | solution.py:418
  9.3 5.5 %collective-permute-start.3 = (bf16[192,256]{1,0:T(8,128)(2,1)S(1)}, bf16[192,256]{1,0:T(8,128)(2,1)S(1)}, u32[]{:S(2)}, u32[]{:S(2)}) collective-permute-start(bf16[192,256]{1,0:T(8,128)(2,1)S(1)} %slice.17), channel_id=1, source_target_pairs={{0,6},{2,0},{4,2},{6,4},{1,7},{3,1},{5,3},{7,5},{8,14},{10,8},{12,... | collective-permute-start | bytes 294920 | tf_op jit(solution)/shard_map/ppermute | solution.py:419
  12.3 4.0 %collective-permute-start.5 = (bf16[384,256]{1,0:T(8,128)(2,1)S(1)}, bf16[384,256]{1,0:T(8,128)(2,1)S(1)}, u32[]{:S(2)}, u32[]{:S(2)}) collective-permute-start(bf16[384,256]{1,0:T(8,128)(2,1)S(1)} %collective-permute-done.h1), channel_id=1, source_target_pairs={{0,1},{1,0},{2,3},{3,2},{4,5},{5,4},{6,7},{7,6},{8,9},{9,8},{10,11... | collective-permute-start | bytes 589832 | tf_op jit(solution)/shard_map/ppermute | solution.py:421
  12.3 4.0 %collective-permute-start.6 = (bf16[384,256]{1,0:T(8,128)(2,1)S(1)}, bf16[384,256]{1,0:T(8,128)(2,1)S(1)}, u32[]{:S(2)}, u32[]{:S(2)}) collective-permute-start(bf16[384,256]{1,0:T(8,128)(2,1)S(1)} %collective-permute-done.1.h2), channel_id=1, source_target_pairs={{0,1},{1,0},{2,3},{3,2},{4,5},{5,4},{6,7},{7,6},{8,9},{9,8},{10,11... | collective-permute-start | bytes 589832 | tf_op jit(solution)/shard_map/ppermute | solution.py:421
  14.8 1.3 %collective-permute-start.7 = (bf16[192,256]{1,0:T(8,128)(2,1)S(1)}, bf16[192,256]{1,0:T(8,128)(2,1)S(1)}, u32[]{:S(2)}, u32[]{:S(2)}) collective-permute-start(bf16[192,256]{1,0:T(8,128)(2,1)S(1)} %collective-permute-done.2.h3), channel_id=1, source_target_pairs={{0,1},{1,0},{2,3},{3,2},{4,5},{5,4},{6,7},{7,6},{8,9},{9,8},{10,11... | collective-permute-start | bytes 294920 | tf_op jit(solution)/shard_map/ppermute | solution.py:421
  14.8 1.5 %collective-permute-start.8 = (bf16[192,256]{1,0:T(8,128)(2,1)S(1)}, bf16[192,256]{1,0:T(8,128)(2,1)S(1)}, u32[]{:S(2)}, u32[]{:S(2)}) collective-permute-start(bf16[192,256]{1,0:T(8,128)(2,1)S(1)} %collective-permute-done.3.h4), channel_id=1, source_target_pairs={{0,1},{1,0},{2,3},{3,2},{4,5},{5,4},{6,7},{7,6},{8,9},{9,8},{10,11... | collective-permute-start | bytes 294920 | tf_op jit(solution)/shard_map/ppermute | solution.py:421
  18.5 8.5 %collective-permute-start.10 = (bf16[384,256]{1,0:T(8,128)(2,1)S(1)}, bf16[384,256]{1,0:T(8,128)(2,1)S(1)}, u32[]{:S(2)}, u32[]{:S(2)}) collective-permute-start(bf16[384,256]{1,0:T(8,128)(2,1)S(1)} %get-tuple-element.43.refs_0_), channel_id=1, source_target_pairs={{0,224},{32,0},{64,32},{96,64},{128,96},{160,128},{192,160},{224,1... | collective-permute-start | bytes 589832 | tf_op jit(solution)/shard_map/ppermute | solution.py:444
  19.6 7.4 %collective-permute-start.9 = (bf16[384,256]{1,0:T(8,128)(2,1)S(1)}, bf16[384,256]{1,0:T(8,128)(2,1)S(1)}, u32[]{:S(2)}, u32[]{:S(2)}) collective-permute-start(bf16[384,256]{1,0:T(8,128)(2,1)S(1)} %get-tuple-element.43.refs_0_), channel_id=1, source_target_pairs={{0,32},{32,64},{64,96},{96,128},{128,160},{160,192},{192,224},{224... | collective-permute-start | bytes 589832 | tf_op jit(solution)/shard_map/ppermute | solution.py:443
  27.0 9.8 %collective-permute-start.11 = (bf16[384,256]{1,0:T(8,128)(2,1)S(1)}, bf16[384,256]{1,0:T(8,128)(2,1)S(1)}, u32[]{:S(2)}, u32[]{:S(2)}) collective-permute-start(bf16[384,256]{1,0:T(8,128)(2,1)S(1)} %collective-permute-done.9.refs_1_), channel_id=1, source_target_pairs={{0,32},{32,64},{64,96},{96,128},{128,160},{160,192},{192,224},{224... | collective-permute-start | bytes 589832 | tf_op jit(solution)/shard_map/ppermute | solution.py:461
  30.0 7.0 %collective-permute-start.12 = (bf16[384,256]{1,0:T(8,128)(2,1)S(1)}, bf16[384,256]{1,0:T(8,128)(2,1)S(1)}, u32[]{:S(2)}, u32[]{:S(2)}) collective-permute-start(bf16[384,256]{1,0:T(8,128)(2,1)S(1)} %collective-permute-done.10.refs_2_), channel_id=1, source_target_pairs={{0,224},{32,0},{64,32},{96,64},{128,96},{160,128},{192,160},{224,1... | collective-permute-start | bytes 589832 | tf_op jit(solution)/shard_map/ppermute | solution.py:462
  36.9 12.8 %collective-permute-start.13 = (bf16[384,256]{1,0:T(8,128)(2,1)S(1)}, bf16[384,256]{1,0:T(8,128)(2,1)S(1)}, u32[]{:S(2)}, u32[]{:S(2)}) collective-permute-start(bf16[384,256]{1,0:T(8,128)(2,1)S(1)} %collective-permute-done.11.refs_3_), channel_id=1, source_target_pairs={{0,32},{32,64},{64,96},{96,128},{128,160},{160,192},{192,224},{224... | collective-permute-start | bytes 589832 | tf_op jit(solution)/shard_map/ppermute | solution.py:472
  40.0 9.7 %collective-permute-start.14 = (bf16[384,256]{1,0:T(8,128)(2,1)S(1)}, bf16[384,256]{1,0:T(8,128)(2,1)S(1)}, u32[]{:S(2)}, u32[]{:S(2)}) collective-permute-start(bf16[384,256]{1,0:T(8,128)(2,1)S(1)} %collective-permute-done.12.refs_4_), channel_id=1, source_target_pairs={{0,224},{32,0},{64,32},{96,64},{128,96},{160,128},{192,160},{224,1... | collective-permute-start | bytes 589832 | tf_op jit(solution)/shard_map/ppermute | solution.py:473
  40.0 7.6 %collective-permute-start.15 = (bf16[512,128]{1,0:T(8,128)(2,1)S(1)}, bf16[512,128]{1,0:T(8,128)(2,1)S(1)}, u32[]{:S(2)}, u32[]{:S(2)}) collective-permute-start(bf16[512,128]{1,0:T(8,128)(2,1)S(1)} %get-tuple-element.67.m0), channel_id=1, source_target_pairs={{0,8},{8,16},{16,24},{24,0},{1,9},{9,17},{17,25},{25,1},{2,10},{10... | collective-permute-start | bytes 393224 | tf_op jit(solution)/shard_map/ppermute | solution.py:476
  41.5 6.1 %collective-permute-start.16 = (bf16[512,128]{1,0:T(8,128)(2,1)S(1)}, bf16[512,128]{1,0:T(8,128)(2,1)S(1)}, u32[]{:S(2)}, u32[]{:S(2)}) collective-permute-start(bf16[512,128]{1,0:T(8,128)(2,1)S(1)} %get-tuple-element.67.m0), channel_id=1, source_target_pairs={{0,24},{8,0},{16,8},{24,16},{1,25},{9,1},{17,9},{25,17},{2,26},{10... | collective-permute-start | bytes 393224 | tf_op jit(solution)/shard_map/ppermute | solution.py:477
  43.2 6.5 %collective-permute-start.17 = (bf16[512,128]{1,0:T(8,128)(2,1)S(1)}, bf16[512,128]{1,0:T(8,128)(2,1)S(1)}, u32[]{:S(2)}, u32[]{:S(2)}) collective-permute-start(bf16[512,128]{1,0:T(8,128)(2,1)S(1)} %get-tuple-element.67.m0), channel_id=1, source_target_pairs={{0,16},{8,24},{16,0},{24,8},{1,17},{9,25},{17,1},{25,9},{2,18},{10... | collective-permute-start | bytes 393224 | tf_op jit(solution)/shard_map/ppermute | solution.py:478
  49.7 9.6 %collective-permute-start.18 = (bf16[384,256]{1,0:T(8,128)(2,1)S(1)}, bf16[384,256]{1,0:T(8,128)(2,1)S(1)}, u32[]{:S(2)}, u32[]{:S(2)}) collective-permute-start(bf16[384,256]{1,0:T(8,128)(2,1)S(1)} %collective-permute-done.13.refs_5_), channel_id=1, source_target_pairs={{0,32},{32,64},{64,96},{96,128},{128,160},{160,192},{192,224},{224... | collective-permute-start | bytes 589832 | tf_op jit(solution)/shard_map/ppermute | solution.py:481
  54.8 30.0 %all-to-all-start = ((bf16[8,128,128]{2,1,0:T(8,128)(2,1)}), bf16[8,128,128]{2,1,0:T(8,128)(2,1)S(1)}, u32[]{:S(2)}, u32[]{:S(2)}) async-start(bf16[8,128,128]{2,1,0:T(8,128)(2,1)} %get-tuple-element.79), calls=%async_computation | async-start | bytes 524288 | tf_op jit(solution)/shard_map/all_to_all | solution.py:487
  80.3 6.0 %collective-permute-start.19 = (bf16[2,144,384]{2,1,0:T(8,128)(2,1)S(1)}, bf16[2,144,384]{2,1,0:T(8,128)(2,1)S(1)}, u32[]{:S(2)}, u32[]{:S(2)}) collective-permute-start(bf16[2,144,384]{2,1,0:T(8,128)(2,1)S(1)} %get-tuple-element.74), channel_id=1, source_target_pairs={{0,24},{8,0},{16,8},{24,16},{1,25},{9,1},{17,9},{25,17},{2,26},{10... | collective-permute-start | bytes 663560 | tf_op jit(solution)/shard_map/ppermute | solution.py:511
  81.9 9.5 %collective-permute-start.20 = (bf16[2,144,384]{2,1,0:T(8,128)(2,1)S(1)}, bf16[2,144,384]{2,1,0:T(8,128)(2,1)S(1)}, u32[]{:S(2)}, u32[]{:S(2)}) collective-permute-start(bf16[2,144,384]{2,1,0:T(8,128)(2,1)S(1)} %get-tuple-element.75), channel_id=1, source_target_pairs={{0,8},{8,16},{16,24},{24,0},{1,9},{9,17},{17,25},{25,1},{2,10},{10... | collective-permute-start | bytes 663560 | tf_op jit(solution)/shard_map/ppermute | solution.py:512
  82.4 9.0 %collective-permute-start.21 = (bf16[2,144,384]{2,1,0:T(8,128)(2,1)S(1)}, bf16[2,144,384]{2,1,0:T(8,128)(2,1)S(1)}, u32[]{:S(2)}, u32[]{:S(2)}) collective-permute-start(bf16[2,144,384]{2,1,0:T(8,128)(2,1)S(1)} %get-tuple-element.76), channel_id=1, source_target_pairs={{0,16},{8,24},{16,0},{24,8},{1,17},{9,25},{17,1},{25,9},{2,18},{10... | collective-permute-start | bytes 663560 | tf_op jit(solution)/shard_map/ppermute | solution.py:513
  96.2 2.3 %collective-permute-start.22 = (bf16[4,48,2048]{2,1,0:T(8,128)(2,1)S(1)}, bf16[4,48,2048]{2,1,0:T(8,128)(2,1)S(1)}, u32[]{:S(2)}, u32[]{:S(2)}) collective-permute-start(bf16[4,48,2048]{2,1,0:T(8,128)(2,1)S(1)} %get-tuple-element.82), channel_id=1, source_target_pairs={{0,1},{1,0},{2,3},{3,2},{4,5},{5,4},{6,7},{7,6},{8,9},{9,8},{10,11... | collective-permute-start | bytes 2359304 | tf_op jit(solution)/shard_map/ppermute | solution.py:527
  (25 other events, 185.2 us)

commit v2 on v1

--- a/solution.py
+++ b/solution.py
@@ -19,7 +19,6 @@
 KEY_EPS = 1e-06
 NEGATIVE = -1e30
 SPAN = 64
-GROUP = 12
 MIB = 1024 * 1024
 GRANT = 28
 NT = (((1,), (1,)), ((), ()))
@@ -75,14 +74,13 @@
 
 
 def project_kernel(
-    piece_ref,
-    own, h1, h2, h3, h4, g0, g1, g2, g3, g4, gain_ref, weights,
+    own, h1, h2, h3, g0, g1, g2, g3, gain_ref, weights,
     normed, q_out, kv_out,
 ):
     half = own.shape[0] // 2
     pieces = [
-        h1[...], h2[...], jnp.concatenate([h3[...], h4[...]], axis=0),
-        g0[...], g1[...], g2[...], jnp.concatenate([g3[...], g4[...]], axis=0),
+        h1[...], h2[...], h3[...],
+        g0[...], g1[...], g2[...], g3[...],
         jnp.concatenate([own[half:], own[:half]], axis=0),
     ]
     squares = None
@@ -92,13 +90,25 @@
         part = part[:, :128] + part[:, 128:]
         squares = part if squares is None else squares + part
     scale = lax.rsqrt(jnp.sum(squares, axis=-1, keepdims=True) / 2048.0 + NORM_EPS)
-    for number, piece in enumerate(pieces):
-        place = piece_ref[number]
+    y, core = lax.axis_index("y"), lax.axis_index("c")
+    ys = [(y + 3) & 3, (y + 1) & 3, (y + 2) & 3]
+    places = [2 * a + core for a in ys] + [2 * a + 1 - core for a in (y, *ys)] + [2 * y + core]
+    for place, piece in zip(places, pieces):
         gain = gain_ref[pl.ds(place, 1), :]
         value = (piece.astype(F32) * scale * gain).astype(BF16)
         normed[:, pl.ds(pl.multiple_of(place * 256, 256), 256)] = value
     kv_out[...] = dot(normed[...], weights[:, :256]).astype(BF16)
     q_out[...] = dot(normed[...], weights[:, 256:]).astype(BF16)
+
+
+def line_places():
+    x = lax.axis_index("x")
+    return [x, (x + 3) & 3, (x + 1) & 3, (x + 2) & 3]
+
+
+def ring_places():
+    z = lax.axis_index("z")
+    return [z] + [(z + 8 + s) & 7 for s in (-1, 1, -2, 2, -3, 3, 4)]
 
 
 def same_head():
@@ -184,17 +194,27 @@
     diagonal = diagonal_mask()
     first = lane_ids((SPAN, 128)) < HD
     keep = (first, jnp.logical_not(first))
-    solved = []
-    group = GROUP
-    for base in range(0, 2 * count, group):
-        lowers = [lower_ref[base + n] for n in range(group)]
-        state = [[rhs_ref[base + n, 8 * b : 8 * b + 8] for b in range(SPAN // 8)] for n in range(group)]
-        for s in range(SPAN - 1):
-            for n in range(group):
+    units = range(2 * count)
+    lowers = [lower_ref[n] for n in units]
+    state = [[rhs_ref[n, 8 * b : 8 * b + 8] for b in range(SPAN // 8)] for n in units]
+    half = SPAN // 2
+
+    def substitute(start):
+        for s in range(start, start + half - 1):
+            for n in units:
                 row = state[n][s // 8][s % 8 : s % 8 + 1]
-                for b in range(s // 8 if s % 8 < 7 else s // 8 + 1, SPAN // 8):
+                for b in range(s // 8 if s % 8 < 7 else s // 8 + 1, (start + half) // 8):
                     state[n][b] = state[n][b] + lowers[n][8 * b : 8 * b + 8, s : s + 1] * row
-        solved += [jnp.concatenate(one, axis=0) for one in state]
+
+    substitute(0)
+    rest = jnp.zeros((128 - half, 128), F32)
+    for n in units:
+        above = jnp.concatenate(state[n][: half // 8] + [rest], axis=0)
+        more = exact(lowers[n][half:], above)
+        for b in range(half // 8, SPAN // 8):
+            state[n][b] = state[n][b] + more[8 * b - half : 8 * b - half + 8]
+    substitute(half)
+    solved = [jnp.concatenate(one, axis=0) for one in state]
     prefix = jnp.where(diagonal, 1.0, 0.0).astype(F32)
     for c in range(count):
         got, moved = [], []
@@ -215,65 +235,76 @@
     message_out[rows:, :] = prefix.astype(BF16)
 
 
-def along_x_kernel(place_ref, m0, m1, m2, m3, before_out, total_out, parts):
+def along_x_kernel(m0, m1, m2, m3, before_out, total_out, parts):
     rows = m0.shape[0] - 128
     same = same_head()
     identity = jnp.where(diagonal_mask(), 1.0, 0.0).astype(BF16)
-    mine = place_ref[1]
-    for n, ref in enumerate((m0, m1, m2, m3)):
-        parts[place_ref[10 + n]] = ref[rows:, :]
+    mine = lax.axis_index("x")
+    for place, ref in zip(line_places(), (m0, m1, m2, m3)):
+        parts[place] = ref[rows:, :]
     total = parts[0]
     for j in range(1, 4):
         total = compose(total, parts[j], same)
-    for n in range(8):
-        total_out[n] = total.astype(BF16)
+    total_out[...] = total.astype(BF16)
     before = jnp.where(mine > 0, parts[0], identity)
     for j in range(1, 3):
         before = compose(before, jnp.where(j < mine, parts[j], identity), same)
     before_out[...] = before
 
 
-def along_z_kernel(place_ref, parts_ref, before_ref, state_out):
+def window_kernel(line_ref, p1, p2, p3, window_out, near_out):
     same = same_head()
     identity = jnp.where(diagonal_mask(), 1.0, 0.0).astype(BF16)
-    mine = place_ref[0]
-    level = [jnp.where(j < mine, parts_ref[j], identity) for j in range(7)]
-    level.append(before_ref[...])
-    while len(level) > 1:
-        level = [compose(level[i], level[i + 1], same) for i in range(0, len(level), 2)]
-    state_out[...] = jnp.where(same, 0.0, level[0])
+    mine = lax.axis_index("z")
+    near = jnp.where(mine >= 3, p3[...], identity)
+    for far, part in ((2, p2), (1, p1)):
+        near = compose(near, jnp.where(mine >= far, part[...], identity), same)
+    near_out[...] = near
+    window_out[...] = compose(near, line_ref[...], same).astype(BF16)
+
+
+def state_before(window, near, before):
+    same = same_head()
+    identity = jnp.where(diagonal_mask(), 1.0, 0.0).astype(BF16)
+    window = jnp.where(lax.axis_index("z") >= 4, window, identity)
+    total = compose(compose(window, near, same), before, same)
+    return jnp.where(same, 0.0, total)
 
 
 TALL = 144
 
 
-def attention_kernel(
-    place_ref, m0, m1, m2, m3, *refs
-):
-    kvs, outs = refs[:8], refs[8:12]
-    row_max, weighted, queries, keys, turned, scores, weights, rescales, units = refs[12:]
-    rows = m0.shape[0] - 128
+def attention_kernel(pair, *refs):
+    lead, refs = refs[:2], refs[2:]
+    taken = 8 if pair else 2
+    kvs, refs = refs[:taken], refs[taken:]
+    outs, refs = refs[:2], refs[2:]
+    keys, turned = refs[:2] if pair else kvs
+    row_max, weighted, queries, scores, units = refs[2:] if pair else refs
+    rows = lead[0].shape[0] - 128
     wide = 2 * rows
-    my_z, my_x = place_ref[0], place_ref[1]
+    blocks_at, lines_at = ring_places(), line_places()
+    my_z, my_x = blocks_at[0], lines_at[0]
     first = lane_ids((rows, 128)) < HD
-    for n, ref in enumerate((m0, m1, m2, m3)):
+    for n, ref in enumerate(lead):
         scaled = (ref[:rows, :].astype(F32) * (HD**-0.5)).astype(BF16)
-        at = slice((n % 2) * rows, (n % 2 + 1) * rows)
-        queries[2 * (n // 2), at, :] = jnp.where(first, scaled, 0).astype(BF16)
-        queries[2 * (n // 2) + 1, at, :] = jnp.where(first, 0, scaled).astype(BF16)
-    ones = jnp.where(row_ids((TALL - 128, rows)) == 0, 1.0, 0.0).astype(BF16)
-    for n, ref in enumerate(kvs):
-        keys[n] = ref[:, :128]
-        turned[n, :128, :] = jnp.transpose(ref[:, 128:])
-        turned[n, 128:, :] = ones
+        at = slice(n * rows, (n + 1) * rows)
+        queries[0, at, :] = jnp.where(first, scaled, 0).astype(BF16)
+        queries[1, at, :] = jnp.where(first, 0, scaled).astype(BF16)
+    if pair:
+        ones = jnp.where(row_ids((TALL - 128, rows)) == 0, 1.0, 0.0).astype(BF16)
+        for n, ref in enumerate(kvs):
+            keys[n] = ref[:, :128]
+            turned[n, :128, :] = jnp.transpose(ref[:, 128:])
+            turned[n, 128:, :] = ones
     row_max[...] = jnp.full_like(row_max, NEGATIVE)
     weighted[...] = jnp.zeros_like(weighted)
 
-    def score(pair, n, out):
+    def score(n, out):
         for m in range(2):
-            out[m] = dot(keys[n], queries[2 * pair + m], NT)
-
-    def soften(slot, source, target, factors, limit=None):
+            out[m] = dot(keys[n], queries[m], NT)
+
+    def soft_gather(slot, n, source, limit=None):
         for m in range(2):
             i = 2 * slot + m
             got = source[m]
@@ -281,65 +312,48 @@
                 got = jnp.where(row_ids((rows, wide)) <= limit, got, NEGATIVE)
             old = row_max[i, :1, :]
             new = jnp.maximum(old, jnp.max(got, axis=0, keepdims=True))
-            target[m] = jnp.exp(got - new).astype(BF16)
-            factors[m] = jnp.broadcast_to(jnp.exp(old - new), (8, wide))
+            soft = jnp.exp(got - new).astype(BF16)
             row_max[i] = jnp.broadcast_to(new, (8, wide))
-
-    def gather(slot, n, source, factors):
-        for m in range(2):
-            i = 2 * slot + m
-            weighted[i] = weighted[i] * factors[m, :1, :] + dot(turned[n], source[m])
-
-    def put(at, pair, n, slot):
-        units[0, at] = pair
-        units[1, at] = n
-        units[2, at] = slot
-
-    put(0, 1, 0, 1)
-    total = jnp.int32(1)
+            weighted[i] = weighted[i] * jnp.exp(old - new) + dot(turned[n], soft)
+
+    def put(at, n, slot):
+        units[0, at] = n
+        units[1, at] = slot
+
+    total = jnp.int32(0)
     for n in range(1, 8):
-        wanted = place_ref[2 + n] < my_z
-        for pair in range(2):
-            put(total, pair, n, pair)
-            total = total + wanted.astype(jnp.int32)
-    for extra in range(4):
-        put(total + extra, 0, 0, 2)
+        put(total, n, 0)
+        total = total + (blocks_at[n] < my_z).astype(jnp.int32)
+    for extra in range(3):
+        put(total + extra, 0, 1)
 
     column = lane_ids((1, wide))
     within = jnp.where(column < rows, column, column - rows)
-
-    def limit(pair):
-        x_of = jnp.where(column < rows, place_ref[10 + 2 * pair], place_ref[11 + 2 * pair])
-        return jnp.where(x_of > my_x, rows, jnp.where(x_of == my_x, within, -1))
-
-    score(0, 0, scores[0])
-    score(1, 0, scores[1])
-    soften(0, scores[0], weights[0], rescales[0], limit(0))
-    score(units[0, 1], units[1, 1], scores[0])
-    soften(1, scores[1], weights[1], rescales[1], limit(1))
-    gather(0, 0, weights[0], rescales[0])
+    x_of = jnp.where(column < rows, lines_at[2 * pair], lines_at[2 * pair + 1])
+    limit = jnp.where(x_of > my_x, rows, jnp.where(x_of == my_x, within, -1))
+    score(0, scores[1])
+    score(units[0, 0], scores[0])
+    soft_gather(0, 0, scores[1], limit)
 
     def step(at, now, other):
-        score(units[0, at + 1], units[1, at + 1], scores[other])
-        soften(units[2, at], scores[now], weights[now], rescales[now])
-        gather(units[2, at - 1], units[1, at - 1], weights[other], rescales[other])
+        score(units[0, at + 1], scores[other])
+        soft_gather(units[1, at], units[0, at], scores[now])
 
     def two(t, carry):
-        step(2 * t + 1, 0, 1)
-        step(2 * t + 2, 1, 0)
+        step(2 * t, 0, 1)
+        step(2 * t + 1, 1, 0)
         return carry
 
     lax.fori_loop(0, (total + 1) // 2, two, 0)
 
     for n, out in enumerate(outs):
-        at = slice((n % 2) * rows, (n % 2 + 1) * rows)
+        at = slice(n * rows, (n + 1) * rows)
         for m in range(2):
-            i = 2 * (n // 2) + m
-            top = row_max[i, :1, at]
+            top = row_max[m, :1, at]
             some = top > 0.5 * NEGATIVE
-            row_sum = jnp.where(some, weighted[i, 128:129, at], 1.0)
+            row_sum = jnp.where(some, weighted[m, 128:129, at], 1.0)
             share = jnp.where(some, 1.0 / row_sum, 0.0)
-            out[m, :128, :] = (weighted[i, :128, at] * share).astype(BF16)
+            out[m, :128, :] = (weighted[m, :128, at] * share).astype(BF16)
             logs = jnp.where(some, top + jnp.log(row_sum), NEGATIVE)
             high = logs.astype(BF16).astype(F32)
             middle = (logs - high).astype(BF16).astype(F32)
@@ -349,7 +363,7 @@
 
 
 def finish_kernel(
-    place_ref, lambda_ref, p0, p1, p2, p3, read_ref, local_ref, state_ref, wr_ref, wa_ref,
+    lambda_ref, p0, p1, p2, p3, read_ref, local_ref, window_ref, near_ref, before_ref, wr_ref, wa_ref,
     mine_out, other_out, logs_out,
 ):
     rows = read_ref.shape[0]
@@ -369,10 +383,11 @@
             term = p[m, :128, :].astype(F32) * (share / total)
             got = term if got is None else got + term
         maps.append(got)
-    head = maps[0] - lambda_ref[0] * maps[1]
+    head = maps[0] - lambda_ref[...] * maps[1]
     head = head * lax.rsqrt(jnp.mean(head * head, axis=0, keepdims=True) + HEAD_EPS)
     att_mix = jnp.transpose(head.astype(BF16))
-    recurrent = local_ref[...] + exact(read_ref[...], state_ref[...], NT)
+    state = state_before(window_ref[...], near_ref[...], before_ref[...])
+    recurrent = local_ref[...] + exact(read_ref[...], state, NT)
     recurrent = pltpu.roll(recurrent, HD, 1)
     first = lane_ids((rows, 128)) < HD
 
@@ -384,20 +399,30 @@
     centered = recurrent - per_head(recurrent)
     rec_mix = (centered * lax.rsqrt(per_head(centered * centered) + GROUP_EPS)).astype(BF16)
     mix = jnp.concatenate([rec_mix, att_mix], axis=1)
-    core = place_ref[0]
+    core, y = lax.axis_index("c"), lax.axis_index("y")
     for n in range(8):
         at = slice(256 * n, 256 * n + 256)
         weight = jnp.concatenate([wr_ref[:, at], wa_ref[:, at]], axis=0)
         got = dot(mix, weight).astype(BF16)
-        for y in range(4):
-            even = got[96 * y : 96 * y + 48]
-            odd = got[96 * y + 48 : 96 * y + 96]
-            mine_out[y, :, at] = jnp.where(core == 0, even, odd)
-            other_out[y, :, at] = jnp.where(core == 0, odd, even)
-
-
-def rms_rows(values, gain):
-    return values * lax.rsqrt(jnp.mean(values * values, axis=-1, keepdims=True) + NORM_EPS) * gain
+        for place in range(4):
+            even = got[96 * place : 96 * place + 48]
+            odd = got[96 * place + 48 : 96 * place + 96]
+            mine_out[(place - y) & 3, :, at] = jnp.where(core == 0, even, odd)
+            other_out[(place - y) & 3, :, at] = jnp.where(core == 0, odd, even)
+
+
+def pair_kernel(mine_ref, other_ref, *outs):
+    for n, out in enumerate(outs):
+        total = mine_ref[n].astype(F32) + other_ref[n].astype(F32)
+        out[...] = total.astype(out.dtype)
+
+
+def norm_kernel(own_ref, p1, p2, p3, gain_ref, out_ref):
+    total = own_ref[...]
+    for part in (p1, p2, p3):
+        total = total + part[...].astype(F32)
+    scale = lax.rsqrt(jnp.mean(total * total, axis=-1, keepdims=True) + NORM_EPS)
+    out_ref[...] = (total * scale * gain_ref[...]).astype(BF16)
 
 
 def per_device(
@@ -407,7 +432,6 @@
 ):
     permute = lax.ppermute
     together = lax.optimization_barrier
-    z, x, y, core = (lax.axis_index(a) for a in ("z", "x", "y", "c"))
     rows = hidden_in.shape[0]
     half = rows // 2
     count = rows // SPAN
@@ -415,26 +439,14 @@
 
     up = permute(hidden_in, "y", ring(4, 1))
     down = permute(hidden_in, "y", ring(4, -1))
-    far_a = permute(up[:half], "y", ring(4, 1))
-    far_b = permute(down[half:], "y", ring(4, -1))
-    mine = [up, down, far_a, far_b]
+    mine = [up, down, permute(hidden_in, "y", ring(4, 2))]
     theirs = [permute(a, "c", ring(2, 1)) for a in (hidden_in, *mine)]
-    ys = [(y + 3) % 4, (y + 1) % 4, (y + 2) % 4, y]
-    piece_at = jnp.stack(
-        [2 * a + core for a in ys[:3]] + [2 * a + 1 - core for a in (y, *ys[:3])] + [2 * y + core]
-    ).astype(jnp.int32)
-    places = jnp.stack(
-        [z, x, z]
-        + [a for s in (1, 2, 3) for a in ((z + 8 - s) % 8, (z + s) % 8)]
-        + [(z + 4) % 8, x, (x + 3) % 4, (x + 1) % 4, (x + 2) % 4]
-    ).astype(jnp.int32)
-
     turned_in = jnp.concatenate([hidden_in[half:], hidden_in[:half]], axis=0)
     pair_weights = jnp.concatenate([key_pair, value_pair, query_pair], axis=2).reshape(2048, 384)
     normed, q, kv = call(
         project_kernel,
         (shaped((rows, 2048), BF16), shaped((rows, 128), BF16), shaped((rows, 256), BF16)),
-        (piece_at,),
+        (),
         (turned_in, *mine, *theirs, in_gain.reshape(8, 256), pair_weights),
         flops=2 * rows * 2048 * 896,
         name="project",
@@ -481,54 +493,74 @@
     right4 = permute(right3, "z", ring(8, 1))
     before, line = call(
         along_x_kernel,
-        (shaped((128, 128), F32), shaped((8, 128, 128), BF16)),
-        (places,), messages, scratch=(pltpu.VMEM((4, 128, 128), BF16),), flops=10**8, name="along_x",
-    )
-    line_parts = lax.all_to_all(line, "z", 0, 0, tiled=True)
+        (shaped((128, 128), F32), shaped((128, 128), BF16)),
+        (), messages, scratch=(pltpu.VMEM((4, 128, 128), BF16),), flops=10**8, name="along_x",
+    )
+    lines = [permute(line, "z", ring(8, s)) for s in (1, 2, 3)]
 
     payload = shaped((2, TALL, rows), BF16)
     wide = 2 * rows
 
-    def pair(shape, kind):
-        return [pltpu.VMEM(shape, kind)] * 2
-
-    outs = call(
-        attention_kernel,
-        (payload,) * 4,
-        (places,),
-        (*messages, kv, right1, left1, right2, left2, right3, left3, right4),
-        scratch=[
-            pltpu.VMEM((6, 8, wide), F32), pltpu.VMEM((6, TALL, wide), F32),
-            pltpu.VMEM((4, wide, 128), BF16), pltpu.VMEM((8, rows, 128), BF16),
-            pltpu.VMEM((8, TALL, rows), BF16), pair((2, rows, wide), F32),
-            pair((2, rows, wide), BF16), pair((2, 8, wide), F32), pltpu.SMEM((3, 32), jnp.int32),
-        ],
-        flops=16 * 10**9,
-        name="attention",
-    )
-    back = [
-        outs[0],
-        permute(outs[1], "x", ring(4, -1)),
-        permute(outs[2], "x", ring(4, 1)),
-        permute(outs[3], "x", ring(4, 2)),
-    ]
-    state = call(
-        along_z_kernel, shaped((128, 128), F32), (places,), (line_parts, before),
-        flops=10**8, name="along_z",
-    )
+    def attend(pair, lead, arrays):
+        return call(
+            functools.partial(attention_kernel, pair),
+            (payload,) * 2
+            + ((shaped((8, rows, 128), BF16), shaped((8, TALL, rows), BF16)) if pair else ()),
+            (),
+            (*lead, *arrays),
+            scratch=[
+                pltpu.VMEM((4, 8, wide), F32), pltpu.VMEM((4, TALL, wide), F32),
+                pltpu.VMEM((2, wide, 128), BF16), [pltpu.VMEM((2, rows, wide), F32)] * 2,
+                pltpu.SMEM((2, 16), jnp.int32),
+            ],
+            flops=8 * 10**9,
+            name=f"attention{pair}",
+        )
+
+    to_next, to_far, keys, turned = attend(
+        1, messages[2:], (kv, right1, left1, right2, left2, right3, left3, right4)
+    )
+    to_next, to_far, keys, turned, line, lines = together((to_next, to_far, keys, turned, line, lines))
+    from_before = permute(to_next, "x", ring(4, 1))
+    from_far = permute(to_far, "x", ring(4, 2))
+    window, near = call(
+        window_kernel,
+        (shaped((128, 128), BF16), shaped((128, 128), F32)),
+        (), (line, *lines), flops=10**8, name="window",
+    )
+    window, keys = together((window, keys))
+    window = permute(window, "z", ring(8, 4))
+    ours, to_before = attend(0, messages[:2], (keys, turned))
+    back = [ours, from_before, permute(to_before, "x", ring(4, -1)), from_far]
     ours, others, log_sums = call(
         finish_kernel,
         (shaped((4, rows // 8, 2048), BF16), shaped((4, rows // 8, 2048), BF16), shaped((2, rows), F32)),
-        (core.reshape(1), mix_lambda),
-        (*back, read, local, state, out_recurrent, out_attention),
+        (),
+        (mix_lambda.reshape(1, 1), *back, read, local, window, near, before, out_recurrent, out_attention),
         flops=10**9,
         name="finish",
     )
     theirs = permute(others, "c", ring(2, 1))
-    summed = (ours.astype(F32) + theirs.astype(F32)).astype(BF16)
-    parts = lax.all_to_all(summed, "y", 0, 0, tiled=True)
-    projected = jnp.sum(parts.astype(F32), axis=0)
-    layer_out = rms_rows(projected, out_gain).astype(BF16)
+    piece = (rows // 8, 2048)
+    own, plus1, plus2, plus3 = call(
+        pair_kernel,
+        (shaped(piece, F32),) + (shaped(piece, BF16),) * 3,
+        (), (ours, theirs), flops=10**8, name="pair",
+    )
+    layer_out = call(
+        norm_kernel,
+        shaped(piece, BF16),
+        (),
+        (
+            own,
+            permute(plus1, "y", ring(4, 1)),
+            permute(plus3, "y", ring(4, -1)),
+            permute(plus2, "y", ring(4, 2)),
+            out_gain.reshape(1, 2048),
+        ),
+        flops=10**8,
+        name="norm",
+    )
     return (layer_out, log_sums[None])
 
 

time: 117 us -> 101 us (0.86)
  blocking collectives: 16.6 us -> 0 us
  waiting for transfers between devices: 19.8 us -> 33.2 us
  local copies, waits for them, and re-layouts: 8.57 us -> 1.74 us
  Pallas kernels: 33.1 us -> 28.7 us
  other arithmetic: 2.89 us -> 1.58 us
    all_to_all x1 -> x0, blocking collectives: 16.6 us -> none  [per_device(): parts = lax.all_to_all(summed, 'y', 0, 0, tiled=True)]
    ppermute x5 -> x11, waiting for transfers between devices: 7.26 us -> 18 us  [the longest x1 9.1 us: per_device(): permute(plus1, 'y', ring(4, 1))]
    unnamed x50 -> x22, local copies, waits for them, and re-layouts: 8.36 us -> 0.07 us
    ppermute x5 -> x11, starting transfers between devices: 7.24 us -> 13.8 us  [the longest x3 4.57 us: per_device(): lines = [permute(line, 'z', ring(8, s)) for s in (1, 2, 3)]]
    all_to_all x1 -> x0, starting transfers between devices: 4.51 us -> none  [per_device(): line_parts = lax.all_to_all(line, 'z', 0, 0, tiled=True)]
    pallas_call x7 -> x10, Pallas kernels: 33.1 us -> 28.7 us  [call(): pl.pallas_call(kernel, out_shape=outs, in_specs=[pl.BlockSpec(memory_spac...]
    ppermute x1, waiting for transfers between devices: 0.01 us -> 3.7 us  [per_device(): down = permute(hidden_in, 'y', ring(4, -1))]
    ppermute x1, starting transfers between devices: 2.23 us -> 0.08 us  [per_device(): right = permute(kv, 'z', ring(8, 1))]
  transfers between devices with their start and end apart: 24 -> 28, of which waited for: 11 -> 11; matrix products, arithmetic and copies ran while one was open for 2% -> 3% of each run, Pallas kernels for 25% -> 16%
where the time goes in v2:
time: 101 us; the launch traced here: 100 us
  starting transfers between devices  33.7 us (33%)
  waiting for transfers between devices  33.2 us (33%)
  Pallas kernels  28.7 us (28%)
  local copies, waits for them, and re-layouts  1.74 us (2%)
  other arithmetic  1.58 us (2%)
  between operations  1.55 us (2%)
    pallas_call x10, Pallas kernels, call(): pl.pallas_call(kernel, out_shape=outs, in_specs=[pl.BlockSpec(memory_spac...  28.7 us
    ppermute x1, waiting for transfers between devices, per_device(): permute(plus1, 'y', ring(4, 1))  9.1 us
    ppermute x1, waiting for transfers between devices, per_device(): window = permute(window, 'z', ring(8, 4))  7.17 us
    ppermute x3, starting transfers between devices, per_device(): lines = [permute(line, 'z', ring(8, s)) for s in (1, 2, 3)]  4.57 us
    ppermute x1, waiting for transfers between devices, per_device(): down = permute(hidden_in, 'y', ring(4, -1))  3.7 us
    ppermute x1, starting transfers between devices, per_device(): right4 = permute(right3, 'z', ring(8, 1))  3.24 us
    ppermute x1, starting transfers between devices, per_device(): right = permute(right2, 'z', ring(8, 1))  2.95 us
    ppermute x1, starting transfers between devices, per_device(): right = permute(right1, 'z', ring(8, 1))  2.79 us
  transfers between devices with their start and end apart: 28, of which 11 were waited for; matrix products, arithmetic and copies ran while one was open for 3% of the time, Pallas kernels for 16%

profile of v2, /device:TPU:224, one launch (start us, length us, event | category | flops | bytes accessed | tf_op | source)
XLA Modules:
  0.0 100.4 jit_solution(14531174966897061877)
XLA Ops:
  3.9 2.0 %collective-permute-start.2 = (bf16[384,256]{1,0:T(8,128)(2,1)}, bf16[384,256]{1,0:T(8,128)(2,1)S(1)}, u32[]{:S(2)}, u32[]{:S(2)}) collective-permute-start(bf16[384,256]{1,0:T(8,128)(2,1)} %param.17), channel_id=1, source_target_pairs={{0,4},{2,6},{4,0},{6,2},{1,5},{3,7},{5,1},{7,3},{8,12},{10,14},{12... | collective-permute-start | bytes 589832 | tf_op jit(solution)/shard_map/ppermute | solution.py:442
  8.8 3.7 %collective-permute-done.1.h2 = bf16[384,256]{1,0:T(8,128)(2,1)S(1)} collective-permute-done((bf16[384,256]{1,0:T(8,128)(2,1)}, bf16[384,256]{1,0:T(8,128)(2,1)S(1)}, u32[]{:S(2)}, u32[]{:S(2)}) %collective-permute-start.1) | collective-permute-done | bytes 196640 | tf_op jit(solution)/shard_map/ppermute | solution.py:441
  12.5 1.7 %collective-permute-done.2.h3 = bf16[384,256]{1,0:T(8,128)(2,1)S(1)} collective-permute-done((bf16[384,256]{1,0:T(8,128)(2,1)}, bf16[384,256]{1,0:T(8,128)(2,1)S(1)}, u32[]{:S(2)}, u32[]{:S(2)}) %collective-permute-start.2) | collective-permute-done | bytes 196640 | tf_op jit(solution)/shard_map/ppermute | solution.py:442
  15.9 1.8 %project.1 = (bf16[384,2048]{1,0:T(8,128)(2,1)S(1)}, bf16[384,128]{1,0:T(8,128)(2,1)S(1)}, bf16[384,256]{1,0:T(8,128)(2,1)S(1)}) custom-call(bf16[384,256]{1,0:T(8,128)(2,1)S(1)} %pad_maximum_fusion.own, bf16[384,256]{1,0:T(8,128)(2,1)S(1)} %collective-permute-done.h1, bf16[384,256]{1,0:T(8,128)(2,1)S(1)} %collective-permute-done.1.h2, ...), custom_call_target="tpu_custom_call" | custom-call | flops 1409286144 | bytes 1409286 | tf_op jit(solution)/shard_map/project/pallas_call | solution.py:30
  17.8 2.0 %collective-permute-start.8 = (bf16[384,256]{1,0:T(8,128)(2,1)S(1)}, bf16[384,256]{1,0:T(8,128)(2,1)S(1)}, u32[]{:S(2)}, u32[]{:S(2)}) collective-permute-start(bf16[384,256]{1,0:T(8,128)(2,1)S(1)} %get-tuple-element.61.refs_2_), channel_id=1, source_target_pairs={{0,224},{32,0},{64,32},{96,64},{128,96},{160,128},{192,160},{224,1... | collective-permute-start | bytes 589832 | tf_op jit(solution)/shard_map/ppermute | solution.py:456
  19.9 3.8 %chunks.1 = (f32[12,64,128]{2,1,0:T(8,128)S(1)}, f32[12,64,128]{2,1,0:T(8,128)S(1)}, f32[12,64,128]{2,1,0:T(8,128)S(1)}, f32[6,64,128]{2,1,0:T(8,128)S(1)}, f32[...) custom-call(bf16[384,2048]{1,0:T(8,128)(2,1)S(1)} %get-tuple-element.62.normed, ...), custom_call_target="tpu_custom_call" | custom-call | flops 6000000000 | bytes 6000000 | tf_op jit(solution)/shard_map/chunks/pallas_call | solution.py:30
  26.9 2.8 %collective-permute-start.9 = (bf16[384,256]{1,0:T(8,128)(2,1)S(1)}, bf16[384,256]{1,0:T(8,128)(2,1)S(1)}, u32[]{:S(2)}, u32[]{:S(2)}) collective-permute-start(bf16[384,256]{1,0:T(8,128)(2,1)S(1)} %collective-permute-done.7.refs_3_), channel_id=1, source_target_pairs={{0,32},{32,64},{64,96},{96,128},{128,160},{160,192},{192,224},{224... | collective-permute-start | bytes 589832 | tf_op jit(solution)/shard_map/ppermute | solution.py:473
  29.7 3.8 %recurrent.1 = (f32[384,128]{1,0:T(8,128)S(1)}, f32[384,128]{1,0:T(8,128)S(1)}, bf16[512,128]{1,0:T(8,128)(2,1)S(1)}) custom-call(f32[12,64,128]{2,1,0:T(8,128)S(1)} %get-tuple-element.73.lower_ref, f32[12,64,128]{2,1,0:T(8,128)S(1)} %get-tuple-element.74.reading_ref, f32[12,64,128]{2,1,0:T(8,128)S(1)} %get-tuple-element.75.rhs_ref, ...), custom_call_target="tpu_custom_call" | custom-call | flops 6000000000 | bytes 6000000 | tf_op jit(solution)/shard_map/recurrent/pallas_call | solution.py:30
  34.1 3.0 %collective-permute-start.11 = (bf16[384,256]{1,0:T(8,128)(2,1)S(1)}, bf16[384,256]{1,0:T(8,128)(2,1)S(1)}, u32[]{:S(2)}, u32[]{:S(2)}) collective-permute-start(bf16[384,256]{1,0:T(8,128)(2,1)S(1)} %collective-permute-done.9.refs_5_), channel_id=1, source_target_pairs={{0,32},{32,64},{64,96},{96,128},{128,160},{160,192},{192,224},{224... | collective-permute-start | bytes 589832 | tf_op jit(solution)/shard_map/ppermute | solution.py:484
  38.6 1.7 %collective-permute-start.14 = (bf16[512,128]{1,0:T(8,128)(2,1)S(1)}, bf16[512,128]{1,0:T(8,128)(2,1)S(1)}, u32[]{:S(2)}, u32[]{:S(2)}) collective-permute-start(bf16[512,128]{1,0:T(8,128)(2,1)S(1)} %get-tuple-element.85.m0.refs_0_), channel_id=1, source_target_pairs={{0,24},{8,0},{16,8},{24,16},{1,25},{9,1},{17,9},{25,17},{2,26},{10... | collective-permute-start | bytes 393224 | tf_op jit(solution)/shard_map/ppermute | solution.py:489
  40.3 1.8 %collective-permute-start.15 = (bf16[512,128]{1,0:T(8,128)(2,1)S(1)}, bf16[512,128]{1,0:T(8,128)(2,1)S(1)}, u32[]{:S(2)}, u32[]{:S(2)}) collective-permute-start(bf16[512,128]{1,0:T(8,128)(2,1)S(1)} %get-tuple-element.85.m0.refs_0_), channel_id=1, source_target_pairs={{0,16},{8,24},{16,0},{24,8},{1,17},{9,25},{17,1},{25,9},{2,18},{10... | collective-permute-start | bytes 393224 | tf_op jit(solution)/shard_map/ppermute | solution.py:490
  42.1 2.5 %collective-permute-done.13.m1.refs_1_ = bf16[512,128]{1,0:T(8,128)(2,1)S(1)} collective-permute-done((bf16[512,128]{1,0:T(8,128)(2,1)S(1)}, bf16[512,128]{1,0:T(8,128)(2,1)S(1)}, u32[]{:S(2)}, u32[]{:S(2)}) %collective-permute-start.13) | collective-permute-done | bytes 131104 | tf_op jit(solution)/shard_map/ppermute | solution.py:488
  44.7 2.1 %collective-permute-done.15.refs_1_.m3 = bf16[512,128]{1,0:T(8,128)(2,1)S(1)} collective-permute-done((bf16[512,128]{1,0:T(8,128)(2,1)S(1)}, bf16[512,128]{1,0:T(8,128)(2,1)S(1)}, u32[]{:S(2)}, u32[]{:S(2)}) %collective-permute-start.15) | collective-permute-done | bytes 131104 | tf_op jit(solution)/shard_map/ppermute | solution.py:490
  46.8 3.2 %collective-permute-start.16 = (bf16[384,256]{1,0:T(8,128)(2,1)S(1)}, bf16[384,256]{1,0:T(8,128)(2,1)S(1)}, u32[]{:S(2)}, u32[]{:S(2)}) collective-permute-start(bf16[384,256]{1,0:T(8,128)(2,1)S(1)} %collective-permute-done.11.refs_7_), channel_id=1, source_target_pairs={{0,32},{32,64},{64,96},{96,128},{128,160},{160,192},{192,224},{224... | collective-permute-start | bytes 589832 | tf_op jit(solution)/shard_map/ppermute | solution.py:493
  50.6 1.8 %collective-permute-start.18 = (bf16[128,128]{1,0:T(8,128)(2,1)S(1)}, bf16[128,128]{1,0:T(8,128)(2,1)S(1)}, u32[]{:S(2)}, u32[]{:S(2)}) collective-permute-start(bf16[128,128]{1,0:T(8,128)(2,1)S(1)} %get-tuple-element.96.line_ref), channel_id=1, source_target_pairs={{0,64},{32,96},{64,128},{96,160},{128,192},{160,224},{192,0},{224,... | collective-permute-start | bytes 98312 | tf_op jit(solution)/shard_map/ppermute | solution.py:499
  52.4 2.7 %collective-permute-start.19 = (bf16[128,128]{1,0:T(8,128)(2,1)S(1)}, bf16[128,128]{1,0:T(8,128)(2,1)S(1)}, u32[]{:S(2)}, u32[]{:S(2)}) collective-permute-start(bf16[128,128]{1,0:T(8,128)(2,1)S(1)} %get-tuple-element.96.line_ref), channel_id=1, source_target_pairs={{0,96},{32,128},{64,160},{96,192},{128,224},{160,0},{192,32},{224,... | collective-permute-start | bytes 98312 | tf_op jit(solution)/shard_map/ppermute | solution.py:499
  55.1 7.9 %attention1.1 = (bf16[2,144,384]{2,1,0:T(8,128)(2,1)S(1)}, bf16[2,144,384]{2,1,0:T(8,128)(2,1)S(1)}, bf16[8,384,128]{2,1,0:T(8,128)(2,1)S(1)}, bf16[8,144,384]{2,1,0:T(8,128)(2,1)S(1)}) custom-call(bf16[512,128]{1,0:T(8,128)(2,1)S(1)} %collective-permute-done.14.refs_0_.m2, bf16[512,128]{1,0:T(8,128)(2,1)S(1)} %collective-permute-done.15.refs_1_.m3, ...), custom_call_target="tpu_custom_call" | custom-call | flops 8000000000 | bytes 8000000 | tf_op jit(solution)/shard_map/attention1/pallas_call | solution.py:30
  63.4 7.3 %attention0.1 = (bf16[2,144,384]{2,1,0:T(8,128)(2,1)S(1)}, bf16[2,144,384]{2,1,0:T(8,128)(2,1)S(1)}) custom-call(bf16[512,128]{1,0:T(8,128)(2,1)S(1)} %get-tuple-element.85.m0.refs_0_, bf16[512,128]{1,0:T(8,128)(2,1)S(1)} %collective-permute-done.13.m1.refs_1_, bf16[8,384,128]{2,1,0:T(8,128)(2,1)S(1)} %get-tuple-element.102.refs_2_, ...), custom_call_target="tpu_custom_call" | custom-call | flops 8000000000 | bytes 8000000 | tf_op jit(solution)/shard_map/attention0/pallas_call | solution.py:30
  72.8 1.8 %collective-permute-start.22 = (bf16[2,144,384]{2,1,0:T(8,128)(2,1)S(1)}, bf16[2,144,384]{2,1,0:T(8,128)(2,1)S(1)}, u32[]{:S(2)}, u32[]{:S(2)}) collective-permute-start(bf16[2,144,384]{2,1,0:T(8,128)(2,1)S(1)} %get-tuple-element.107), channel_id=1, source_target_pairs={{0,16},{8,24},{16,0},{24,8},{1,17},{9,25},{17,1},{25,9},{2,18},{10... | collective-permute-start | bytes 663560 | tf_op jit(solution)/shard_map/ppermute | solution.py:525
  75.3 7.2 %collective-permute-done.23.window_ref = bf16[128,128]{1,0:T(8,128)(2,1)S(1)} collective-permute-done((bf16[128,128]{1,0:T(8,128)(2,1)S(1)}, bf16[128,128]{1,0:T(8,128)(2,1)S(1)}, u32[]{:S(2)}, u32[]{:S(2)}) %collective-permute-start.23) | collective-permute-done | bytes 32800 | tf_op jit(solution)/shard_map/ppermute | solution.py:532
  82.5 2.1 %finish.1 = (bf16[4,48,2048]{2,1,0:T(8,128)(2,1)S(1)}, bf16[4,48,2048]{2,1,0:T(8,128)(2,1)S(1)}, f32[2,384]{1,0:T(2,128)}) custom-call(f32[1,1]{1,0:T(1,128)} %bitcast.7.lambda_ref, bf16[2,144,384]{2,1,0:T(8,128)(2,1)S(1)} %get-tuple-element.104.p0, bf16[2,144,384]{2,1,0:T(8,128)(2,1)S(1)} %collective-permute-done.20.p1, ...), custom_call_target="tpu_custom_call" | custom-call | flops 1000000000 | bytes 1000000 | tf_op jit(solution)/shard_map/finish/pallas_call | solution.py:30
  84.6 2.3 %collective-permute-done.24.other_ref = bf16[4,48,2048]{2,1,0:T(8,128)(2,1)S(1)} collective-permute-done((bf16[4,48,2048]{2,1,0:T(8,128)(2,1)S(1)}, bf16[4,48,2048]{2,1,0:T(8,128)(2,1)S(1)}, u32[]{:S(2)}, u32[]{:S(2)}) %collective-permute-start.24) | collective-permute-done | bytes 786464 | tf_op jit(solution)/shard_map/ppermute | solution.py:543
  88.2 2.1 %collective-permute-start.26 = (bf16[48,2048]{1,0:T(8,128)(2,1)S(1)}, bf16[48,2048]{1,0:T(8,128)(2,1)S(1)}, u32[]{:S(2)}, u32[]{:S(2)}) collective-permute-start(bf16[48,2048]{1,0:T(8,128)(2,1)S(1)} %get-tuple-element.117), channel_id=1, source_target_pairs={{0,6},{2,0},{4,2},{6,4},{1,7},{3,1},{5,3},{7,5},{8,14},{10,8},{12,... | collective-permute-start | bytes 589832 | tf_op jit(solution)/shard_map/ppermute | solution.py:557
  90.4 9.1 %collective-permute-done.25.p1 = bf16[48,2048]{1,0:T(8,128)(2,1)S(1)} collective-permute-done((bf16[48,2048]{1,0:T(8,128)(2,1)S(1)}, bf16[48,2048]{1,0:T(8,128)(2,1)S(1)}, u32[]{:S(2)}, u32[]{:S(2)}) %collective-permute-start.25) | collective-permute-done | bytes 196640 | tf_op jit(solution)/shard_map/ppermute | solution.py:556
  (68 shorter events, 18.6 us)
Async XLA Ops:
  0.6 8.2 %collective-permute-start = (bf16[384,256]{1,0:T(8,128)(2,1)}, bf16[384,256]{1,0:T(8,128)(2,1)S(1)}, u32[]{:S(2)}, u32[]{:S(2)}) collective-permute-start(bf16[384,256]{1,0:T(8,128)(2,1)} %param.17), channel_id=1, source_target_pairs={{0,2},{2,4},{4,6},{6,0},{1,3},{3,5},{5,7},{7,1},{8,10},{10,12},{12... | collective-permute-start | bytes 589832 | tf_op jit(solution)/shard_map/ppermute | solution.py:440
  2.3 10.2 %collective-permute-start.1 = (bf16[384,256]{1,0:T(8,128)(2,1)}, bf16[384,256]{1,0:T(8,128)(2,1)S(1)}, u32[]{:S(2)}, u32[]{:S(2)}) collective-permute-start(bf16[384,256]{1,0:T(8,128)(2,1)} %param.17), channel_id=1, source_target_pairs={{0,6},{2,0},{4,2},{6,4},{1,7},{3,1},{5,3},{7,5},{8,14},{10,8},{12,... | collective-permute-start | bytes 589832 | tf_op jit(solution)/shard_map/ppermute | solution.py:441
  3.9 10.3 %collective-permute-start.2 = (bf16[384,256]{1,0:T(8,128)(2,1)}, bf16[384,256]{1,0:T(8,128)(2,1)S(1)}, u32[]{:S(2)}, u32[]{:S(2)}) collective-permute-start(bf16[384,256]{1,0:T(8,128)(2,1)} %param.17), channel_id=1, source_target_pairs={{0,4},{2,6},{4,0},{6,2},{1,5},{3,7},{5,1},{7,3},{8,12},{10,14},{12... | collective-permute-start | bytes 589832 | tf_op jit(solution)/shard_map/ppermute | solution.py:442
  5.9 10.0 %collective-permute-start.3 = (bf16[384,256]{1,0:T(8,128)(2,1)}, bf16[384,256]{1,0:T(8,128)(2,1)S(1)}, u32[]{:S(2)}, u32[]{:S(2)}) collective-permute-start(bf16[384,256]{1,0:T(8,128)(2,1)} %param.17), channel_id=1, source_target_pairs={{0,1},{1,0},{2,3},{3,2},{4,5},{5,4},{6,7},{7,6},{8,9},{9,8},{10,11... | collective-permute-start | bytes 589832 | tf_op jit(solution)/shard_map/ppermute | solution.py:443
  8.8 7.1 %collective-permute-start.4 = (bf16[384,256]{1,0:T(8,128)(2,1)S(1)}, bf16[384,256]{1,0:T(8,128)(2,1)S(1)}, u32[]{:S(2)}, u32[]{:S(2)}) collective-permute-start(bf16[384,256]{1,0:T(8,128)(2,1)S(1)} %collective-permute-done.h1), channel_id=1, source_target_pairs={{0,1},{1,0},{2,3},{3,2},{4,5},{5,4},{6,7},{7,6},{8,9},{9,8},{10,11... | collective-permute-start | bytes 589832 | tf_op jit(solution)/shard_map/ppermute | solution.py:443
  17.7 7.4 %collective-permute-start.7 = (bf16[384,256]{1,0:T(8,128)(2,1)S(1)}, bf16[384,256]{1,0:T(8,128)(2,1)S(1)}, u32[]{:S(2)}, u32[]{:S(2)}) collective-permute-start(bf16[384,256]{1,0:T(8,128)(2,1)S(1)} %get-tuple-element.61.refs_2_), channel_id=1, source_target_pairs={{0,32},{32,64},{64,96},{96,128},{128,160},{160,192},{192,224},{224... | collective-permute-start | bytes 589832 | tf_op jit(solution)/shard_map/ppermute | solution.py:455
  17.8 8.6 %collective-permute-start.8 = (bf16[384,256]{1,0:T(8,128)(2,1)S(1)}, bf16[384,256]{1,0:T(8,128)(2,1)S(1)}, u32[]{:S(2)}, u32[]{:S(2)}) collective-permute-start(bf16[384,256]{1,0:T(8,128)(2,1)S(1)} %get-tuple-element.61.refs_2_), channel_id=1, source_target_pairs={{0,224},{32,0},{64,32},{96,64},{128,96},{160,128},{192,160},{224,1... | collective-permute-start | bytes 589832 | tf_op jit(solution)/shard_map/ppermute | solution.py:456
  26.4 7.7 %collective-permute-start.10 = (bf16[384,256]{1,0:T(8,128)(2,1)S(1)}, bf16[384,256]{1,0:T(8,128)(2,1)S(1)}, u32[]{:S(2)}, u32[]{:S(2)}) collective-permute-start(bf16[384,256]{1,0:T(8,128)(2,1)S(1)} %collective-permute-done.8.refs_4_), channel_id=1, source_target_pairs={{0,224},{32,0},{64,32},{96,64},{128,96},{160,128},{192,160},{224,1... | collective-permute-start | bytes 589832 | tf_op jit(solution)/shard_map/ppermute | solution.py:474
  26.9 7.2 %collective-permute-start.9 = (bf16[384,256]{1,0:T(8,128)(2,1)S(1)}, bf16[384,256]{1,0:T(8,128)(2,1)S(1)}, u32[]{:S(2)}, u32[]{:S(2)}) collective-permute-start(bf16[384,256]{1,0:T(8,128)(2,1)S(1)} %collective-permute-done.7.refs_3_), channel_id=1, source_target_pairs={{0,32},{32,64},{64,96},{96,128},{128,160},{160,192},{192,224},{224... | collective-permute-start | bytes 589832 | tf_op jit(solution)/shard_map/ppermute | solution.py:473
  34.1 12.7 %collective-permute-start.11 = (bf16[384,256]{1,0:T(8,128)(2,1)S(1)}, bf16[384,256]{1,0:T(8,128)(2,1)S(1)}, u32[]{:S(2)}, u32[]{:S(2)}) collective-permute-start(bf16[384,256]{1,0:T(8,128)(2,1)S(1)} %collective-permute-done.9.refs_5_), channel_id=1, source_target_pairs={{0,32},{32,64},{64,96},{96,128},{128,160},{160,192},{192,224},{224... | collective-permute-start | bytes 589832 | tf_op jit(solution)/shard_map/ppermute | solution.py:484
  37.1 9.7 %collective-permute-start.12 = (bf16[384,256]{1,0:T(8,128)(2,1)S(1)}, bf16[384,256]{1,0:T(8,128)(2,1)S(1)}, u32[]{:S(2)}, u32[]{:S(2)}) collective-permute-start(bf16[384,256]{1,0:T(8,128)(2,1)S(1)} %collective-permute-done.10.refs_6_), channel_id=1, source_target_pairs={{0,224},{32,0},{64,32},{96,64},{128,96},{160,128},{192,160},{224,1... | collective-permute-start | bytes 589832 | tf_op jit(solution)/shard_map/ppermute | solution.py:485
  37.1 7.6 %collective-permute-start.13 = (bf16[512,128]{1,0:T(8,128)(2,1)S(1)}, bf16[512,128]{1,0:T(8,128)(2,1)S(1)}, u32[]{:S(2)}, u32[]{:S(2)}) collective-permute-start(bf16[512,128]{1,0:T(8,128)(2,1)S(1)} %get-tuple-element.85.m0.refs_0_), channel_id=1, source_target_pairs={{0,8},{8,16},{16,24},{24,0},{1,9},{9,17},{17,25},{25,1},{2,10},{10... | collective-permute-start | bytes 393224 | tf_op jit(solution)/shard_map/ppermute | solution.py:488
  40.3 6.5 %collective-permute-start.15 = (bf16[512,128]{1,0:T(8,128)(2,1)S(1)}, bf16[512,128]{1,0:T(8,128)(2,1)S(1)}, u32[]{:S(2)}, u32[]{:S(2)}) collective-permute-start(bf16[512,128]{1,0:T(8,128)(2,1)S(1)} %get-tuple-element.85.m0.refs_0_), channel_id=1, source_target_pairs={{0,16},{8,24},{16,0},{24,8},{1,17},{9,25},{17,1},{25,9},{2,18},{10... | collective-permute-start | bytes 393224 | tf_op jit(solution)/shard_map/ppermute | solution.py:490
  46.8 8.3 %collective-permute-start.16 = (bf16[384,256]{1,0:T(8,128)(2,1)S(1)}, bf16[384,256]{1,0:T(8,128)(2,1)S(1)}, u32[]{:S(2)}, u32[]{:S(2)}) collective-permute-start(bf16[384,256]{1,0:T(8,128)(2,1)S(1)} %collective-permute-done.11.refs_7_), channel_id=1, source_target_pairs={{0,32},{32,64},{64,96},{96,128},{128,160},{160,192},{192,224},{224... | collective-permute-start | bytes 589832 | tf_op jit(solution)/shard_map/ppermute | solution.py:493
  50.5 12.4 %collective-permute-start.17 = (bf16[128,128]{1,0:T(8,128)(2,1)S(1)}, bf16[128,128]{1,0:T(8,128)(2,1)S(1)}, u32[]{:S(2)}, u32[]{:S(2)}) collective-permute-start(bf16[128,128]{1,0:T(8,128)(2,1)S(1)} %get-tuple-element.96.line_ref), channel_id=1, source_target_pairs={{0,32},{32,64},{64,96},{96,128},{128,160},{160,192},{192,224},{224... | collective-permute-start | bytes 98312 | tf_op jit(solution)/shard_map/ppermute | solution.py:499
  50.6 12.4 %collective-permute-start.18 = (bf16[128,128]{1,0:T(8,128)(2,1)S(1)}, bf16[128,128]{1,0:T(8,128)(2,1)S(1)}, u32[]{:S(2)}, u32[]{:S(2)}) collective-permute-start(bf16[128,128]{1,0:T(8,128)(2,1)S(1)} %get-tuple-element.96.line_ref), channel_id=1, source_target_pairs={{0,64},{32,96},{64,128},{96,160},{128,192},{160,224},{192,0},{224,... | collective-permute-start | bytes 98312 | tf_op jit(solution)/shard_map/ppermute | solution.py:499
  52.4 10.6 %collective-permute-start.19 = (bf16[128,128]{1,0:T(8,128)(2,1)S(1)}, bf16[128,128]{1,0:T(8,128)(2,1)S(1)}, u32[]{:S(2)}, u32[]{:S(2)}) collective-permute-start(bf16[128,128]{1,0:T(8,128)(2,1)S(1)} %get-tuple-element.96.line_ref), channel_id=1, source_target_pairs={{0,96},{32,128},{64,160},{96,192},{128,224},{160,0},{192,32},{224,... | collective-permute-start | bytes 98312 | tf_op jit(solution)/shard_map/ppermute | solution.py:499
  70.7 11.7 %collective-permute-start.21 = (bf16[2,144,384]{2,1,0:T(8,128)(2,1)S(1)}, bf16[2,144,384]{2,1,0:T(8,128)(2,1)S(1)}, u32[]{:S(2)}, u32[]{:S(2)}) collective-permute-start(bf16[2,144,384]{2,1,0:T(8,128)(2,1)S(1)} %get-tuple-element.106), channel_id=1, source_target_pairs={{0,24},{8,0},{16,8},{24,16},{1,25},{9,1},{17,9},{25,17},{2,26},{10... | collective-permute-start | bytes 663560 | tf_op jit(solution)/shard_map/ppermute | solution.py:534
  72.3 10.1 %collective-permute-start.20 = (bf16[2,144,384]{2,1,0:T(8,128)(2,1)S(1)}, bf16[2,144,384]{2,1,0:T(8,128)(2,1)S(1)}, u32[]{:S(2)}, u32[]{:S(2)}) collective-permute-start(bf16[2,144,384]{2,1,0:T(8,128)(2,1)S(1)} %get-tuple-element.105), channel_id=1, source_target_pairs={{0,8},{8,16},{16,24},{24,0},{1,9},{9,17},{17,25},{25,1},{2,10},{10... | collective-permute-start | bytes 663560 | tf_op jit(solution)/shard_map/ppermute | solution.py:524
  72.8 9.6 %collective-permute-start.22 = (bf16[2,144,384]{2,1,0:T(8,128)(2,1)S(1)}, bf16[2,144,384]{2,1,0:T(8,128)(2,1)S(1)}, u32[]{:S(2)}, u32[]{:S(2)}) collective-permute-start(bf16[2,144,384]{2,1,0:T(8,128)(2,1)S(1)} %get-tuple-element.107), channel_id=1, source_target_pairs={{0,16},{8,24},{16,0},{24,8},{1,17},{9,25},{17,1},{25,9},{2,18},{10... | collective-permute-start | bytes 663560 | tf_op jit(solution)/shard_map/ppermute | solution.py:525
  74.6 7.8 %collective-permute-start.23 = (bf16[128,128]{1,0:T(8,128)(2,1)S(1)}, bf16[128,128]{1,0:T(8,128)(2,1)S(1)}, u32[]{:S(2)}, u32[]{:S(2)}) collective-permute-start(bf16[128,128]{1,0:T(8,128)(2,1)S(1)} %get-tuple-element.110), channel_id=1, source_target_pairs={{0,128},{32,160},{64,192},{96,224},{128,0},{160,32},{192,64},{224,... | collective-permute-start | bytes 98312 | tf_op jit(solution)/shard_map/ppermute | solution.py:532
  87.1 12.4 %collective-permute-start.25 = (bf16[48,2048]{1,0:T(8,128)(2,1)S(1)}, bf16[48,2048]{1,0:T(8,128)(2,1)S(1)}, u32[]{:S(2)}, u32[]{:S(2)}) collective-permute-start(bf16[48,2048]{1,0:T(8,128)(2,1)S(1)} %get-tuple-element.116), channel_id=1, source_target_pairs={{0,2},{2,4},{4,6},{6,0},{1,3},{3,5},{5,7},{7,1},{8,10},{10,12},{12... | collective-permute-start | bytes 589832 | tf_op jit(solution)/shard_map/ppermute | solution.py:556
  88.2 11.3 %collective-permute-start.26 = (bf16[48,2048]{1,0:T(8,128)(2,1)S(1)}, bf16[48,2048]{1,0:T(8,128)(2,1)S(1)}, u32[]{:S(2)}, u32[]{:S(2)}) collective-permute-start(bf16[48,2048]{1,0:T(8,128)(2,1)S(1)} %get-tuple-element.117), channel_id=1, source_target_pairs={{0,6},{2,0},{4,2},{6,4},{1,7},{3,1},{5,3},{7,5},{8,14},{10,8},{12,... | collective-permute-start | bytes 589832 | tf_op jit(solution)/shard_map/ppermute | solution.py:557
  90.4 9.1 %collective-permute-start.27 = (bf16[48,2048]{1,0:T(8,128)(2,1)S(1)}, bf16[48,2048]{1,0:T(8,128)(2,1)S(1)}, u32[]{:S(2)}, u32[]{:S(2)}) collective-permute-start(bf16[48,2048]{1,0:T(8,128)(2,1)S(1)} %get-tuple-element.118), channel_id=1, source_target_pairs={{0,4},{2,6},{4,0},{6,2},{1,5},{3,7},{5,1},{7,3},{8,12},{10,14},{12... | collective-permute-start | bytes 589832 | tf_op jit(solution)/shard_map/ppermute | solution.py:558
  (15 other events, 98.7 us)

commit v3 on v2

--- a/solution.py
+++ b/solution.py
@@ -8,6 +8,7 @@
 from jax.experimental.pallas import tpu as pltpu
 from jax.sharding import Mesh
 from jax.sharding import PartitionSpec as P
+
 
 HD = 64
 F32 = jnp.float32
@@ -26,7 +27,7 @@
 NN = (((1,), (0,)), ((), ()))
 
 
-def call(kernel, outs, scalars, arrays, scratch=(), flops=0, grant=GRANT, name=None):
+def call(kernel, outs, scalars, arrays, scratch=(), flops=0, grant=GRANT):
     return pl.pallas_call(
         kernel,
         out_shape=outs,
@@ -36,7 +37,6 @@
         scratch_shapes=list(scratch),
         compiler_params=pltpu.CompilerParams(vmem_limit_bytes=grant * MIB),
         cost_estimate=pl.CostEstimate(flops=flops, bytes_accessed=flops // 1000, transcendentals=0),
-        name=name,
     )(*scalars, *arrays)
 
 
@@ -449,7 +449,6 @@
         (),
         (turned_in, *mine, *theirs, in_gain.reshape(8, 256), pair_weights),
         flops=2 * rows * 2048 * 896,
-        name="project",
     )
 
     right = permute(kv, "z", ring(8, 1))
@@ -467,7 +466,6 @@
             decay_base.reshape(1, 128), decay_shift, learn_rate.reshape(1, 128),
         ),
         flops=6 * 10**9,
-        name="chunks",
     )
     right1, left1, chunked, q = together((right, left, chunked, q))
     right = permute(right1, "z", ring(8, 1))
@@ -478,23 +476,19 @@
         (),
         (*chunked, q),
         flops=6 * 10**9,
-        name="recurrent",
     )
     right2, left2, message = together((right, left, message))
     right = permute(right2, "z", ring(8, 1))
     left = permute(left2, "z", ring(8, -1))
-    messages = [
-        message,
-        permute(message, "x", ring(4, 1)),
-        permute(message, "x", ring(4, -1)),
-        permute(message, "x", ring(4, 2)),
-    ]
-    right3, left3, messages = together((right, left, messages))
+    messages = [message]
+    for shift in (1, -1, 2):
+        messages.append(permute(message, "x", ring(4, shift)))
+    right3, left3 = right, left
     right4 = permute(right3, "z", ring(8, 1))
     before, line = call(
         along_x_kernel,
         (shaped((128, 128), F32), shaped((128, 128), BF16)),
-        (), messages, scratch=(pltpu.VMEM((4, 128, 128), BF16),), flops=10**8, name="along_x",
+        (), messages, scratch=(pltpu.VMEM((4, 128, 128), BF16),), flops=10**8,
     )
     lines = [permute(line, "z", ring(8, s)) for s in (1, 2, 3)]
 
@@ -514,7 +508,6 @@
                 pltpu.SMEM((2, 16), jnp.int32),
             ],
             flops=8 * 10**9,
-            name=f"attention{pair}",
         )
 
     to_next, to_far, keys, turned = attend(
@@ -526,7 +519,7 @@
     window, near = call(
         window_kernel,
         (shaped((128, 128), BF16), shaped((128, 128), F32)),
-        (), (line, *lines), flops=10**8, name="window",
+        (), (line, *lines), flops=10**8,
     )
     window, keys = together((window, keys))
     window = permute(window, "z", ring(8, 4))
@@ -538,14 +531,13 @@
         (),
         (mix_lambda.reshape(1, 1), *back, read, local, window, near, before, out_recurrent, out_attention),
         flops=10**9,
-        name="finish",
     )
     theirs = permute(others, "c", ring(2, 1))
     piece = (rows // 8, 2048)
     own, plus1, plus2, plus3 = call(
         pair_kernel,
         (shaped(piece, F32),) + (shaped(piece, BF16),) * 3,
-        (), (ours, theirs), flops=10**8, name="pair",
+        (), (ours, theirs), flops=10**8,
     )
     layer_out = call(
         norm_kernel,
@@ -559,7 +551,6 @@
             out_gain.reshape(1, 2048),
         ),
         flops=10**8,
-        name="norm",
     )
     return (layer_out, log_sums[None])
 

time: 101 us -> 105 us (1.040)
  waiting for transfers between devices: 33.2 us -> 36.4 us
    ppermute x1, waiting for transfers between devices: 0.01 us -> 3.19 us  [per_device(): right = permute(right2, 'z', ring(8, 1))]
  transfers between devices with their start and end apart: 28 -> 28, of which waited for: 11 -> 12; matrix products, arithmetic and copies ran while one was open for 3% -> 3% of each run, Pallas kernels for 16% -> 15%
where the time goes in v3:
time: 105 us; the launch traced here: 104 us
  waiting for transfers between devices  36.4 us (35%)
  starting transfers between devices  34.1 us (32%)
  Pallas kernels  28.6 us (27%)
  local copies, waits for them, and re-layouts  1.74 us (2%)
  other arithmetic  1.58 us (2%)
  between operations  1.55 us (1%)
    pallas_call x10, Pallas kernels, call(): pl.pallas_call(kernel, out_shape=outs, in_specs=[pl.BlockSpec(memory_spac...  28.6 us
    ppermute x1, waiting for transfers between devices, per_device(): permute(plus1, 'y', ring(4, 1))  9.1 us
    ppermute x1, waiting for transfers between devices, per_device(): window = permute(window, 'z', ring(8, 4))  7.17 us
    ppermute x3, starting transfers between devices, per_device(): messages.append(permute(message, 'x', ring(4, shift)))  5.05 us
    ppermute x3, waiting for transfers between devices, per_device(): messages.append(permute(message, 'x', ring(4, shift)))  4.66 us
    ppermute x3, starting transfers between devices, per_device(): lines = [permute(line, 'z', ring(8, s)) for s in (1, 2, 3)]  4.56 us
    ppermute x1, waiting for transfers between devices, per_device(): down = permute(hidden_in, 'y', ring(4, -1))  3.7 us
    ppermute x1, starting transfers between devices, per_device(): right4 = permute(right3, 'z', ring(8, 1))  3.69 us
  transfers between devices with their start and end apart: 28, of which 12 were waited for; matrix products, arithmetic and copies ran while one was open for 3% of the time, Pallas kernels for 15%

profile of v3, /device:TPU:224, one launch (start us, length us, event | category | flops | bytes accessed | tf_op | source)
XLA Modules:
  0.0 104.0 jit_solution(10437382475719293819)
XLA Ops:
  2.3 1.7 %collective-permute-start.1 = (bf16[384,256]{1,0:T(8,128)(2,1)}, bf16[384,256]{1,0:T(8,128)(2,1)S(1)}, u32[]{:S(2)}, u32[]{:S(2)}) collective-permute-start(bf16[384,256]{1,0:T(8,128)(2,1)} %param.17), channel_id=1, source_target_pairs={{0,6},{2,0},{4,2},{6,4},{1,7},{3,1},{5,3},{7,5},{8,14},{10,8},{12,... | collective-permute-start | bytes 589832 | tf_op jit(solution)/shard_map/ppermute | solution.py:441
  3.9 2.0 %collective-permute-start.2 = (bf16[384,256]{1,0:T(8,128)(2,1)}, bf16[384,256]{1,0:T(8,128)(2,1)S(1)}, u32[]{:S(2)}, u32[]{:S(2)}) collective-permute-start(bf16[384,256]{1,0:T(8,128)(2,1)} %param.17), channel_id=1, source_target_pairs={{0,4},{2,6},{4,0},{6,2},{1,5},{3,7},{5,1},{7,3},{8,12},{10,14},{12... | collective-permute-start | bytes 589832 | tf_op jit(solution)/shard_map/ppermute | solution.py:442
  8.8 3.7 %collective-permute-done.1.h2 = bf16[384,256]{1,0:T(8,128)(2,1)S(1)} collective-permute-done((bf16[384,256]{1,0:T(8,128)(2,1)}, bf16[384,256]{1,0:T(8,128)(2,1)S(1)}, u32[]{:S(2)}, u32[]{:S(2)}) %collective-permute-start.1) | collective-permute-done | bytes 196640 | tf_op jit(solution)/shard_map/ppermute | solution.py:441
  12.5 1.7 %collective-permute-done.2.h3 = bf16[384,256]{1,0:T(8,128)(2,1)S(1)} collective-permute-done((bf16[384,256]{1,0:T(8,128)(2,1)}, bf16[384,256]{1,0:T(8,128)(2,1)S(1)}, u32[]{:S(2)}, u32[]{:S(2)}) %collective-permute-start.2) | collective-permute-done | bytes 196640 | tf_op jit(solution)/shard_map/ppermute | solution.py:442
  15.9 1.8 %shard_map.176 = (bf16[384,2048]{1,0:T(8,128)(2,1)S(1)}, bf16[384,128]{1,0:T(8,128)(2,1)S(1)}, bf16[384,256]{1,0:T(8,128)(2,1)S(1)}) custom-call(bf16[384,256]{1,0:T(8,128)(2,1)S(1)} %pad_maximum_fusion.own, bf16[384,256]{1,0:T(8,128)(2,1)S(1)} %collective-permute-done.h1, bf16[384,256]{1,0:T(8,128)(2,1)S(1)} %collective-permute-done.1.h2, ...), custom_call_target="tpu_custom_call" | custom-call | flops 1409286144 | bytes 1409286 | tf_op jit(solution)/shard_map/pallas_call | solution.py:31
  17.8 2.0 %collective-permute-start.8 = (bf16[384,256]{1,0:T(8,128)(2,1)S(1)}, bf16[384,256]{1,0:T(8,128)(2,1)S(1)}, u32[]{:S(2)}, u32[]{:S(2)}) collective-permute-start(bf16[384,256]{1,0:T(8,128)(2,1)S(1)} %get-tuple-element.55.refs_2_), channel_id=1, source_target_pairs={{0,224},{32,0},{64,32},{96,64},{128,96},{160,128},{192,160},{224,1... | collective-permute-start | bytes 589832 | tf_op jit(solution)/shard_map/ppermute | solution.py:455
  19.9 3.8 %shard_map.177 = (f32[12,64,128]{2,1,0:T(8,128)S(1)}, f32[12,64,128]{2,1,0:T(8,128)S(1)}, f32[12,64,128]{2,1,0:T(8,128)S(1)}, f32[6,64,128]{2,1,0:T(8,128)S(1)},...) custom-call(bf16[384,2048]{1,0:T(8,128)(2,1)S(1)} %get-tuple-element.56.normed, ...), custom_call_target="tpu_custom_call" | custom-call | flops 6000000000 | bytes 6000000 | tf_op jit(solution)/shard_map/pallas_call | solution.py:31
  26.9 2.8 %collective-permute-start.9 = (bf16[384,256]{1,0:T(8,128)(2,1)S(1)}, bf16[384,256]{1,0:T(8,128)(2,1)S(1)}, u32[]{:S(2)}, u32[]{:S(2)}) collective-permute-start(bf16[384,256]{1,0:T(8,128)(2,1)S(1)} %collective-permute-done.7.refs_3_), channel_id=1, source_target_pairs={{0,32},{32,64},{64,96},{96,128},{128,160},{160,192},{192,224},{224... | collective-permute-start | bytes 589832 | tf_op jit(solution)/shard_map/ppermute | solution.py:471
  29.7 3.8 %shard_map.178 = (f32[384,128]{1,0:T(8,128)S(1)}, f32[384,128]{1,0:T(8,128)S(1)}, bf16[512,128]{1,0:T(8,128)(2,1)S(1)}) custom-call(f32[12,64,128]{2,1,0:T(8,128)S(1)} %get-tuple-element.67.lower_ref, f32[12,64,128]{2,1,0:T(8,128)S(1)} %get-tuple-element.68.reading_ref, f32[12,64,128]{2,1,0:T(8,128)S(1)} %get-tuple-element.69.rhs_ref, ...), custom_call_target="tpu_custom_call" | custom-call | flops 6000000000 | bytes 6000000 | tf_op jit(solution)/shard_map/pallas_call | solution.py:31
  34.1 3.0 %collective-permute-start.14 = (bf16[384,256]{1,0:T(8,128)(2,1)S(1)}, bf16[384,256]{1,0:T(8,128)(2,1)S(1)}, u32[]{:S(2)}, u32[]{:S(2)}) collective-permute-start(bf16[384,256]{1,0:T(8,128)(2,1)S(1)} %collective-permute-done.9.refs_5_), channel_id=1, source_target_pairs={{0,32},{32,64},{64,96},{96,128},{128,160},{160,192},{192,224},{224... | collective-permute-start | bytes 589832 | tf_op jit(solution)/shard_map/ppermute | solution.py:481
  37.1 3.2 %collective-permute-done.14.refs_7_ = bf16[384,256]{1,0:T(8,128)(2,1)S(1)} collective-permute-done((bf16[384,256]{1,0:T(8,128)(2,1)S(1)}, bf16[384,256]{1,0:T(8,128)(2,1)S(1)}, u32[]{:S(2)}, u32[]{:S(2)}) %collective-permute-start.14) | collective-permute-done | bytes 196640 | tf_op jit(solution)/shard_map/ppermute | solution.py:481
  40.3 3.7 %collective-permute-start.16 = (bf16[384,256]{1,0:T(8,128)(2,1)S(1)}, bf16[384,256]{1,0:T(8,128)(2,1)S(1)}, u32[]{:S(2)}, u32[]{:S(2)}) collective-permute-start(bf16[384,256]{1,0:T(8,128)(2,1)S(1)} %collective-permute-done.14.refs_7_), channel_id=1, source_target_pairs={{0,32},{32,64},{64,96},{96,128},{128,160},{160,192},{192,224},{224... | collective-permute-start | bytes 589832 | tf_op jit(solution)/shard_map/ppermute | solution.py:487
  45.4 1.7 %collective-permute-start.12 = (bf16[512,128]{1,0:T(8,128)(2,1)S(1)}, bf16[512,128]{1,0:T(8,128)(2,1)S(1)}, u32[]{:S(2)}, u32[]{:S(2)}) collective-permute-start(bf16[512,128]{1,0:T(8,128)(2,1)S(1)} %get-tuple-element.76.m0.refs_0_), channel_id=1, source_target_pairs={{0,24},{8,0},{16,8},{24,16},{1,25},{9,1},{17,9},{25,17},{2,26},{10... | collective-permute-start | bytes 393224 | tf_op jit(solution)/shard_map/ppermute | solution.py:485
  47.2 1.8 %collective-permute-start.13 = (bf16[512,128]{1,0:T(8,128)(2,1)S(1)}, bf16[512,128]{1,0:T(8,128)(2,1)S(1)}, u32[]{:S(2)}, u32[]{:S(2)}) collective-permute-start(bf16[512,128]{1,0:T(8,128)(2,1)S(1)} %get-tuple-element.76.m0.refs_0_), channel_id=1, source_target_pairs={{0,16},{8,24},{16,0},{24,8},{1,17},{9,25},{17,1},{25,9},{2,18},{10... | collective-permute-start | bytes 393224 | tf_op jit(solution)/shard_map/ppermute | solution.py:485
  50.6 3.0 %collective-permute-done.13.refs_1_.m3 = bf16[512,128]{1,0:T(8,128)(2,1)S(1)} collective-permute-done((bf16[512,128]{1,0:T(8,128)(2,1)S(1)}, bf16[512,128]{1,0:T(8,128)(2,1)S(1)}, u32[]{:S(2)}, u32[]{:S(2)}) %collective-permute-start.13) | collective-permute-done | bytes 131104 | tf_op jit(solution)/shard_map/ppermute | solution.py:485
  55.6 3.1 %collective-permute-start.19 = (bf16[128,128]{1,0:T(8,128)(2,1)S(1)}, bf16[128,128]{1,0:T(8,128)(2,1)S(1)}, u32[]{:S(2)}, u32[]{:S(2)}) collective-permute-start(bf16[128,128]{1,0:T(8,128)(2,1)S(1)} %get-tuple-element.84.line_ref), channel_id=1, source_target_pairs={{0,96},{32,128},{64,160},{96,192},{128,224},{160,0},{192,32},{224,... | collective-permute-start | bytes 98312 | tf_op jit(solution)/shard_map/ppermute | solution.py:493
  58.7 7.9 %shard_map.179 = (bf16[2,144,384]{2,1,0:T(8,128)(2,1)S(1)}, bf16[2,144,384]{2,1,0:T(8,128)(2,1)S(1)}, bf16[8,384,128]{2,1,0:T(8,128)(2,1)S(1)}, bf16[8,144,384]{2,1,0:T(8,128)(2,1)S(1)}) custom-call(bf16[512,128]{1,0:T(8,128)(2,1)S(1)} %collective-permute-done.12.refs_0_.m2, bf16[512,128]{1,0:T(8,128)(2,1)S(1)} %collective-permute-done.13.refs_1_.m3, ...), custom_call_target="tpu_custom_call" | custom-call | flops 8000000000 | bytes 8000000 | tf_op jit(solution)/shard_map/pallas_call | solution.py:31
  67.1 7.3 %shard_map.182 = (bf16[2,144,384]{2,1,0:T(8,128)(2,1)S(1)}, bf16[2,144,384]{2,1,0:T(8,128)(2,1)S(1)}) custom-call(bf16[512,128]{1,0:T(8,128)(2,1)S(1)} %get-tuple-element.76.m0.refs_0_, bf16[512,128]{1,0:T(8,128)(2,1)S(1)} %collective-permute-done.11.m1.refs_1_, bf16[8,384,128]{2,1,0:T(8,128)(2,1)S(1)} %get-tuple-element.90.refs_2_, ...), custom_call_target="tpu_custom_call" | custom-call | flops 8000000000 | bytes 8000000 | tf_op jit(solution)/shard_map/pallas_call | solution.py:31
  76.5 1.8 %collective-permute-start.22 = (bf16[2,144,384]{2,1,0:T(8,128)(2,1)S(1)}, bf16[2,144,384]{2,1,0:T(8,128)(2,1)S(1)}, u32[]{:S(2)}, u32[]{:S(2)}) collective-permute-start(bf16[2,144,384]{2,1,0:T(8,128)(2,1)S(1)} %get-tuple-element.95), channel_id=1, source_target_pairs={{0,16},{8,24},{16,0},{24,8},{1,17},{9,25},{17,1},{25,9},{2,18},{10... | collective-permute-start | bytes 663560 | tf_op jit(solution)/shard_map/ppermute | solution.py:518
  78.9 7.2 %collective-permute-done.23.window_ref = bf16[128,128]{1,0:T(8,128)(2,1)S(1)} collective-permute-done((bf16[128,128]{1,0:T(8,128)(2,1)S(1)}, bf16[128,128]{1,0:T(8,128)(2,1)S(1)}, u32[]{:S(2)}, u32[]{:S(2)}) %collective-permute-start.23) | collective-permute-done | bytes 32800 | tf_op jit(solution)/shard_map/ppermute | solution.py:525
  86.1 2.1 %shard_map.183 = (bf16[4,48,2048]{2,1,0:T(8,128)(2,1)S(1)}, bf16[4,48,2048]{2,1,0:T(8,128)(2,1)S(1)}, f32[2,384]{1,0:T(2,128)}) custom-call(f32[1,1]{1,0:T(1,128)} %bitcast.7.lambda_ref, bf16[2,144,384]{2,1,0:T(8,128)(2,1)S(1)} %get-tuple-element.92.p0, bf16[2,144,384]{2,1,0:T(8,128)(2,1)S(1)} %collective-permute-done.20.p1, ...), custom_call_target="tpu_custom_call" | custom-call | flops 1000000000 | bytes 1000000 | tf_op jit(solution)/shard_map/pallas_call | solution.py:31
  88.2 2.3 %collective-permute-done.24.other_ref = bf16[4,48,2048]{2,1,0:T(8,128)(2,1)S(1)} collective-permute-done((bf16[4,48,2048]{2,1,0:T(8,128)(2,1)S(1)}, bf16[4,48,2048]{2,1,0:T(8,128)(2,1)S(1)}, u32[]{:S(2)}, u32[]{:S(2)}) %collective-permute-start.24) | collective-permute-done | bytes 786464 | tf_op jit(solution)/shard_map/ppermute | solution.py:535
  91.9 2.1 %collective-permute-start.26 = (bf16[48,2048]{1,0:T(8,128)(2,1)S(1)}, bf16[48,2048]{1,0:T(8,128)(2,1)S(1)}, u32[]{:S(2)}, u32[]{:S(2)}) collective-permute-start(bf16[48,2048]{1,0:T(8,128)(2,1)S(1)} %get-tuple-element.105), channel_id=1, source_target_pairs={{0,6},{2,0},{4,2},{6,4},{1,7},{3,1},{5,3},{7,5},{8,14},{10,8},{12,... | collective-permute-start | bytes 589832 | tf_op jit(solution)/shard_map/ppermute | solution.py:549
  94.0 9.1 %collective-permute-done.25.p1 = bf16[48,2048]{1,0:T(8,128)(2,1)S(1)} collective-permute-done((bf16[48,2048]{1,0:T(8,128)(2,1)S(1)}, bf16[48,2048]{1,0:T(8,128)(2,1)S(1)}, u32[]{:S(2)}, u32[]{:S(2)}) %collective-permute-start.25) | collective-permute-done | bytes 196640 | tf_op jit(solution)/shard_map/ppermute | solution.py:548
  (68 shorter events, 19.9 us)
Async XLA Ops:
  0.6 8.2 %collective-permute-start = (bf16[384,256]{1,0:T(8,128)(2,1)}, bf16[384,256]{1,0:T(8,128)(2,1)S(1)}, u32[]{:S(2)}, u32[]{:S(2)}) collective-permute-start(bf16[384,256]{1,0:T(8,128)(2,1)} %param.17), channel_id=1, source_target_pairs={{0,2},{2,4},{4,6},{6,0},{1,3},{3,5},{5,7},{7,1},{8,10},{10,12},{12... | collective-permute-start | bytes 589832 | tf_op jit(solution)/shard_map/ppermute | solution.py:440
  2.3 10.2 %collective-permute-start.1 = (bf16[384,256]{1,0:T(8,128)(2,1)}, bf16[384,256]{1,0:T(8,128)(2,1)S(1)}, u32[]{:S(2)}, u32[]{:S(2)}) collective-permute-start(bf16[384,256]{1,0:T(8,128)(2,1)} %param.17), channel_id=1, source_target_pairs={{0,6},{2,0},{4,2},{6,4},{1,7},{3,1},{5,3},{7,5},{8,14},{10,8},{12,... | collective-permute-start | bytes 589832 | tf_op jit(solution)/shard_map/ppermute | solution.py:441
  3.9 10.3 %collective-permute-start.2 = (bf16[384,256]{1,0:T(8,128)(2,1)}, bf16[384,256]{1,0:T(8,128)(2,1)S(1)}, u32[]{:S(2)}, u32[]{:S(2)}) collective-permute-start(bf16[384,256]{1,0:T(8,128)(2,1)} %param.17), channel_id=1, source_target_pairs={{0,4},{2,6},{4,0},{6,2},{1,5},{3,7},{5,1},{7,3},{8,12},{10,14},{12... | collective-permute-start | bytes 589832 | tf_op jit(solution)/shard_map/ppermute | solution.py:442
  5.9 10.0 %collective-permute-start.3 = (bf16[384,256]{1,0:T(8,128)(2,1)}, bf16[384,256]{1,0:T(8,128)(2,1)S(1)}, u32[]{:S(2)}, u32[]{:S(2)}) collective-permute-start(bf16[384,256]{1,0:T(8,128)(2,1)} %param.17), channel_id=1, source_target_pairs={{0,1},{1,0},{2,3},{3,2},{4,5},{5,4},{6,7},{7,6},{8,9},{9,8},{10,11... | collective-permute-start | bytes 589832 | tf_op jit(solution)/shard_map/ppermute | solution.py:443
  8.8 7.1 %collective-permute-start.4 = (bf16[384,256]{1,0:T(8,128)(2,1)S(1)}, bf16[384,256]{1,0:T(8,128)(2,1)S(1)}, u32[]{:S(2)}, u32[]{:S(2)}) collective-permute-start(bf16[384,256]{1,0:T(8,128)(2,1)S(1)} %collective-permute-done.h1), channel_id=1, source_target_pairs={{0,1},{1,0},{2,3},{3,2},{4,5},{5,4},{6,7},{7,6},{8,9},{9,8},{10,11... | collective-permute-start | bytes 589832 | tf_op jit(solution)/shard_map/ppermute | solution.py:443
  17.7 7.4 %collective-permute-start.7 = (bf16[384,256]{1,0:T(8,128)(2,1)S(1)}, bf16[384,256]{1,0:T(8,128)(2,1)S(1)}, u32[]{:S(2)}, u32[]{:S(2)}) collective-permute-start(bf16[384,256]{1,0:T(8,128)(2,1)S(1)} %get-tuple-element.55.refs_2_), channel_id=1, source_target_pairs={{0,32},{32,64},{64,96},{96,128},{128,160},{160,192},{192,224},{224... | collective-permute-start | bytes 589832 | tf_op jit(solution)/shard_map/ppermute | solution.py:454
  17.8 8.6 %collective-permute-start.8 = (bf16[384,256]{1,0:T(8,128)(2,1)S(1)}, bf16[384,256]{1,0:T(8,128)(2,1)S(1)}, u32[]{:S(2)}, u32[]{:S(2)}) collective-permute-start(bf16[384,256]{1,0:T(8,128)(2,1)S(1)} %get-tuple-element.55.refs_2_), channel_id=1, source_target_pairs={{0,224},{32,0},{64,32},{96,64},{128,96},{160,128},{192,160},{224,1... | collective-permute-start | bytes 589832 | tf_op jit(solution)/shard_map/ppermute | solution.py:455
  26.4 7.7 %collective-permute-start.10 = (bf16[384,256]{1,0:T(8,128)(2,1)S(1)}, bf16[384,256]{1,0:T(8,128)(2,1)S(1)}, u32[]{:S(2)}, u32[]{:S(2)}) collective-permute-start(bf16[384,256]{1,0:T(8,128)(2,1)S(1)} %collective-permute-done.8.refs_4_), channel_id=1, source_target_pairs={{0,224},{32,0},{64,32},{96,64},{128,96},{160,128},{192,160},{224,1... | collective-permute-start | bytes 589832 | tf_op jit(solution)/shard_map/ppermute | solution.py:472
  26.9 7.2 %collective-permute-start.9 = (bf16[384,256]{1,0:T(8,128)(2,1)S(1)}, bf16[384,256]{1,0:T(8,128)(2,1)S(1)}, u32[]{:S(2)}, u32[]{:S(2)}) collective-permute-start(bf16[384,256]{1,0:T(8,128)(2,1)S(1)} %collective-permute-done.7.refs_3_), channel_id=1, source_target_pairs={{0,32},{32,64},{64,96},{96,128},{128,160},{160,192},{192,224},{224... | collective-permute-start | bytes 589832 | tf_op jit(solution)/shard_map/ppermute | solution.py:471
  34.1 6.1 %collective-permute-start.14 = (bf16[384,256]{1,0:T(8,128)(2,1)S(1)}, bf16[384,256]{1,0:T(8,128)(2,1)S(1)}, u32[]{:S(2)}, u32[]{:S(2)}) collective-permute-start(bf16[384,256]{1,0:T(8,128)(2,1)S(1)} %collective-permute-done.9.refs_5_), channel_id=1, source_target_pairs={{0,32},{32,64},{64,96},{96,128},{128,160},{160,192},{192,224},{224... | collective-permute-start | bytes 589832 | tf_op jit(solution)/shard_map/ppermute | solution.py:481
  37.1 21.6 %collective-permute-start.15 = (bf16[384,256]{1,0:T(8,128)(2,1)S(1)}, bf16[384,256]{1,0:T(8,128)(2,1)S(1)}, u32[]{:S(2)}, u32[]{:S(2)}) collective-permute-start(bf16[384,256]{1,0:T(8,128)(2,1)S(1)} %collective-permute-done.10.refs_6_), channel_id=1, source_target_pairs={{0,224},{32,0},{64,32},{96,64},{128,96},{160,128},{192,160},{224,1... | collective-permute-start | bytes 589832 | tf_op jit(solution)/shard_map/ppermute | solution.py:482
  40.3 18.5 %collective-permute-start.16 = (bf16[384,256]{1,0:T(8,128)(2,1)S(1)}, bf16[384,256]{1,0:T(8,128)(2,1)S(1)}, u32[]{:S(2)}, u32[]{:S(2)}) collective-permute-start(bf16[384,256]{1,0:T(8,128)(2,1)S(1)} %collective-permute-done.14.refs_7_), channel_id=1, source_target_pairs={{0,32},{32,64},{64,96},{96,128},{128,160},{160,192},{192,224},{224... | collective-permute-start | bytes 589832 | tf_op jit(solution)/shard_map/ppermute | solution.py:487
  44.0 6.7 %collective-permute-start.11 = (bf16[512,128]{1,0:T(8,128)(2,1)S(1)}, bf16[512,128]{1,0:T(8,128)(2,1)S(1)}, u32[]{:S(2)}, u32[]{:S(2)}) collective-permute-start(bf16[512,128]{1,0:T(8,128)(2,1)S(1)} %get-tuple-element.76.m0.refs_0_), channel_id=1, source_target_pairs={{0,8},{8,16},{16,24},{24,0},{1,9},{9,17},{17,25},{25,1},{2,10},{10... | collective-permute-start | bytes 393224 | tf_op jit(solution)/shard_map/ppermute | solution.py:485
  47.2 6.5 %collective-permute-start.13 = (bf16[512,128]{1,0:T(8,128)(2,1)S(1)}, bf16[512,128]{1,0:T(8,128)(2,1)S(1)}, u32[]{:S(2)}, u32[]{:S(2)}) collective-permute-start(bf16[512,128]{1,0:T(8,128)(2,1)S(1)} %get-tuple-element.76.m0.refs_0_), channel_id=1, source_target_pairs={{0,16},{8,24},{16,0},{24,8},{1,17},{9,25},{17,1},{25,9},{2,18},{10... | collective-permute-start | bytes 393224 | tf_op jit(solution)/shard_map/ppermute | solution.py:485
  54.1 12.4 %collective-permute-start.17 = (bf16[128,128]{1,0:T(8,128)(2,1)S(1)}, bf16[128,128]{1,0:T(8,128)(2,1)S(1)}, u32[]{:S(2)}, u32[]{:S(2)}) collective-permute-start(bf16[128,128]{1,0:T(8,128)(2,1)S(1)} %get-tuple-element.84.line_ref), channel_id=1, source_target_pairs={{0,32},{32,64},{64,96},{96,128},{128,160},{160,192},{192,224},{224... | collective-permute-start | bytes 98312 | tf_op jit(solution)/shard_map/ppermute | solution.py:493
  54.2 12.4 %collective-permute-start.18 = (bf16[128,128]{1,0:T(8,128)(2,1)S(1)}, bf16[128,128]{1,0:T(8,128)(2,1)S(1)}, u32[]{:S(2)}, u32[]{:S(2)}) collective-permute-start(bf16[128,128]{1,0:T(8,128)(2,1)S(1)} %get-tuple-element.84.line_ref), channel_id=1, source_target_pairs={{0,64},{32,96},{64,128},{96,160},{128,192},{160,224},{192,0},{224,... | collective-permute-start | bytes 98312 | tf_op jit(solution)/shard_map/ppermute | solution.py:493
  55.6 11.0 %collective-permute-start.19 = (bf16[128,128]{1,0:T(8,128)(2,1)S(1)}, bf16[128,128]{1,0:T(8,128)(2,1)S(1)}, u32[]{:S(2)}, u32[]{:S(2)}) collective-permute-start(bf16[128,128]{1,0:T(8,128)(2,1)S(1)} %get-tuple-element.84.line_ref), channel_id=1, source_target_pairs={{0,96},{32,128},{64,160},{96,192},{128,224},{160,0},{192,32},{224,... | collective-permute-start | bytes 98312 | tf_op jit(solution)/shard_map/ppermute | solution.py:493
  74.4 11.7 %collective-permute-start.21 = (bf16[2,144,384]{2,1,0:T(8,128)(2,1)S(1)}, bf16[2,144,384]{2,1,0:T(8,128)(2,1)S(1)}, u32[]{:S(2)}, u32[]{:S(2)}) collective-permute-start(bf16[2,144,384]{2,1,0:T(8,128)(2,1)S(1)} %get-tuple-element.94), channel_id=1, source_target_pairs={{0,24},{8,0},{16,8},{24,16},{1,25},{9,1},{17,9},{25,17},{2,26},{10... | collective-permute-start | bytes 663560 | tf_op jit(solution)/shard_map/ppermute | solution.py:527
  76.0 10.1 %collective-permute-start.20 = (bf16[2,144,384]{2,1,0:T(8,128)(2,1)S(1)}, bf16[2,144,384]{2,1,0:T(8,128)(2,1)S(1)}, u32[]{:S(2)}, u32[]{:S(2)}) collective-permute-start(bf16[2,144,384]{2,1,0:T(8,128)(2,1)S(1)} %get-tuple-element.93), channel_id=1, source_target_pairs={{0,8},{8,16},{16,24},{24,0},{1,9},{9,17},{17,25},{25,1},{2,10},{10... | collective-permute-start | bytes 663560 | tf_op jit(solution)/shard_map/ppermute | solution.py:517
  76.5 9.6 %collective-permute-start.22 = (bf16[2,144,384]{2,1,0:T(8,128)(2,1)S(1)}, bf16[2,144,384]{2,1,0:T(8,128)(2,1)S(1)}, u32[]{:S(2)}, u32[]{:S(2)}) collective-permute-start(bf16[2,144,384]{2,1,0:T(8,128)(2,1)S(1)} %get-tuple-element.95), channel_id=1, source_target_pairs={{0,16},{8,24},{16,0},{24,8},{1,17},{9,25},{17,1},{25,9},{2,18},{10... | collective-permute-start | bytes 663560 | tf_op jit(solution)/shard_map/ppermute | solution.py:518
  78.3 7.8 %collective-permute-start.23 = (bf16[128,128]{1,0:T(8,128)(2,1)S(1)}, bf16[128,128]{1,0:T(8,128)(2,1)S(1)}, u32[]{:S(2)}, u32[]{:S(2)}) collective-permute-start(bf16[128,128]{1,0:T(8,128)(2,1)S(1)} %get-tuple-element.98), channel_id=1, source_target_pairs={{0,128},{32,160},{64,192},{96,224},{128,0},{160,32},{192,64},{224,... | collective-permute-start | bytes 98312 | tf_op jit(solution)/shard_map/ppermute | solution.py:525
  90.7 12.4 %collective-permute-start.25 = (bf16[48,2048]{1,0:T(8,128)(2,1)S(1)}, bf16[48,2048]{1,0:T(8,128)(2,1)S(1)}, u32[]{:S(2)}, u32[]{:S(2)}) collective-permute-start(bf16[48,2048]{1,0:T(8,128)(2,1)S(1)} %get-tuple-element.104), channel_id=1, source_target_pairs={{0,2},{2,4},{4,6},{6,0},{1,3},{3,5},{5,7},{7,1},{8,10},{10,12},{12... | collective-permute-start | bytes 589832 | tf_op jit(solution)/shard_map/ppermute | solution.py:548
  91.9 11.3 %collective-permute-start.26 = (bf16[48,2048]{1,0:T(8,128)(2,1)S(1)}, bf16[48,2048]{1,0:T(8,128)(2,1)S(1)}, u32[]{:S(2)}, u32[]{:S(2)}) collective-permute-start(bf16[48,2048]{1,0:T(8,128)(2,1)S(1)} %get-tuple-element.105), channel_id=1, source_target_pairs={{0,6},{2,0},{4,2},{6,4},{1,7},{3,1},{5,3},{7,5},{8,14},{10,8},{12,... | collective-permute-start | bytes 589832 | tf_op jit(solution)/shard_map/ppermute | solution.py:549
  94.0 9.1 %collective-permute-start.27 = (bf16[48,2048]{1,0:T(8,128)(2,1)S(1)}, bf16[48,2048]{1,0:T(8,128)(2,1)S(1)}, u32[]{:S(2)}, u32[]{:S(2)}) collective-permute-start(bf16[48,2048]{1,0:T(8,128)(2,1)S(1)} %get-tuple-element.106), channel_id=1, source_target_pairs={{0,4},{2,6},{4,0},{6,2},{1,5},{3,7},{5,1},{7,3},{8,12},{10,14},{12... | collective-permute-start | bytes 589832 | tf_op jit(solution)/shard_map/ppermute | solution.py:550
  (15 other events, 97.8 us)

commit v4 on v3

--- a/solution.py
+++ b/solution.py
@@ -274,15 +274,16 @@
 TALL = 144
 
 
-def attention_kernel(pair, *refs):
-    lead, refs = refs[:2], refs[2:]
-    taken = 8 if pair else 2
+def attention_kernel(others, *refs):
+    many = 3 if others else 1
+    lead, refs = refs[:many], refs[many:]
+    taken = 8 if others else 2
     kvs, refs = refs[:taken], refs[taken:]
-    outs, refs = refs[:2], refs[2:]
-    keys, turned = refs[:2] if pair else kvs
-    row_max, weighted, queries, scores, units = refs[2:] if pair else refs
+    outs, refs = refs[:many], refs[many:]
+    keys, turned = refs[:2] if others else kvs
+    row_max, weighted, queries, scores, units = refs[2:] if others else refs
     rows = lead[0].shape[0] - 128
-    wide = 2 * rows
+    wide = many * rows
     blocks_at, lines_at = ring_places(), line_places()
     my_z, my_x = blocks_at[0], lines_at[0]
     first = lane_ids((rows, 128)) < HD
@@ -291,60 +292,60 @@
         at = slice(n * rows, (n + 1) * rows)
         queries[0, at, :] = jnp.where(first, scaled, 0).astype(BF16)
         queries[1, at, :] = jnp.where(first, 0, scaled).astype(BF16)
-    if pair:
+    if others:
         ones = jnp.where(row_ids((TALL - 128, rows)) == 0, 1.0, 0.0).astype(BF16)
         for n, ref in enumerate(kvs):
             keys[n] = ref[:, :128]
             turned[n, :128, :] = jnp.transpose(ref[:, 128:])
             turned[n, 128:, :] = ones
-    row_max[...] = jnp.full_like(row_max, NEGATIVE)
-    weighted[...] = jnp.zeros_like(weighted)
 
     def score(n, out):
         for m in range(2):
             out[m] = dot(keys[n], queries[m], NT)
 
-    def soft_gather(slot, n, source, limit=None):
+    def soft_gather(n, source, limit=None):
         for m in range(2):
-            i = 2 * slot + m
             got = source[m]
-            if limit is not None:
+            if limit is None:
+                old = row_max[m, :1, :]
+                new = jnp.maximum(old, jnp.max(got, axis=0, keepdims=True))
+            else:
                 got = jnp.where(row_ids((rows, wide)) <= limit, got, NEGATIVE)
-            old = row_max[i, :1, :]
-            new = jnp.maximum(old, jnp.max(got, axis=0, keepdims=True))
+                new = jnp.max(got, axis=0, keepdims=True)
             soft = jnp.exp(got - new).astype(BF16)
-            row_max[i] = jnp.broadcast_to(new, (8, wide))
-            weighted[i] = weighted[i] * jnp.exp(old - new) + dot(turned[n], soft)
-
-    def put(at, n, slot):
-        units[0, at] = n
-        units[1, at] = slot
+            row_max[m] = jnp.broadcast_to(new, (8, wide))
+            more = dot(turned[n], soft)
+            weighted[m] = more if limit is not None else weighted[m] * jnp.exp(old - new) + more
 
     total = jnp.int32(0)
+    units[0] = jnp.int32(0)
     for n in range(1, 8):
-        put(total, n, 0)
+        units[total] = jnp.int32(n)
         total = total + (blocks_at[n] < my_z).astype(jnp.int32)
-    for extra in range(3):
-        put(total + extra, 0, 1)
+    units[total] = jnp.int32(0)
 
     column = lane_ids((1, wide))
-    within = jnp.where(column < rows, column, column - rows)
-    x_of = jnp.where(column < rows, lines_at[2 * pair], lines_at[2 * pair + 1])
+    within, x_of = column, jnp.full((1, wide), lines_at[1 if others else 0])
+    for n in range(1, many):
+        within = jnp.where(column < n * rows, within, column - n * rows)
+        x_of = jnp.where(column < n * rows, x_of, lines_at[1 + n])
     limit = jnp.where(x_of > my_x, rows, jnp.where(x_of == my_x, within, -1))
     score(0, scores[1])
-    score(units[0, 0], scores[0])
-    soft_gather(0, 0, scores[1], limit)
-
-    def step(at, now, other):
-        score(units[0, at + 1], scores[other])
-        soft_gather(units[1, at], units[0, at], scores[now])
+    score(units[0], scores[0])
+    soft_gather(0, scores[1], limit)
 
     def two(t, carry):
-        step(2 * t, 0, 1)
-        step(2 * t + 1, 1, 0)
+        score(units[2 * t + 1], scores[1])
+        soft_gather(units[2 * t], scores[0])
+        score(units[2 * t + 2], scores[0])
+        soft_gather(units[2 * t + 1], scores[1])
         return carry
 
-    lax.fori_loop(0, (total + 1) // 2, two, 0)
+    lax.fori_loop(0, total // 2, two, 0)
+
+    @pl.when(total % 2 == 1)
+    def _():
+        soft_gather(units[total - 1], scores[0])
 
     for n, out in enumerate(outs):
         at = slice(n * rows, (n + 1) * rows)
@@ -417,7 +418,8 @@
         out[...] = total.astype(out.dtype)
 
 
-def norm_kernel(own_ref, p1, p2, p3, gain_ref, out_ref):
+def norm_kernel(own_ref, p1, p2, p3, gain_ref, logs_ref, out_ref, logs_out):
+    logs_out[...] = logs_ref[...]
     total = own_ref[...]
     for part in (p1, p2, p3):
         total = total + part[...].astype(F32)
@@ -493,29 +495,32 @@
     lines = [permute(line, "z", ring(8, s)) for s in (1, 2, 3)]
 
     payload = shaped((2, TALL, rows), BF16)
-    wide = 2 * rows
-
-    def attend(pair, lead, arrays):
+
+    def attend(others, lead, arrays):
+        wide = len(lead) * rows
         return call(
-            functools.partial(attention_kernel, pair),
-            (payload,) * 2
-            + ((shaped((8, rows, 128), BF16), shaped((8, TALL, rows), BF16)) if pair else ()),
+            functools.partial(attention_kernel, others),
+            (payload,) * len(lead)
+            + ((shaped((8, rows, 128), BF16), shaped((8, TALL, rows), BF16)) if others else ()),
             (),
             (*lead, *arrays),
             scratch=[
-                pltpu.VMEM((4, 8, wide), F32), pltpu.VMEM((4, TALL, wide), F32),
+                pltpu.VMEM((2, 8, wide), F32), pltpu.VMEM((2, TALL, wide), F32),
                 pltpu.VMEM((2, wide, 128), BF16), [pltpu.VMEM((2, rows, wide), F32)] * 2,
-                pltpu.SMEM((2, 16), jnp.int32),
+                pltpu.SMEM((16,), jnp.int32),
             ],
             flops=8 * 10**9,
         )
 
-    to_next, to_far, keys, turned = attend(
-        1, messages[2:], (kv, right1, left1, right2, left2, right3, left3, right4)
-    )
-    to_next, to_far, keys, turned, line, lines = together((to_next, to_far, keys, turned, line, lines))
+    to_before, to_next, to_far, keys, turned = attend(
+        True, messages[1:], (kv, right1, left1, right2, left2, right3, left3, right4)
+    )
+    to_before, to_next, to_far, keys, turned, line, lines = together(
+        (to_before, to_next, to_far, keys, turned, line, lines)
+    )
+    from_far = permute(to_far, "x", ring(4, 2))
     from_before = permute(to_next, "x", ring(4, 1))
-    from_far = permute(to_far, "x", ring(4, 2))
+    from_next = permute(to_before, "x", ring(4, -1))
     window, near = call(
         window_kernel,
         (shaped((128, 128), BF16), shaped((128, 128), F32)),
@@ -523,8 +528,8 @@
     )
     window, keys = together((window, keys))
     window = permute(window, "z", ring(8, 4))
-    ours, to_before = attend(0, messages[:2], (keys, turned))
-    back = [ours, from_before, permute(to_before, "x", ring(4, -1)), from_far]
+    (ours,) = attend(False, messages[:1], (keys, turned))
+    back = [ours, from_before, from_next, from_far]
     ours, others, log_sums = call(
         finish_kernel,
         (shaped((4, rows // 8, 2048), BF16), shaped((4, rows // 8, 2048), BF16), shaped((2, rows), F32)),
@@ -539,16 +544,16 @@
         (shaped(piece, F32),) + (shaped(piece, BF16),) * 3,
         (), (ours, theirs), flops=10**8,
     )
-    layer_out = call(
+    layer_out, log_sums = call(
         norm_kernel,
-        shaped(piece, BF16),
+        (shaped(piece, BF16), shaped((2, rows), F32)),
         (),
         (
             own,
             permute(plus1, "y", ring(4, 1)),
             permute(plus3, "y", ring(4, -1)),
             permute(plus2, "y", ring(4, 2)),
-            out_gain.reshape(1, 2048),
+            out_gain.reshape(1, 2048), log_sums,
         ),
         flops=10**8,
     )

time: 105 us -> 99.2 us (0.945)
  waiting for transfers between devices: 36.4 us -> 32.6 us
  Pallas kernels: 28.6 us -> 27.4 us
    ppermute x1, waiting for transfers between devices: 7.17 us -> 4.01 us  [per_device(): window = permute(window, 'z', ring(8, 4))]
    ppermute x1, starting transfers between devices: 1.63 us -> 2.98 us  [per_device(): from_next = permute(to_before, 'x', ring(4, -1))]
    pallas_call x10, Pallas kernels: 28.6 us -> 27.4 us  [call(): pl.pallas_call(kernel, out_shape=outs, in_specs=[pl.BlockSpec(memory_spac...]
    ppermute x1, starting transfers between devices: 1.81 us -> 0.6 us  [per_device(): from_far = permute(to_far, 'x', ring(4, 2))]
  transfers between devices with their start and end apart: 28 -> 28, of which waited for: 12 -> 12; matrix products, arithmetic and copies ran while one was open for 3% -> 3% of each run, Pallas kernels for 15% -> 23%
where the time goes in v4:
time: 99.2 us; the launch traced here: 99 us
  starting transfers between devices  34.2 us (34%)
  waiting for transfers between devices  32.6 us (33%)
  Pallas kernels  27.4 us (28%)
  local copies, waits for them, and re-layouts  1.75 us (2%)
  other arithmetic  1.58 us (2%)
  between operations  1.58 us (2%)
    pallas_call x10, Pallas kernels, call(): pl.pallas_call(kernel, out_shape=outs, in_specs=[pl.BlockSpec(memory_spac...  27.4 us
    ppermute x1, waiting for transfers between devices, per_device(): permute(plus1, 'y', ring(4, 1))  9.13 us
    ppermute x3, starting transfers between devices, per_device(): messages.append(permute(message, 'x', ring(4, shift)))  5.05 us
    ppermute x3, starting transfers between devices, per_device(): lines = [permute(line, 'z', ring(8, s)) for s in (1, 2, 3)]  4.56 us
    ppermute x1, waiting for transfers between devices, per_device(): window = permute(window, 'z', ring(8, 4))  4.01 us
    ppermute x3, waiting for transfers between devices, per_device(): messages.append(permute(message, 'x', ring(4, shift)))  4.01 us
    ppermute x1, waiting for transfers between devices, per_device(): down = permute(hidden_in, 'y', ring(4, -1))  3.7 us
    ppermute x1, starting transfers between devices, per_device(): right4 = permute(right3, 'z', ring(8, 1))  3.69 us
  transfers between devices with their start and end apart: 28, of which 12 were waited for; matrix products, arithmetic and copies ran while one was open for 3% of the time, Pallas kernels for 23%

profile of v4, /device:TPU:224, one launch (start us, length us, event | category | flops | bytes accessed | tf_op | source)
XLA Modules:
  0.0 99.0 jit_solution(16395065353458882816)
XLA Ops:
  0.6 1.7 %collective-permute-start = (bf16[384,256]{1,0:T(8,128)(2,1)}, bf16[384,256]{1,0:T(8,128)(2,1)S(1)}, u32[]{:S(2)}, u32[]{:S(2)}) collective-permute-start(bf16[384,256]{1,0:T(8,128)(2,1)} %param.17), channel_id=1, source_target_pairs={{0,2},{2,4},{4,6},{6,0},{1,3},{3,5},{5,7},{7,1},{8,10},{10,12},{12... | collective-permute-start | bytes 589832 | tf_op jit(solution)/shard_map/ppermute | solution.py:442
  2.3 1.7 %collective-permute-start.1 = (bf16[384,256]{1,0:T(8,128)(2,1)}, bf16[384,256]{1,0:T(8,128)(2,1)S(1)}, u32[]{:S(2)}, u32[]{:S(2)}) collective-permute-start(bf16[384,256]{1,0:T(8,128)(2,1)} %param.17), channel_id=1, source_target_pairs={{0,6},{2,0},{4,2},{6,4},{1,7},{3,1},{5,3},{7,5},{8,14},{10,8},{12,... | collective-permute-start | bytes 589832 | tf_op jit(solution)/shard_map/ppermute | solution.py:443
  3.9 2.0 %collective-permute-start.2 = (bf16[384,256]{1,0:T(8,128)(2,1)}, bf16[384,256]{1,0:T(8,128)(2,1)S(1)}, u32[]{:S(2)}, u32[]{:S(2)}) collective-permute-start(bf16[384,256]{1,0:T(8,128)(2,1)} %param.17), channel_id=1, source_target_pairs={{0,4},{2,6},{4,0},{6,2},{1,5},{3,7},{5,1},{7,3},{8,12},{10,14},{12... | collective-permute-start | bytes 589832 | tf_op jit(solution)/shard_map/ppermute | solution.py:444
  8.8 3.7 %collective-permute-done.1.h2 = bf16[384,256]{1,0:T(8,128)(2,1)S(1)} collective-permute-done((bf16[384,256]{1,0:T(8,128)(2,1)}, bf16[384,256]{1,0:T(8,128)(2,1)S(1)}, u32[]{:S(2)}, u32[]{:S(2)}) %collective-permute-start.1) | collective-permute-done | bytes 196640 | tf_op jit(solution)/shard_map/ppermute | solution.py:443
  12.5 1.7 %collective-permute-done.2.h3 = bf16[384,256]{1,0:T(8,128)(2,1)S(1)} collective-permute-done((bf16[384,256]{1,0:T(8,128)(2,1)}, bf16[384,256]{1,0:T(8,128)(2,1)S(1)}, u32[]{:S(2)}, u32[]{:S(2)}) %collective-permute-start.2) | collective-permute-done | bytes 196640 | tf_op jit(solution)/shard_map/ppermute | solution.py:444
  15.9 1.8 %shard_map.176 = (bf16[384,2048]{1,0:T(8,128)(2,1)S(1)}, bf16[384,128]{1,0:T(8,128)(2,1)S(1)}, bf16[384,256]{1,0:T(8,128)(2,1)S(1)}) custom-call(bf16[384,256]{1,0:T(8,128)(2,1)S(1)} %pad_maximum_fusion.own, bf16[384,256]{1,0:T(8,128)(2,1)S(1)} %collective-permute-done.h1, bf16[384,256]{1,0:T(8,128)(2,1)S(1)} %collective-permute-done.1.h2, ...), custom_call_target="tpu_custom_call" | custom-call | flops 1409286144 | bytes 1409286 | tf_op jit(solution)/shard_map/pallas_call | solution.py:31
  17.8 2.0 %collective-permute-start.8 = (bf16[384,256]{1,0:T(8,128)(2,1)S(1)}, bf16[384,256]{1,0:T(8,128)(2,1)S(1)}, u32[]{:S(2)}, u32[]{:S(2)}) collective-permute-start(bf16[384,256]{1,0:T(8,128)(2,1)S(1)} %get-tuple-element.57.refs_3_), channel_id=1, source_target_pairs={{0,224},{32,0},{64,32},{96,64},{128,96},{160,128},{192,160},{224,1... | collective-permute-start | bytes 589832 | tf_op jit(solution)/shard_map/ppermute | solution.py:457
  19.9 3.8 %shard_map.177 = (f32[12,64,128]{2,1,0:T(8,128)S(1)}, f32[12,64,128]{2,1,0:T(8,128)S(1)}, f32[12,64,128]{2,1,0:T(8,128)S(1)}, f32[6,64,128]{2,1,0:T(8,128)S(1)},...) custom-call(bf16[384,2048]{1,0:T(8,128)(2,1)S(1)} %get-tuple-element.58.normed, ...), custom_call_target="tpu_custom_call" | custom-call | flops 6000000000 | bytes 6000000 | tf_op jit(solution)/shard_map/pallas_call | solution.py:31
  26.9 2.8 %collective-permute-start.9 = (bf16[384,256]{1,0:T(8,128)(2,1)S(1)}, bf16[384,256]{1,0:T(8,128)(2,1)S(1)}, u32[]{:S(2)}, u32[]{:S(2)}) collective-permute-start(bf16[384,256]{1,0:T(8,128)(2,1)S(1)} %collective-permute-done.7.refs_4_), channel_id=1, source_target_pairs={{0,32},{32,64},{64,96},{96,128},{128,160},{160,192},{192,224},{224... | collective-permute-start | bytes 589832 | tf_op jit(solution)/shard_map/ppermute | solution.py:473
  29.7 3.8 %shard_map.178 = (f32[384,128]{1,0:T(8,128)S(1)}, f32[384,128]{1,0:T(8,128)S(1)}, bf16[512,128]{1,0:T(8,128)(2,1)S(1)}) custom-call(f32[12,64,128]{2,1,0:T(8,128)S(1)} %get-tuple-element.69.lower_ref, f32[12,64,128]{2,1,0:T(8,128)S(1)} %get-tuple-element.70.reading_ref, f32[12,64,128]{2,1,0:T(8,128)S(1)} %get-tuple-element.71.rhs_ref, ...), custom_call_target="tpu_custom_call" | custom-call | flops 6000000000 | bytes 6000000 | tf_op jit(solution)/shard_map/pallas_call | solution.py:31
  34.1 3.0 %collective-permute-start.14 = (bf16[384,256]{1,0:T(8,128)(2,1)S(1)}, bf16[384,256]{1,0:T(8,128)(2,1)S(1)}, u32[]{:S(2)}, u32[]{:S(2)}) collective-permute-start(bf16[384,256]{1,0:T(8,128)(2,1)S(1)} %collective-permute-done.9.refs_6_), channel_id=1, source_target_pairs={{0,32},{32,64},{64,96},{96,128},{128,160},{160,192},{192,224},{224... | collective-permute-start | bytes 589832 | tf_op jit(solution)/shard_map/ppermute | solution.py:483
  37.1 3.2 %collective-permute-done.14.refs_8_ = bf16[384,256]{1,0:T(8,128)(2,1)S(1)} collective-permute-done((bf16[384,256]{1,0:T(8,128)(2,1)S(1)}, bf16[384,256]{1,0:T(8,128)(2,1)S(1)}, u32[]{:S(2)}, u32[]{:S(2)}) %collective-permute-start.14) | collective-permute-done | bytes 196640 | tf_op jit(solution)/shard_map/ppermute | solution.py:483
  40.3 3.7 %collective-permute-start.16 = (bf16[384,256]{1,0:T(8,128)(2,1)S(1)}, bf16[384,256]{1,0:T(8,128)(2,1)S(1)}, u32[]{:S(2)}, u32[]{:S(2)}) collective-permute-start(bf16[384,256]{1,0:T(8,128)(2,1)S(1)} %collective-permute-done.14.refs_8_), channel_id=1, source_target_pairs={{0,32},{32,64},{64,96},{96,128},{128,160},{160,192},{192,224},{224... | collective-permute-start | bytes 589832 | tf_op jit(solution)/shard_map/ppermute | solution.py:489
  45.4 1.7 %collective-permute-start.12 = (bf16[512,128]{1,0:T(8,128)(2,1)S(1)}, bf16[512,128]{1,0:T(8,128)(2,1)S(1)}, u32[]{:S(2)}, u32[]{:S(2)}) collective-permute-start(bf16[512,128]{1,0:T(8,128)(2,1)S(1)} %get-tuple-element.78.m0.refs_0_), channel_id=1, source_target_pairs={{0,24},{8,0},{16,8},{24,16},{1,25},{9,1},{17,9},{25,17},{2,26},{10... | collective-permute-start | bytes 393224 | tf_op jit(solution)/shard_map/ppermute | solution.py:487
  47.2 1.8 %collective-permute-start.13 = (bf16[512,128]{1,0:T(8,128)(2,1)S(1)}, bf16[512,128]{1,0:T(8,128)(2,1)S(1)}, u32[]{:S(2)}, u32[]{:S(2)}) collective-permute-start(bf16[512,128]{1,0:T(8,128)(2,1)S(1)} %get-tuple-element.78.m0.refs_0_), channel_id=1, source_target_pairs={{0,16},{8,24},{16,0},{24,8},{1,17},{9,25},{17,1},{25,9},{2,18},{10... | collective-permute-start | bytes 393224 | tf_op jit(solution)/shard_map/ppermute | solution.py:487
  50.6 3.0 %collective-permute-done.13.refs_2_.m3 = bf16[512,128]{1,0:T(8,128)(2,1)S(1)} collective-permute-done((bf16[512,128]{1,0:T(8,128)(2,1)S(1)}, bf16[512,128]{1,0:T(8,128)(2,1)S(1)}, u32[]{:S(2)}, u32[]{:S(2)}) %collective-permute-start.13) | collective-permute-done | bytes 131104 | tf_op jit(solution)/shard_map/ppermute | solution.py:487
  55.6 3.1 %collective-permute-start.19 = (bf16[128,128]{1,0:T(8,128)(2,1)S(1)}, bf16[128,128]{1,0:T(8,128)(2,1)S(1)}, u32[]{:S(2)}, u32[]{:S(2)}) collective-permute-start(bf16[128,128]{1,0:T(8,128)(2,1)S(1)} %get-tuple-element.87.line_ref), channel_id=1, source_target_pairs={{0,96},{32,128},{64,160},{96,192},{128,224},{160,0},{192,32},{224,... | collective-permute-start | bytes 98312 | tf_op jit(solution)/shard_map/ppermute | solution.py:495
  58.7 10.5 %shard_map.179 = (bf16[2,144,384]{2,1,0:T(8,128)(2,1)S(1)}, bf16[2,144,384]{2,1,0:T(8,128)(2,1)S(1)}, bf16[2,144,384]{2,1,0:T(8,128)(2,1)S(1)}, bf16[8,384,128]{2,1,0:T(8,128)(2,1)S(1)}, bf16[8,144,384]{2,1,0:T(8,128)(2,1)S(1)}) custom-call(bf16[512,128]{1,0:T(8,128)(2,1)S(1)} %collective-permute-done.11.refs_0_.m1, ...), custom_call_target="tpu_custom_call" | custom-call | flops 8000000000 | bytes 8000000 | tf_op jit(solution)/shard_map/pallas_call | solution.py:31
  70.1 3.0 %collective-permute-start.21 = (bf16[2,144,384]{2,1,0:T(8,128)(2,1)S(1)}, bf16[2,144,384]{2,1,0:T(8,128)(2,1)S(1)}, u32[]{:S(2)}, u32[]{:S(2)}) collective-permute-start(bf16[2,144,384]{2,1,0:T(8,128)(2,1)S(1)} %get-tuple-element.96), channel_id=1, source_target_pairs={{0,24},{8,0},{16,8},{24,16},{1,25},{9,1},{17,9},{25,17},{2,26},{10... | collective-permute-start | bytes 663560 | tf_op jit(solution)/shard_map/ppermute | solution.py:523
  73.7 3.8 %shard_map.182.p0 = bf16[2,144,384]{2,1,0:T(8,128)(2,1)S(1)} custom-call(bf16[512,128]{1,0:T(8,128)(2,1)S(1)} %get-tuple-element.78.m0.refs_0_, bf16[8,384,128]{2,1,0:T(8,128)(2,1)S(1)} %get-tuple-element.93.refs_1_, bf16[8,144,384]{2,1,0:T(8,128)(2,1)S(1)} %get-tuple-element.94.refs_2_), custom_call_target="tpu_custom_call" | custom-call | flops 8000000000 | bytes 8000000 | tf_op jit(solution)/shard_map/pallas_call | solution.py:31
  77.5 4.0 %collective-permute-done.23.window_ref = bf16[128,128]{1,0:T(8,128)(2,1)S(1)} collective-permute-done((bf16[128,128]{1,0:T(8,128)(2,1)S(1)}, bf16[128,128]{1,0:T(8,128)(2,1)S(1)}, u32[]{:S(2)}, u32[]{:S(2)}) %collective-permute-start.23) | collective-permute-done | bytes 32800 | tf_op jit(solution)/shard_map/ppermute | solution.py:530
  83.2 2.3 %collective-permute-done.24.other_ref = bf16[4,48,2048]{2,1,0:T(8,128)(2,1)S(1)} collective-permute-done((bf16[4,48,2048]{2,1,0:T(8,128)(2,1)S(1)}, bf16[4,48,2048]{2,1,0:T(8,128)(2,1)S(1)}, u32[]{:S(2)}, u32[]{:S(2)}) %collective-permute-start.24) | collective-permute-done | bytes 786464 | tf_op jit(solution)/shard_map/ppermute | solution.py:540
  86.8 2.2 %collective-permute-start.26 = (bf16[48,2048]{1,0:T(8,128)(2,1)S(1)}, bf16[48,2048]{1,0:T(8,128)(2,1)S(1)}, u32[]{:S(2)}, u32[]{:S(2)}) collective-permute-start(bf16[48,2048]{1,0:T(8,128)(2,1)S(1)} %get-tuple-element.107), channel_id=1, source_target_pairs={{0,6},{2,0},{4,2},{6,4},{1,7},{3,1},{5,3},{7,5},{8,14},{10,8},{12,... | collective-permute-start | bytes 589832 | tf_op jit(solution)/shard_map/ppermute | solution.py:554
  89.0 9.1 %collective-permute-done.25.p1 = bf16[48,2048]{1,0:T(8,128)(2,1)S(1)} collective-permute-done((bf16[48,2048]{1,0:T(8,128)(2,1)S(1)}, bf16[48,2048]{1,0:T(8,128)(2,1)S(1)}, u32[]{:S(2)}, u32[]{:S(2)}) %collective-permute-start.25) | collective-permute-done | bytes 196640 | tf_op jit(solution)/shard_map/ppermute | solution.py:553
  (68 shorter events, 18.1 us)
Async XLA Ops:
  0.6 8.2 %collective-permute-start = (bf16[384,256]{1,0:T(8,128)(2,1)}, bf16[384,256]{1,0:T(8,128)(2,1)S(1)}, u32[]{:S(2)}, u32[]{:S(2)}) collective-permute-start(bf16[384,256]{1,0:T(8,128)(2,1)} %param.17), channel_id=1, source_target_pairs={{0,2},{2,4},{4,6},{6,0},{1,3},{3,5},{5,7},{7,1},{8,10},{10,12},{12... | collective-permute-start | bytes 589832 | tf_op jit(solution)/shard_map/ppermute | solution.py:442
  2.3 10.2 %collective-permute-start.1 = (bf16[384,256]{1,0:T(8,128)(2,1)}, bf16[384,256]{1,0:T(8,128)(2,1)S(1)}, u32[]{:S(2)}, u32[]{:S(2)}) collective-permute-start(bf16[384,256]{1,0:T(8,128)(2,1)} %param.17), channel_id=1, source_target_pairs={{0,6},{2,0},{4,2},{6,4},{1,7},{3,1},{5,3},{7,5},{8,14},{10,8},{12,... | collective-permute-start | bytes 589832 | tf_op jit(solution)/shard_map/ppermute | solution.py:443
  3.9 10.3 %collective-permute-start.2 = (bf16[384,256]{1,0:T(8,128)(2,1)}, bf16[384,256]{1,0:T(8,128)(2,1)S(1)}, u32[]{:S(2)}, u32[]{:S(2)}) collective-permute-start(bf16[384,256]{1,0:T(8,128)(2,1)} %param.17), channel_id=1, source_target_pairs={{0,4},{2,6},{4,0},{6,2},{1,5},{3,7},{5,1},{7,3},{8,12},{10,14},{12... | collective-permute-start | bytes 589832 | tf_op jit(solution)/shard_map/ppermute | solution.py:444
  5.9 10.0 %collective-permute-start.3 = (bf16[384,256]{1,0:T(8,128)(2,1)}, bf16[384,256]{1,0:T(8,128)(2,1)S(1)}, u32[]{:S(2)}, u32[]{:S(2)}) collective-permute-start(bf16[384,256]{1,0:T(8,128)(2,1)} %param.17), channel_id=1, source_target_pairs={{0,1},{1,0},{2,3},{3,2},{4,5},{5,4},{6,7},{7,6},{8,9},{9,8},{10,11... | collective-permute-start | bytes 589832 | tf_op jit(solution)/shard_map/ppermute | solution.py:445
  8.8 7.1 %collective-permute-start.4 = (bf16[384,256]{1,0:T(8,128)(2,1)S(1)}, bf16[384,256]{1,0:T(8,128)(2,1)S(1)}, u32[]{:S(2)}, u32[]{:S(2)}) collective-permute-start(bf16[384,256]{1,0:T(8,128)(2,1)S(1)} %collective-permute-done.h1), channel_id=1, source_target_pairs={{0,1},{1,0},{2,3},{3,2},{4,5},{5,4},{6,7},{7,6},{8,9},{9,8},{10,11... | collective-permute-start | bytes 589832 | tf_op jit(solution)/shard_map/ppermute | solution.py:445
  17.7 7.4 %collective-permute-start.7 = (bf16[384,256]{1,0:T(8,128)(2,1)S(1)}, bf16[384,256]{1,0:T(8,128)(2,1)S(1)}, u32[]{:S(2)}, u32[]{:S(2)}) collective-permute-start(bf16[384,256]{1,0:T(8,128)(2,1)S(1)} %get-tuple-element.57.refs_3_), channel_id=1, source_target_pairs={{0,32},{32,64},{64,96},{96,128},{128,160},{160,192},{192,224},{224... | collective-permute-start | bytes 589832 | tf_op jit(solution)/shard_map/ppermute | solution.py:456
  17.8 8.6 %collective-permute-start.8 = (bf16[384,256]{1,0:T(8,128)(2,1)S(1)}, bf16[384,256]{1,0:T(8,128)(2,1)S(1)}, u32[]{:S(2)}, u32[]{:S(2)}) collective-permute-start(bf16[384,256]{1,0:T(8,128)(2,1)S(1)} %get-tuple-element.57.refs_3_), channel_id=1, source_target_pairs={{0,224},{32,0},{64,32},{96,64},{128,96},{160,128},{192,160},{224,1... | collective-permute-start | bytes 589832 | tf_op jit(solution)/shard_map/ppermute | solution.py:457
  26.4 7.7 %collective-permute-start.10 = (bf16[384,256]{1,0:T(8,128)(2,1)S(1)}, bf16[384,256]{1,0:T(8,128)(2,1)S(1)}, u32[]{:S(2)}, u32[]{:S(2)}) collective-permute-start(bf16[384,256]{1,0:T(8,128)(2,1)S(1)} %collective-permute-done.8.refs_5_), channel_id=1, source_target_pairs={{0,224},{32,0},{64,32},{96,64},{128,96},{160,128},{192,160},{224,1... | collective-permute-start | bytes 589832 | tf_op jit(solution)/shard_map/ppermute | solution.py:474
  26.9 7.2 %collective-permute-start.9 = (bf16[384,256]{1,0:T(8,128)(2,1)S(1)}, bf16[384,256]{1,0:T(8,128)(2,1)S(1)}, u32[]{:S(2)}, u32[]{:S(2)}) collective-permute-start(bf16[384,256]{1,0:T(8,128)(2,1)S(1)} %collective-permute-done.7.refs_4_), channel_id=1, source_target_pairs={{0,32},{32,64},{64,96},{96,128},{128,160},{160,192},{192,224},{224... | collective-permute-start | bytes 589832 | tf_op jit(solution)/shard_map/ppermute | solution.py:473
  34.1 6.1 %collective-permute-start.14 = (bf16[384,256]{1,0:T(8,128)(2,1)S(1)}, bf16[384,256]{1,0:T(8,128)(2,1)S(1)}, u32[]{:S(2)}, u32[]{:S(2)}) collective-permute-start(bf16[384,256]{1,0:T(8,128)(2,1)S(1)} %collective-permute-done.9.refs_6_), channel_id=1, source_target_pairs={{0,32},{32,64},{64,96},{96,128},{128,160},{160,192},{192,224},{224... | collective-permute-start | bytes 589832 | tf_op jit(solution)/shard_map/ppermute | solution.py:483
  37.1 21.6 %collective-permute-start.15 = (bf16[384,256]{1,0:T(8,128)(2,1)S(1)}, bf16[384,256]{1,0:T(8,128)(2,1)S(1)}, u32[]{:S(2)}, u32[]{:S(2)}) collective-permute-start(bf16[384,256]{1,0:T(8,128)(2,1)S(1)} %collective-permute-done.10.refs_7_), channel_id=1, source_target_pairs={{0,224},{32,0},{64,32},{96,64},{128,96},{160,128},{192,160},{224,1... | collective-permute-start | bytes 589832 | tf_op jit(solution)/shard_map/ppermute | solution.py:484
  40.3 18.5 %collective-permute-start.16 = (bf16[384,256]{1,0:T(8,128)(2,1)S(1)}, bf16[384,256]{1,0:T(8,128)(2,1)S(1)}, u32[]{:S(2)}, u32[]{:S(2)}) collective-permute-start(bf16[384,256]{1,0:T(8,128)(2,1)S(1)} %collective-permute-done.14.refs_8_), channel_id=1, source_target_pairs={{0,32},{32,64},{64,96},{96,128},{128,160},{160,192},{192,224},{224... | collective-permute-start | bytes 589832 | tf_op jit(solution)/shard_map/ppermute | solution.py:489
  44.0 6.7 %collective-permute-start.11 = (bf16[512,128]{1,0:T(8,128)(2,1)S(1)}, bf16[512,128]{1,0:T(8,128)(2,1)S(1)}, u32[]{:S(2)}, u32[]{:S(2)}) collective-permute-start(bf16[512,128]{1,0:T(8,128)(2,1)S(1)} %get-tuple-element.78.m0.refs_0_), channel_id=1, source_target_pairs={{0,8},{8,16},{16,24},{24,0},{1,9},{9,17},{17,25},{25,1},{2,10},{10... | collective-permute-start | bytes 393224 | tf_op jit(solution)/shard_map/ppermute | solution.py:487
  47.2 6.5 %collective-permute-start.13 = (bf16[512,128]{1,0:T(8,128)(2,1)S(1)}, bf16[512,128]{1,0:T(8,128)(2,1)S(1)}, u32[]{:S(2)}, u32[]{:S(2)}) collective-permute-start(bf16[512,128]{1,0:T(8,128)(2,1)S(1)} %get-tuple-element.78.m0.refs_0_), channel_id=1, source_target_pairs={{0,16},{8,24},{16,0},{24,8},{1,17},{9,25},{17,1},{25,9},{2,18},{10... | collective-permute-start | bytes 393224 | tf_op jit(solution)/shard_map/ppermute | solution.py:487
  54.2 15.1 %collective-permute-start.17 = (bf16[128,128]{1,0:T(8,128)(2,1)S(1)}, bf16[128,128]{1,0:T(8,128)(2,1)S(1)}, u32[]{:S(2)}, u32[]{:S(2)}) collective-permute-start(bf16[128,128]{1,0:T(8,128)(2,1)S(1)} %get-tuple-element.87.line_ref), channel_id=1, source_target_pairs={{0,32},{32,64},{64,96},{96,128},{128,160},{160,192},{192,224},{224... | collective-permute-start | bytes 98312 | tf_op jit(solution)/shard_map/ppermute | solution.py:495
  54.2 15.0 %collective-permute-start.18 = (bf16[128,128]{1,0:T(8,128)(2,1)S(1)}, bf16[128,128]{1,0:T(8,128)(2,1)S(1)}, u32[]{:S(2)}, u32[]{:S(2)}) collective-permute-start(bf16[128,128]{1,0:T(8,128)(2,1)S(1)} %get-tuple-element.87.line_ref), channel_id=1, source_target_pairs={{0,64},{32,96},{64,128},{96,160},{128,192},{160,224},{192,0},{224,... | collective-permute-start | bytes 98312 | tf_op jit(solution)/shard_map/ppermute | solution.py:495
  55.6 13.7 %collective-permute-start.19 = (bf16[128,128]{1,0:T(8,128)(2,1)S(1)}, bf16[128,128]{1,0:T(8,128)(2,1)S(1)}, u32[]{:S(2)}, u32[]{:S(2)}) collective-permute-start(bf16[128,128]{1,0:T(8,128)(2,1)S(1)} %get-tuple-element.87.line_ref), channel_id=1, source_target_pairs={{0,96},{32,128},{64,160},{96,192},{128,224},{160,0},{192,32},{224,... | collective-permute-start | bytes 98312 | tf_op jit(solution)/shard_map/ppermute | solution.py:495
  69.8 11.7 %collective-permute-start.20 = (bf16[2,144,384]{2,1,0:T(8,128)(2,1)S(1)}, bf16[2,144,384]{2,1,0:T(8,128)(2,1)S(1)}, u32[]{:S(2)}, u32[]{:S(2)}) collective-permute-start(bf16[2,144,384]{2,1,0:T(8,128)(2,1)S(1)} %get-tuple-element.95), channel_id=1, source_target_pairs={{0,8},{8,16},{16,24},{24,0},{1,9},{9,17},{17,25},{25,1},{2,10},{10... | collective-permute-start | bytes 663560 | tf_op jit(solution)/shard_map/ppermute | solution.py:522
  70.1 11.4 %collective-permute-start.21 = (bf16[2,144,384]{2,1,0:T(8,128)(2,1)S(1)}, bf16[2,144,384]{2,1,0:T(8,128)(2,1)S(1)}, u32[]{:S(2)}, u32[]{:S(2)}) collective-permute-start(bf16[2,144,384]{2,1,0:T(8,128)(2,1)S(1)} %get-tuple-element.96), channel_id=1, source_target_pairs={{0,24},{8,0},{16,8},{24,16},{1,25},{9,1},{17,9},{25,17},{2,26},{10... | collective-permute-start | bytes 663560 | tf_op jit(solution)/shard_map/ppermute | solution.py:523
  73.1 8.4 %collective-permute-start.22 = (bf16[2,144,384]{2,1,0:T(8,128)(2,1)S(1)}, bf16[2,144,384]{2,1,0:T(8,128)(2,1)S(1)}, u32[]{:S(2)}, u32[]{:S(2)}) collective-permute-start(bf16[2,144,384]{2,1,0:T(8,128)(2,1)S(1)} %get-tuple-element.97), channel_id=1, source_target_pairs={{0,16},{8,24},{16,0},{24,8},{1,17},{9,25},{17,1},{25,9},{2,18},{10... | collective-permute-start | bytes 663560 | tf_op jit(solution)/shard_map/ppermute | solution.py:521
  73.7 7.8 %collective-permute-start.23 = (bf16[128,128]{1,0:T(8,128)(2,1)S(1)}, bf16[128,128]{1,0:T(8,128)(2,1)S(1)}, u32[]{:S(2)}, u32[]{:S(2)}) collective-permute-start(bf16[128,128]{1,0:T(8,128)(2,1)S(1)} %get-tuple-element.100), channel_id=1, source_target_pairs={{0,128},{32,160},{64,192},{96,224},{128,0},{160,32},{192,64},{224,... | collective-permute-start | bytes 98312 | tf_op jit(solution)/shard_map/ppermute | solution.py:530
  85.7 12.4 %collective-permute-start.25 = (bf16[48,2048]{1,0:T(8,128)(2,1)S(1)}, bf16[48,2048]{1,0:T(8,128)(2,1)S(1)}, u32[]{:S(2)}, u32[]{:S(2)}) collective-permute-start(bf16[48,2048]{1,0:T(8,128)(2,1)S(1)} %get-tuple-element.106), channel_id=1, source_target_pairs={{0,2},{2,4},{4,6},{6,0},{1,3},{3,5},{5,7},{7,1},{8,10},{10,12},{12... | collective-permute-start | bytes 589832 | tf_op jit(solution)/shard_map/ppermute | solution.py:553
  86.8 11.3 %collective-permute-start.26 = (bf16[48,2048]{1,0:T(8,128)(2,1)S(1)}, bf16[48,2048]{1,0:T(8,128)(2,1)S(1)}, u32[]{:S(2)}, u32[]{:S(2)}) collective-permute-start(bf16[48,2048]{1,0:T(8,128)(2,1)S(1)} %get-tuple-element.107), channel_id=1, source_target_pairs={{0,6},{2,0},{4,2},{6,4},{1,7},{3,1},{5,3},{7,5},{8,14},{10,8},{12,... | collective-permute-start | bytes 589832 | tf_op jit(solution)/shard_map/ppermute | solution.py:554
  89.0 9.1 %collective-permute-start.27 = (bf16[48,2048]{1,0:T(8,128)(2,1)S(1)}, bf16[48,2048]{1,0:T(8,128)(2,1)S(1)}, u32[]{:S(2)}, u32[]{:S(2)}) collective-permute-start(bf16[48,2048]{1,0:T(8,128)(2,1)S(1)} %get-tuple-element.108), channel_id=1, source_target_pairs={{0,4},{2,6},{4,0},{6,2},{1,5},{3,7},{5,1},{7,3},{8,12},{10,14},{12... | collective-permute-start | bytes 589832 | tf_op jit(solution)/shard_map/ppermute | solution.py:555
  (15 other events, 83.4 us)
